TPU v7x, 128 devices: a whole 4x4x4 slice. The times are simulated.
128 devices in a mesh: sp: 16 (over z, x), dp: 8 (over y, core).
Axes of the slice: x: 4, y: 4, z: 4, core: 2. Of those that a mesh axis runs over, the one named last changes fastest.
Arguments:
- residual: bfloat16 [8, 2048, 2048], P('dp', 'sp'), may hold values from -6 to 6
- query: bfloat16 [8, 2048, 2048], P('dp', 'sp'), may hold values from -6 to 6
- key: bfloat16 [8, 2048, 2048], P('dp', 'sp'), may hold values from -6 to 6
- value: bfloat16 [8, 2048, 2048], P('dp', 'sp'), may hold values from -6 to 6
- output_gate_input: bfloat16 [8, 2048, 2048], P('dp', 'sp'), may hold values from -6 to 6
- write_strength_logit: bfloat16 [8, 2048, 16], P('dp', 'sp'), may hold values from -6 to 6
- decay_head_input: bfloat16 [8, 2048, 16], P('dp', 'sp'), may hold values from -5 to 5
- added_log_decay: float32 [8, 16, 2048], P('dp', 'sp'), may hold values from -2 to 0
- head_decay_rate: float32 [16], P('sp'), may hold values from 0 to 1
- head_norm_gain: float32 [128], replicated, may hold values from 0.1 to 1.9
- output_projection: bfloat16 [2048, 2048], P(None, 'dp'), may hold values from -0.125 to 0.125
- mixer_norm_gain: float32 [2048], replicated, may hold values from 0.1 to 1.9
- token_expert_index: int32 [8, 2048, 4], P('dp', 'sp'), may hold values from 0 to 127, all different within a row; in each aligned block of 128 rows (0 to 127, 128 to 255, ..., all dimensions but the last counted through in order) at most 6 rows name the same one
- token_expert_weight: float32 [8, 2048, 4], P('dp', 'sp'), may hold values from 0.1 to 0.6
- expert_gate_weight: bfloat16 [128, 2048, 1024], P(('sp', 'dp')), may hold values from -1 to 1
- expert_up_weight: bfloat16 [128, 2048, 1024], P(('sp', 'dp')), may hold values from -1 to 1
- expert_down_weight: bfloat16 [128, 1024, 2048], P(('sp', 'dp')), may hold values from -0.1875 to 0.1875
- feedforward_norm_gain: float32 [2048], replicated, may hold values from 0.1 to 1.9
Outputs:
- blended: float32 [8, 2048, 2048], P('dp', 'sp')
Inputs may be any that keep to these rules, and one draw needn't show every extreme that they name: `token_expert_index`: each row names 4 different experts; within the 128 rows of one device no expert is named by more than 6 rows, and in every draw some expert is named by exactly 6 rows of some device.
All inputs are finite; a program needn't handle non-finite values.
Results may differ from a plain program's by a relative error of at most 0.0062.
Values may be sent and summed in bfloat16 or wider, within the bound.
No kernel may reach another device: no remote copies, remote signals or barrier semaphores. Data moves between devices by JAX's collectives and lax.ppermute only.
A program may use at most 128 MiB of HBM per device.

v0:
```python
import jax
import jax.numpy as jnp
from jax import lax
from jax.experimental import pallas as pl
from jax.experimental.pallas import tpu as pltpu
from jax.sharding import Mesh
from jax.sharding import PartitionSpec as P

DP = ("dp_0", "dp_1")
SP_DP = ("sp", "dp_0", "dp_1")
CLAMP_LIMIT = 7.0
SWISH_SLOPE = 1.702
F32 = jnp.float32
BF16 = jnp.bfloat16
HIGHEST = lax.Precision.HIGHEST
C = 128
EXTRA = 16
VMEM = pl.BlockSpec(memory_space=pltpu.VMEM)
SMEM = pl.BlockSpec(memory_space=pltpu.SMEM)
HBM = pl.BlockSpec(memory_space=pl.ANY)


def dot(a, b):
    return jnp.dot(a, b, preferred_element_type=F32)


def dot_nt(a, b, precision=None):
    return lax.dot_general(
        a, b, (((1,), (1,)), ((), ())), precision=precision, preferred_element_type=F32
    )


def dot_tn(a, b):
    return lax.dot_general(a, b, (((0,), (0,)), ((), ())), preferred_element_type=F32)


def halves(x):
    high = x.astype(BF16)
    return high, (x - high.astype(F32)).astype(BF16)


def iotas(rows, columns):
    shape = (rows, columns)
    return lax.broadcasted_iota(jnp.int32, shape, 0), lax.broadcasted_iota(jnp.int32, shape, 1)


def swap_matrix():
    row, column = iotas(256, 256)
    return jnp.where((row % 16) * 16 + row // 16 == column, 1.0, 0.0).astype(BF16)


def pack_kernel(q_ref, k_ref, v_ref, logit_ref, decay_ref, out_ref):
    heads = out_ref.shape[0]
    row, column = iotas(heads, heads)
    eye = jnp.where(row == column, 1.0, 0.0).astype(BF16)
    logits = dot_nt(eye, logit_ref[0])
    decays = dot_nt(eye, decay_ref[0])
    extra_row, _unused = iotas(EXTRA, C)
    for h in range(heads):
        columns = slice(h * C, (h + 1) * C)
        out_ref[h, 0:C] = k_ref[0, :, columns]
        out_ref[h, C : 2 * C] = q_ref[0, :, columns]
        out_ref[h, 2 * C : 3 * C] = v_ref[0, :, columns]
        extra = jnp.where(extra_row == 0, logits[h : h + 1], decays[h : h + 1])
        out_ref[h, 3 * C : 3 * C + EXTRA] = extra.astype(BF16)


def pack(query, key, value, logit, decay_input):
    heads = logit.shape[2]
    return pl.pallas_call(
        pack_kernel,
        out_shape=jax.ShapeDtypeStruct((heads, 3 * C + EXTRA, C), BF16),
        in_specs=[VMEM] * 5,
        out_specs=VMEM,
        name="pack",
    )(query, key, value, logit, decay_input)


GROUP = 4


def delta_kernel(
    x_ref, added_ref, rate_ref, out_ref,
    a_ref, b_ref, qe_ref, su_ref, cum_col_ref, cum_row_ref, write_col_ref, write_row_ref,
):
    chunks = x_ref.shape[0]
    row, column = iotas(C, C)
    inclusive = row >= column
    strict = row > column
    diagonal = row == column

    chunk_row, _unused = iotas(chunks, C)
    logits = jnp.zeros((chunks, C), F32)
    decays = jnp.zeros((chunks, C), F32)
    for n in range(chunks):
        extra = x_ref[n, 3 * C : 3 * C + EXTRA].astype(F32)
        logits = jnp.where(chunk_row == n, extra[0:1], logits)
        decays = jnp.where(chunk_row == n, extra[1:2], decays)
    softplus = jnp.maximum(decays, 0.0) + jnp.log(1.0 + jnp.exp(-jnp.abs(decays)))
    log_decay = added_ref[...] - rate_ref[0] * softplus
    upper = jnp.where(row <= column, 1.0, 0.0)
    lower = jnp.where(row >= column, 1.0, 0.0)
    eye = jnp.where(diagonal, 1.0, 0.0)
    cum_row_ref[...] = jnp.dot(log_decay, upper, precision=HIGHEST, preferred_element_type=F32)
    cum_col_ref[...] = dot_nt(lower, log_decay, precision=HIGHEST)
    write = 1.0 / (1.0 + jnp.exp(-logits))
    write_row_ref[...] = write
    write_col_ref[...] = dot_nt(eye, write, precision=HIGHEST)

    def column_of(ref, n):
        lane = lax.broadcasted_iota(jnp.int32, (C, ref.shape[1]), 1)
        return jnp.sum(jnp.where(lane == n, ref[...], 0.0), axis=1, keepdims=True)

    def prepare(n):
        keys = x_ref[n, 0:C]
        queries = x_ref[n, C : 2 * C]
        values = x_ref[n, 2 * C : 3 * C]
        cum_c = column_of(cum_col_ref, n)
        write_c = column_of(write_col_ref, n)
        cum_r = cum_row_ref[pl.ds(n, 1), :]
        write_r = write_row_ref[pl.ds(n, 1), :]
        products = dot_nt(jnp.concatenate([keys, queries], axis=0), keys)
        keys_dot, scores = products[:C], products[C:]
        squares = jnp.where(diagonal, keys_dot, 0.0)
        key_c = lax.rsqrt(jnp.sum(squares, axis=1, keepdims=True) + 1e-06)
        key_r = lax.rsqrt(jnp.sum(squares, axis=0, keepdims=True) + 1e-06)
        q32 = queries.astype(F32)
        query_c = lax.rsqrt(jnp.sum(q32 * q32, axis=1, keepdims=True) + 1e-06) * C ** (-0.5)
        within = jnp.exp(jnp.where(inclusive, cum_c - cum_r, -jnp.inf)) * key_r
        lower_part = jnp.where(strict, keys_dot * within * (write_c * key_c), 0.0)
        scores = scores * within * query_c

        high, low = halves(lower_part)
        left = jnp.concatenate([high, low], axis=1)
        pair = (row // 2 == column // 2) & strict
        inverse = jnp.where(pair, -lower_part, eye)
        size = 2
        while size < C:
            high, low = halves(inverse)
            first = dot(left, jnp.concatenate([high, high], axis=0))
            first_high, first_low = halves(first)
            second = dot(
                jnp.concatenate([high, high], axis=1),
                jnp.concatenate([first_high, first_low], axis=0),
            )
            joined = (row // (2 * size) == column // (2 * size)) & (row // size > column // size)
            inverse = jnp.where(joined, -second, inverse)
            size *= 2

        decay_r = jnp.exp(cum_r)
        base_high, base_low = halves(inverse * write_r)
        base = dot(
            jnp.concatenate([base_high, base_low], axis=1),
            jnp.concatenate([values, values], axis=0),
        )
        weight_high, weight_low = halves(inverse * (write_r * decay_r * key_r))
        weight = dot(
            jnp.concatenate([weight_high, weight_low], axis=1),
            jnp.concatenate([keys, keys], axis=0),
        )
        last = cum_c[C - 1 : C]
        both = jnp.concatenate([base, weight], axis=1)
        carried_high, carried_low = halves(both * (key_c * jnp.exp(last - cum_c)))
        keys_t = keys.T
        update = dot(
            jnp.concatenate([keys_t, keys_t], axis=1),
            jnp.concatenate([carried_high, carried_low], axis=0),
        )
        b_ref[n] = update[:, :C]
        a_ref[n] = jnp.where(diagonal, jnp.exp(last), 0.0) - update[:, C:]
        score_high, score_low = halves(scores)
        both = both.astype(BF16)
        seen = dot(
            jnp.concatenate([score_high, score_low], axis=1),
            jnp.concatenate([both, both], axis=0),
        )
        su_ref[n] = seen[:, :C]
        qe_ref[n] = q32 * (query_c * jnp.exp(cum_c)) - seen[:, C:]

    def group(g, carry):
        for k in range(GROUP):
            prepare(g * GROUP + k)
        return carry

    lax.fori_loop(0, chunks // GROUP, group, 0)

    def advance(n, state):
        high, low = halves(state)
        both = jnp.concatenate([high, low], axis=0)
        q_high, q_low = halves(qe_ref[n])
        out = dot(jnp.concatenate([q_high, q_high], axis=1), both) + su_ref[n]
        scale = lax.rsqrt(jnp.mean(out * out, axis=1, keepdims=True) + 1e-05)
        out_ref[n] = (out * scale).astype(BF16)
        a_high, a_low = halves(a_ref[n])
        return (
            dot(jnp.concatenate([a_high, a_high], axis=1), both) + dot(a_low, high) + b_ref[n]
        )

    def steps(g, state):
        for k in range(2):
            state = advance(g * 2 + k, state)
        return state

    lax.fori_loop(0, chunks // 2, steps, jnp.zeros((C, C), F32))


def delta(blocks, added, decay_rate):
    chunks = blocks.shape[0]
    return pl.pallas_call(
        delta_kernel,
        out_shape=jax.ShapeDtypeStruct((chunks, C, C), BF16),
        in_specs=[VMEM, VMEM, SMEM],
        out_specs=VMEM,
        scratch_shapes=[pltpu.VMEM((chunks, C, C), F32)] * 4
        + [
            pltpu.VMEM((C, chunks), F32),
            pltpu.VMEM((chunks, C), F32),
            pltpu.VMEM((C, chunks), F32),
            pltpu.VMEM((chunks, C), F32),
        ],
        cost_estimate=pl.CostEstimate(flops=4 * 10**9, bytes_accessed=2**21, transcendentals=0),
        name="delta",
    )(blocks, added, decay_rate)


def slots_kernel(index_ref, dest_ref, source_ref, count_ref):
    experts = count_ref.shape[0]
    capacity = source_ref.shape[0] // experts

    def clear(e, carry):
        count_ref[e] = 0
        for k in range(capacity):
            source_ref[e * capacity + k] = 0
        return carry

    lax.fori_loop(0, experts, clear, 0)

    def place(t, carry):
        for k in range(4):
            e = index_ref[t * 4 + k]
            used = count_ref[e]
            count_ref[e] = used + 1
            slot = e * capacity + used
            dest_ref[t * 4 + k] = slot
            source_ref[slot] = t
        return carry

    lax.fori_loop(0, index_ref.shape[0] // 4, place, 0)


def slots(index, experts, capacity):
    return pl.pallas_call(
        slots_kernel,
        out_shape=(
            jax.ShapeDtypeStruct(index.shape, jnp.int32),
            jax.ShapeDtypeStruct((experts * capacity,), jnp.int32),
        ),
        in_specs=[SMEM],
        out_specs=(SMEM, SMEM),
        scratch_shapes=[pltpu.SMEM((experts,), jnp.int32)],
        name="slots",
    )(index)


def project_kernel(
    rec_ref, gate_ref, head_gain_ref, residual_ref, gain_ref, source_ref, place_ref,
    *rest,
):
    weight_refs = rest[:8]
    normed_ref, out_ref, gated_ref, mixed_ref, w_ref, sems = rest[8:]
    copies = [
        pltpu.make_async_copy(weight_refs[k], w_ref.at[k], sems.at[k]) for k in range(8)
    ]
    for copy in copies:
        copy.start()
    heads = rec_ref.shape[0]
    head_gain = head_gain_ref[...]
    for h in range(heads):
        columns = slice(h * C, (h + 1) * C)
        gate = gate_ref[0, :, columns].astype(F32)
        gate = gate / (1.0 + jnp.exp(-gate))
        gated_ref[:, columns] = (rec_ref[h].astype(F32) * head_gain * gate).astype(BF16)
    for k in range(8):
        copies[k].wait()
        mixed_ref[place_ref[k]] = dot(gated_ref[...], w_ref[k])
    total = jnp.concatenate([mixed_ref[k] for k in range(8)], axis=1)
    total = total + residual_ref[0].astype(F32)
    centred = total - jnp.mean(total, axis=1, keepdims=True)
    variance = jnp.mean(centred * centred, axis=1, keepdims=True)
    normed = (centred * lax.rsqrt(variance + 1e-05) * gain_ref[...]).astype(BF16)
    swap = swap_matrix()
    tiles = normed.shape[1] // C
    for g in range(normed.shape[0] // 16):
        rows = normed[g * 16 : (g + 1) * 16]
        stacked = jnp.concatenate([rows[:, j * C : (j + 1) * C] for j in range(tiles)], axis=0)
        turned = dot(swap, stacked).astype(BF16)
        normed_ref[g * 16 : (g + 1) * 16] = turned.reshape(16, tiles, C)

    def send(i, carry):
        for k in range(16):
            slot = i * 16 + k
            out_ref[slot] = normed_ref[source_ref[slot]]
        return carry

    lax.fori_loop(0, out_ref.shape[0] // 16, send, 0)


def project(recurrent, gate, head_gain, residual, gain, source, place, weights):
    tokens = residual.shape[1]
    features = residual.shape[2]
    tiles = features // C
    return pl.pallas_call(
        project_kernel,
        out_shape=(
            jax.ShapeDtypeStruct((tokens, tiles, C), BF16),
            jax.ShapeDtypeStruct((source.shape[0], tiles, C), BF16),
        ),
        in_specs=[VMEM] * 5 + [SMEM] * 2 + [HBM] * 8,
        out_specs=(VMEM, VMEM),
        scratch_shapes=[
            pltpu.VMEM((tokens, features), BF16),
            pltpu.VMEM((8, tokens, features // 8), F32),
            pltpu.VMEM((8, features, features // 8), BF16),
            pltpu.SemaphoreType.DMA((8,)),
        ],
        cost_estimate=pl.CostEstimate(flops=10**9, bytes_accessed=2**24, transcendentals=0),
        name="project",
    )(recurrent, gate, head_gain, residual, gain, source, place, *weights)


FF_BLOCK = 256


def expert_kernel(x_ref, gate_ref, up_ref, down_ref, out_ref, rows_ref, hidden_ref, made_ref):
    step = pl.program_id(0)
    slots_ = x_ref.shape[0]
    tiles = x_ref.shape[1]
    groups = slots_ // 16
    ff_steps = hidden_ref.shape[0]

    @pl.when(step == 0)
    def _():
        swap = swap_matrix()

        def turn(i, carry):
            for k in range(4):
                start = pl.multiple_of((i * 4 + k) * 16, 16)
                turned = dot(swap, x_ref[pl.ds(start, 16)].reshape(16 * tiles, C)).astype(BF16)
                for j in range(tiles):
                    rows_ref[pl.ds(start, 16), j * C : (j + 1) * C] = turned[j * 16 : (j + 1) * 16]
            return carry

        lax.fori_loop(0, groups // 4, turn, 0)

    @pl.when(step < ff_steps)
    def _():
        rows = rows_ref[...]
        gate = jnp.minimum(dot(rows, gate_ref[...]), CLAMP_LIMIT)
        up = jnp.clip(dot(rows, up_ref[...]), -CLAMP_LIMIT, CLAMP_LIMIT)
        hidden = gate / (1.0 + jnp.exp(-SWISH_SLOPE * gate)) * (up + 1.0)
        hidden_ref[step] = hidden.astype(BF16)

    @pl.when(step >= ff_steps)
    def _():
        total = dot(hidden_ref[0], down_ref[0:FF_BLOCK])
        for k in range(1, ff_steps):
            total = total + dot(hidden_ref[k], down_ref[k * FF_BLOCK : (k + 1) * FF_BLOCK])
        made_ref[step - ff_steps] = total.astype(BF16)

    @pl.when(step == pl.num_programs(0) - 1)
    def _():
        swap = swap_matrix()
        down_steps, _rows, width = made_ref.shape

        def turn(i, carry):
            for k in range(2):
                start = pl.multiple_of((i * 2 + k) * 16, 16)
                pieces = []
                for d in range(down_steps):
                    piece = made_ref[d, pl.ds(start, 16), :]
                    pieces += [piece[:, j * C : (j + 1) * C] for j in range(width // C)]
                turned = dot(swap, jnp.concatenate(pieces, axis=0)).astype(BF16)
                out_ref[pl.ds(start, 16)] = turned.reshape(16, tiles, C)
            return carry

        lax.fori_loop(0, groups // 2, turn, 0)


def expert(rows, gate_weight, up_weight, down_weight):
    slots_, tiles, _lanes = rows.shape
    features, hidden = gate_weight.shape
    ff_steps = hidden // FF_BLOCK
    width = 512
    down_steps = features // width
    return pl.pallas_call(
        expert_kernel,
        grid=(ff_steps + down_steps,),
        out_shape=jax.ShapeDtypeStruct(rows.shape, BF16),
        in_specs=[
            pl.BlockSpec(rows.shape, lambda i: (0, 0, 0), pipeline_mode=pl.Buffered(1)),
            pl.BlockSpec((features, FF_BLOCK), lambda i: (0, jnp.minimum(i, ff_steps - 1))),
            pl.BlockSpec((features, FF_BLOCK), lambda i: (0, jnp.minimum(i, ff_steps - 1))),
            pl.BlockSpec((hidden, width), lambda i: (0, jnp.maximum(i - ff_steps, 0))),
        ],
        out_specs=pl.BlockSpec(rows.shape, lambda i: (0, 0, 0), pipeline_mode=pl.Buffered(1)),
        scratch_shapes=[
            pltpu.VMEM((slots_, features), BF16),
            pltpu.VMEM((ff_steps, slots_, FF_BLOCK), BF16),
            pltpu.VMEM((down_steps, slots_, width), BF16),
        ],
        compiler_params=pltpu.CompilerParams(dimension_semantics=("arbitrary",)),
        cost_estimate=pl.CostEstimate(flops=10**10, bytes_accessed=2**24, transcendentals=0),
        name="expert",
    )(rows, gate_weight, up_weight, down_weight)


def combine_kernel(back_ref, normed_ref, gain_ref, dest_ref, weight_ref, out_ref, z_ref):
    tokens, tiles, _lanes = normed_ref.shape
    features = tiles * C
    gain = gain_ref[...]

    def token(t):
        total = normed_ref[t].astype(F32)
        for k in range(4):
            slot = dest_ref[t * 4 + k]
            total = total + weight_ref[t * 4 + k] * back_ref[slot].astype(F32)
        centred = total - jnp.sum(total, keepdims=True) * (1.0 / features)
        variance = jnp.sum(centred * centred, keepdims=True) * (1.0 / features)
        z_ref[t] = centred * lax.rsqrt(variance + 1e-05) * gain

    def some(i, carry):
        for k in range(8):
            token(i * 8 + k)
        return carry

    lax.fori_loop(0, tokens // 8, some, 0)
    swap = swap_matrix()
    for g in range(tokens // 16):
        z = z_ref[g * 16 : (g + 1) * 16].reshape(16 * tiles, C)
        high = z.astype(BF16)
        rest = z - high.astype(F32)
        middle = rest.astype(BF16)
        low = (rest - middle.astype(F32)).astype(BF16)
        turned = dot(swap, high) + dot(swap, middle) + dot(swap, low)
        for j in range(tiles):
            out_ref[0, g * 16 : (g + 1) * 16, j * C : (j + 1) * C] = turned[j * 16 : (j + 1) * 16]


def combine(back, normed, gain, dest, weight):
    tokens, tiles, _lanes = normed.shape
    return pl.pallas_call(
        combine_kernel,
        out_shape=jax.ShapeDtypeStruct((1, tokens, tiles * C), F32),
        in_specs=[VMEM] * 3 + [SMEM] * 2,
        out_specs=VMEM,
        scratch_shapes=[pltpu.VMEM((tokens, tiles, C), F32)],
        name="combine",
    )(back, normed, gain, dest, weight)


def gathered(block):
    y_size, core_size = lax.axis_size("dp_0"), lax.axis_size("dp_1")
    y, core = lax.axis_index("dp_0"), lax.axis_index("dp_1")
    found = [block]
    for shift in range(1, y_size):
        pairs = [(i, (i + shift) % y_size) for i in range(y_size)]
        found.append(lax.ppermute(block, "dp_0", pairs))
    places = [((y - shift) % y_size) * core_size + core for shift in range(y_size)]
    swapped = [lax.ppermute(b, "dp_1", [(0, 1), (1, 0)]) for b in found]
    others = [((y - shift) % y_size) * core_size + 1 - core for shift in range(y_size)]
    return found + swapped, jnp.stack(places + others).astype(jnp.int32)


def per_device(
    residual,
    query,
    key,
    value,
    output_gate_input,
    write_strength_logit,
    decay_head_input,
    added_log_decay,
    head_decay_rate,
    head_norm_gain,
    output_projection,
    mixer_norm_gain,
    token_expert_index,
    token_expert_weight,
    expert_gate_weight,
    expert_up_weight,
    expert_down_weight,
    feedforward_norm_gain,
):
    experts = lax.axis_size(SP_DP)
    tokens, features = residual.shape[1:]
    picks = token_expert_index.shape[2]
    capacity = tokens * picks * 3 // (2 * experts)
    tiles = features // C
    weights, places = gathered(output_projection)
    dest, source = slots(token_expert_index.reshape(-1), experts, capacity)
    blocks = pack(query, key, value, write_strength_logit, decay_head_input)
    blocks = lax.all_to_all(blocks, "sp", split_axis=0, concat_axis=0, tiled=True)
    recurrent = delta(blocks, added_log_decay.reshape(-1, C), head_decay_rate)
    returned = lax.all_to_all(recurrent, "sp", split_axis=0, concat_axis=0, tiled=True)
    normed, rows = project(
        returned,
        output_gate_input,
        head_norm_gain.reshape(1, C),
        residual,
        mixer_norm_gain.reshape(1, features),
        source,
        places,
        weights,
    )
    rows = rows.reshape(experts, capacity * tiles, C)
    rows = lax.all_to_all(rows, SP_DP, split_axis=0, concat_axis=0, tiled=True)
    made = expert(
        rows.reshape(experts * capacity, tiles, C),
        expert_gate_weight[0],
        expert_up_weight[0],
        expert_down_weight[0],
    )
    made = made.reshape(experts, capacity * tiles, C)
    back = lax.all_to_all(made, SP_DP, split_axis=0, concat_axis=0, tiled=True)
    return combine(
        back.reshape(experts * capacity, tiles, C),
        normed,
        feedforward_norm_gain.reshape(tiles, C),
        dest,
        token_expert_weight.reshape(-1),
    )


def solution(mesh):
    torus = Mesh(mesh.devices.reshape(mesh.shape["sp"], 4, 2), ("sp", "dp_0", "dp_1"))
    return jax.shard_map(
        per_device,
        mesh=torus,
        in_specs=(
            P(DP, "sp", None),
            P(DP, "sp", None),
            P(DP, "sp", None),
            P(DP, "sp", None),
            P(DP, "sp", None),
            P(DP, "sp", None),
            P(DP, "sp", None),
            P(DP, "sp", None),
            P("sp"),
            P(),
            P(None, DP),
            P(),
            P(DP, "sp", None),
            P(DP, "sp", None),
            P(SP_DP, None, None),
            P(SP_DP, None, None),
            P(SP_DP, None, None),
            P(),
        ),
        out_specs=P(DP, "sp", None),
        check_vma=False,
    )
```

profile of v0, /device:TPU:1, one launch (start us, length us, event | category | flops | bytes accessed | tf_op | source)
XLA Modules:
  0.0 281.3 jit_solution(13730421633433116982)
XLA Ops:
  0.0 1.4 copy.21.logit_ref
  1.4 1.4 copy.22.decay_ref
  2.8 0.0 copy-start.3
  2.8 2.9 %pack.1 = bf16[16,400,128]{2,1,0:T(8,128)(2,1)} custom-call(bf16[1,128,2048]{2,1,0:T(8,128)(2,1)} %q_ref.1, bf16[1,128,2048]{2,1,0:T(8,128)(2,1)} %k_ref.1, bf16[1,128,2048]{2,1,0:T(8,128)(2,1)} %v_ref.1, bf16[1,128,16]{2,1,0:T(8,128)(2,1)} %copy.21.logit_ref, bf16[1,128,16]{2,1,0:T(8,128)(2,1)} %copy.22.decay_ref), custom_call_target="tpu_custom_call" | custom-call | tf_op jit(solution)/shard_map/pack/pallas_call | solution.py:70
  5.7 8.4 %all-to-all-start = ((bf16[16,400,128]{2,1,0:T(8,128)(2,1)}), bf16[16,400,128]{2,1,0:T(8,128)(2,1)S(1)}, u32[]{:S(2)}, u32[]{:S(2)}) async-start(bf16[16,400,128]{2,1,0:T(8,128)(2,1)} %pack.1), calls=%async_computation | async-start | bytes 3276800 | tf_op jit(solution)/shard_map/all_to_all | solution.py:502
  14.2 0.0 copy-done.3
  14.2 1.4 collective-permute-start
  15.5 2.6 collective-permute-start.1
  18.2 1.1 collective-permute-start.2
  19.2 1.8 collective-permute-start.3
  21.0 18.4 %collective-permute-done.rest_1_ = bf16[2048,256]{1,0:T(8,128)(2,1)} collective-permute-done((bf16[2048,256]{1,0:T(8,128)(2,1)S(1)}, bf16[2048,256]{1,0:T(8,128)(2,1)}, u32[]{:S(2)}, u32[]{:S(2)}) %collective-permute-start) | collective-permute-done | bytes 1048608 | tf_op jit(solution)/shard_map/ppermute | solution.py:467
  39.5 2.0 collective-permute-start.4
  41.4 21.6 %collective-permute-done.1.rest_2_ = bf16[2048,256]{1,0:T(8,128)(2,1)} collective-permute-done((bf16[2048,256]{1,0:T(8,128)(2,1)S(1)}, bf16[2048,256]{1,0:T(8,128)(2,1)}, u32[]{:S(2)}, u32[]{:S(2)}) %collective-permute-start.1) | collective-permute-done | bytes 1048608 | tf_op jit(solution)/shard_map/ppermute | solution.py:467
  63.0 1.8 collective-permute-start.5
  64.8 0.0 collective-permute-done.2.rest_3_
  64.9 0.0 collective-permute-start.6
  65.5 0.0 all-to-all-done.x_ref
  65.5 0.0 copy-start.2
  65.5 1.2 copy-done.2
  66.7 0.0 copy-start.4
  66.7 43.0 %delta.1 = bf16[16,128,128]{2,1,0:T(8,128)(2,1)} custom-call(bf16[16,400,128]{2,1,0:T(8,128)(2,1)} %copy-done.2, f32[16,128]{1,0:T(8,128)} %bitcast.29, f32[1]{0:T(128)S(6)} %copy.25.rate_ref), custom_call_target="tpu_custom_call" | custom-call | flops 4000000000 | bytes 2097152 | tf_op jit(solution)/shard_map/delta/pallas_call | solution.py:209
  109.7 6.7 %all-to-all-start.1 = ((bf16[16,128,128]{2,1,0:T(8,128)(2,1)}), bf16[16,128,128]{2,1,0:T(8,128)(2,1)S(1)}, u32[]{:S(2)}, u32[]{:S(2)}) async-start(bf16[16,128,128]{2,1,0:T(8,128)(2,1)} %delta.1), calls=%async_computation.1 | async-start | bytes 1048576 | tf_op jit(solution)/shard_map/all_to_all | solution.py:504
  116.5 0.0 copy-done.4
  116.5 0.1 copy.23
  116.6 0.6 reshape.33.index_ref
  117.2 6.2 %slots.1 = (s32[512]{0:T(512)}, s32[768]{0:T(1024)}) custom-call(s32[512]{0:T(512)} %reshape.33.index_ref), custom_call_target="tpu_custom_call" | custom-call | tf_op jit(solution)/shard_map/slots/pallas_call | solution.py:252
  123.4 0.7 stack.35.place_ref
  124.1 0.0 collective-permute-done.3.rest_4_
  124.1 2.9 %all-to-all-done.1.rec_ref = bf16[16,128,128]{2,1,0:T(8,128)(2,1)S(1)} async-done(((bf16[16,128,128]{2,1,0:T(8,128)(2,1)}), bf16[16,128,128]{2,1,0:T(8,128)(2,1)S(1)}, u32[]{:S(2)}, u32[]{:S(2)}) %all-to-all-start.1) | async-done | bytes 524320 | tf_op jit(solution)/shard_map/all_to_all | solution.py:504
  127.0 0.0 copy-start.1
  127.0 0.0 collective-permute-done.4.rest_5_
  127.0 0.0 collective-permute-done.5.rest_6_
  127.0 0.0 collective-permute-done.6.rest_7_
  127.0 0.8 copy-done.1
  127.8 9.8 %project.1 = (bf16[128,16,128]{2,1,0:T(8,128)(2,1)}, bf16[768,16,128]{2,1,0:T(8,128)(2,1)}) custom-call(bf16[16,128,128]{2,1,0:T(8,128)(2,1)} %copy-done.1, bf16[1,128,2048]{2,1,0:T(8,128)(2,1)} %gate_ref.1, f32[1,128]{1,0:T(1,128)} %bitcast.25, bf16[1,128,2048]{2,1,0:T(8,128)(2,1)} %residual_ref.1, f32[1,2048]{1,0:T(1,128)} %bitcast.24, ...), custom_call_target="tpu_custom_call" | custom-call | flops 1000000000 | bytes 16777216 | tf_op jit(solution)/shard_map/project/pallas_call | solution.py:312
  137.6 48.2 %all_to_all.20 = bf16[128,96,128]{2,1,0:T(8,128)(2,1)} all-to-all(bf16[128,96,128]{2,1,0:T(8,128)(2,1)} %bitcast.20), channel_id=1, replica_groups=mesh['sp'=16,'dp_0'=4,'dp_1'=2] {'sp','dp_0','dp_1'}, dimensions={0} | all-to-all | bytes 6291456 | tf_op jit(solution)/shard_map/all_to_all | solution.py:516
  185.8 26.0 %expert.1 = bf16[768,16,128]{2,1,0:T(8,128)(2,1)} custom-call(bf16[768,16,128]{2,1,0:T(8,128)(2,1)} %bitcast.22, bf16[2048,1024]{1,0:T(8,128)(2,1)} %bitcast.26, bf16[2048,1024]{1,0:T(8,128)(2,1)} %bitcast.27, bf16[1024,2048]{1,0:T(8,128)(2,1)} %bitcast.28), custom_call_target="tpu_custom_call" | custom-call | flops 10000000000 | bytes 16777216 | tf_op jit(solution)/shard_map/expert/pallas_call | solution.py:395
  211.8 0.0 copy-start.5
  211.8 4.6 %all-to-all-start.3 = ((bf16[128,96,128]{2,1,0:T(8,128)(2,1)}), bf16[128,96,128]{2,1,0:T(8,128)(2,1)S(1)}, u32[]{:S(2)}, u32[]{:S(2)}) async-start(bf16[128,96,128]{2,1,0:T(8,128)(2,1)} %bitcast.21), calls=%async_computation.3 | async-start | bytes 6291456 | tf_op jit(solution)/shard_map/all_to_all | solution.py:524
  216.4 0.0 copy-done.5
  216.4 0.1 copy.24
  216.5 0.7 reshape.39.weight_ref
  217.2 41.0 %all-to-all-done.3 = bf16[128,96,128]{2,1,0:T(8,128)(2,1)S(1)} async-done(((bf16[128,96,128]{2,1,0:T(8,128)(2,1)}), bf16[128,96,128]{2,1,0:T(8,128)(2,1)S(1)}, u32[]{:S(2)}, u32[]{:S(2)}) %all-to-all-start.3) | async-done | bytes 3145760 | tf_op jit(solution)/shard_map/all_to_all | solution.py:524
  258.2 0.0 copy-start
  258.2 1.7 copy-done
  259.8 21.5 %combine.1 = f32[1,128,2048]{2,1,0:T(8,128)} custom-call(bf16[768,16,128]{2,1,0:T(8,128)(2,1)} %bitcast.19, bf16[128,16,128]{2,1,0:T(8,128)(2,1)} %get-tuple-element.11.normed_ref, f32[16,128]{1,0:T(8,128)} %bitcast.23, s32[512]{0:T(512)} %get-tuple-element.12.dest_ref, f32[512]{0:T(512)} %reshape.39.weight_ref), custom_call_target="tpu_custom_call" | custom-call | tf_op jit(solution)/shard_map/combine/pallas_call | solution.py:451
Async XLA Ops:
  2.8 11.4 %copy-start.3 = (bf16[2048,256]{1,0:T(8,128)(2,1)S(1)}, bf16[2048,256]{1,0:T(8,128)(2,1)}, u32[]{:S(2)}) copy-start(bf16[2048,256]{1,0:T(8,128)(2,1)} %rest_0_.1) | copy-start | bytes 3145732
  5.7 59.8 %all-to-all-start = ((bf16[16,400,128]{2,1,0:T(8,128)(2,1)}), bf16[16,400,128]{2,1,0:T(8,128)(2,1)S(1)}, u32[]{:S(2)}, u32[]{:S(2)}) async-start(bf16[16,400,128]{2,1,0:T(8,128)(2,1)} %pack.1), calls=%async_computation | async-start | bytes 3276800 | tf_op jit(solution)/shard_map/all_to_all | solution.py:502
  14.2 25.3 %collective-permute-start = (bf16[2048,256]{1,0:T(8,128)(2,1)S(1)}, bf16[2048,256]{1,0:T(8,128)(2,1)}, u32[]{:S(2)}, u32[]{:S(2)}) collective-permute-start(bf16[2048,256]{1,0:T(8,128)(2,1)S(1)} %copy-done.3), channel_id=1, source_target_pairs={{0,2},{2,4},{4,6},{6,0},{1,3},{3,5},{5,7},{7,1},{8,10},{10,12},{12... | collective-permute-start | bytes 3145736 | tf_op jit(solution)/shard_map/ppermute | solution.py:467
  15.5 47.5 %collective-permute-start.1 = (bf16[2048,256]{1,0:T(8,128)(2,1)S(1)}, bf16[2048,256]{1,0:T(8,128)(2,1)}, u32[]{:S(2)}, u32[]{:S(2)}) collective-permute-start(bf16[2048,256]{1,0:T(8,128)(2,1)S(1)} %copy-done.3), channel_id=1, source_target_pairs={{0,4},{2,6},{4,0},{6,2},{1,5},{3,7},{5,1},{7,3},{8,12},{10,14},{12... | collective-permute-start | bytes 3145736 | tf_op jit(solution)/shard_map/ppermute | solution.py:467
  18.2 46.7 %collective-permute-start.2 = (bf16[2048,256]{1,0:T(8,128)(2,1)S(1)}, bf16[2048,256]{1,0:T(8,128)(2,1)}, u32[]{:S(2)}, u32[]{:S(2)}) collective-permute-start(bf16[2048,256]{1,0:T(8,128)(2,1)S(1)} %copy-done.3), channel_id=1, source_target_pairs={{0,6},{2,0},{4,2},{6,4},{1,7},{3,1},{5,3},{7,5},{8,14},{10,8},{12,... | collective-permute-start | bytes 3145736 | tf_op jit(solution)/shard_map/ppermute | solution.py:467
  19.2 104.8 %collective-permute-start.3 = (bf16[2048,256]{1,0:T(8,128)(2,1)S(1)}, bf16[2048,256]{1,0:T(8,128)(2,1)}, u32[]{:S(2)}, u32[]{:S(2)}) collective-permute-start(bf16[2048,256]{1,0:T(8,128)(2,1)S(1)} %copy-done.3), channel_id=1, source_target_pairs={{0,1},{1,0},{2,3},{3,2},{4,5},{5,4},{6,7},{7,6},{8,9},{9,8},{10,11... | collective-permute-start | bytes 3145736 | tf_op jit(solution)/shard_map/ppermute | solution.py:469
  39.5 87.5 %collective-permute-start.4 = (bf16[2048,256]{1,0:T(8,128)(2,1)}, bf16[2048,256]{1,0:T(8,128)(2,1)}, u32[]{:S(2)}, u32[]{:S(2)}) collective-permute-start(bf16[2048,256]{1,0:T(8,128)(2,1)} %collective-permute-done.rest_1_), channel_id=1, source_target_pairs={{0,1},{1,0},{2,3},{3,2},{4,5},{5,4},{6,7},{7,6},{8,9},{9,8},{10,11... | collective-permute-start | bytes 3145736 | tf_op jit(solution)/shard_map/ppermute | solution.py:469
  63.0 63.9 %collective-permute-start.5 = (bf16[2048,256]{1,0:T(8,128)(2,1)}, bf16[2048,256]{1,0:T(8,128)(2,1)}, u32[]{:S(2)}, u32[]{:S(2)}) collective-permute-start(bf16[2048,256]{1,0:T(8,128)(2,1)} %collective-permute-done.1.rest_2_), channel_id=1, source_target_pairs={{0,1},{1,0},{2,3},{3,2},{4,5},{5,4},{6,7},{7,6},{8,9},{9,8},{10,11... | collective-permute-start | bytes 3145736 | tf_op jit(solution)/shard_map/ppermute | solution.py:469
  64.9 62.1 %collective-permute-start.6 = (bf16[2048,256]{1,0:T(8,128)(2,1)}, bf16[2048,256]{1,0:T(8,128)(2,1)}, u32[]{:S(2)}, u32[]{:S(2)}) collective-permute-start(bf16[2048,256]{1,0:T(8,128)(2,1)} %collective-permute-done.2.rest_3_), channel_id=1, source_target_pairs={{0,1},{1,0},{2,3},{3,2},{4,5},{5,4},{6,7},{7,6},{8,9},{9,8},{10,11... | collective-permute-start | bytes 3145736 | tf_op jit(solution)/shard_map/ppermute | solution.py:469
  65.5 1.2 copy-start.2
  66.7 49.8 %copy-start.4 = (s32[1,128,4]{1,2,0:T(4,128)S(1)}, s32[1,128,4]{1,2,0:T(4,128)}, u32[]{:S(2)}) copy-start(s32[1,128,4]{1,2,0:T(4,128)} %param.30) | copy-start | bytes 6148
  109.7 17.3 %all-to-all-start.1 = ((bf16[16,128,128]{2,1,0:T(8,128)(2,1)}), bf16[16,128,128]{2,1,0:T(8,128)(2,1)S(1)}, u32[]{:S(2)}, u32[]{:S(2)}) async-start(bf16[16,128,128]{2,1,0:T(8,128)(2,1)} %delta.1), calls=%async_computation.1 | async-start | bytes 1048576 | tf_op jit(solution)/shard_map/all_to_all | solution.py:504
  127.0 0.8 copy-start.1
  211.8 4.6 %copy-start.5 = (f32[1,128,4]{1,2,0:T(4,128)S(1)}, f32[1,128,4]{1,2,0:T(4,128)}, u32[]{:S(2)}) copy-start(f32[1,128,4]{1,2,0:T(4,128)} %param.31) | copy-start | bytes 6148
  211.8 46.4 %all-to-all-start.3 = ((bf16[128,96,128]{2,1,0:T(8,128)(2,1)}), bf16[128,96,128]{2,1,0:T(8,128)(2,1)S(1)}, u32[]{:S(2)}, u32[]{:S(2)}) async-start(bf16[128,96,128]{2,1,0:T(8,128)(2,1)} %bitcast.21), calls=%async_computation.3 | async-start | bytes 6291456 | tf_op jit(solution)/shard_map/all_to_all | solution.py:524
  258.2 1.7 copy-start
where the time goes:
time: 282 us; the launch traced here: 281 us
  Pallas kernels  109 us (39%)
  waiting for transfers between devices  83.9 us (30%)
  blocking collectives  48.2 us (17%)
  starting transfers between devices  30.3 us (11%)
  local copies, waits for them, and re-layouts  8.66 us (3%)
    all_to_all x1, blocking collectives, per_device(): rows = lax.all_to_all(rows, SP_DP, split_axis=0, concat_axis=0, tiled=True)  48.2 us
    pallas_call x1, Pallas kernels, delta(): pl.pallas_call(delta_kernel, out_shape=jax.ShapeDtypeStruct((chunks, C, C...  43 us
    all_to_all x1, waiting for transfers between devices, per_device(): back = lax.all_to_all(made, SP_DP, split_axis=0, concat_axis=0, tiled=True)  41 us
    ppermute x3, waiting for transfers between devices, gathered(): found.append(lax.ppermute(block, 'dp_0', pairs))  40 us
    pallas_call x1, Pallas kernels, expert(): pl.pallas_call(expert_kernel, grid=(ff_steps + down_steps,), out_shape=ja...  26 us
    pallas_call x1, Pallas kernels, combine(): pl.pallas_call(combine_kernel, out_shape=jax.ShapeDtypeStruct((1, tokens,...  21.5 us
    pallas_call x1, Pallas kernels, project(): pl.pallas_call(project_kernel, out_shape=(jax.ShapeDtypeStruct((tokens, t...  9.79 us
    all_to_all x1, starting transfers between devices, per_device(): lax.all_to_all(blocks, 'sp', split_axis=0, concat_axis=0, tiled=True)  8.42 us
  transfers between devices with their start and end apart: 10, of which 4 were waited for; matrix products, arithmetic and copies ran while one was open for 1% of the time, Pallas kernels for 17%

commit v1 on v0

--- a/solution.py
+++ b/solution.py
@@ -49,29 +49,30 @@
     return jnp.where((row % 16) * 16 + row // 16 == column, 1.0, 0.0).astype(BF16)
 
 
-def pack_kernel(q_ref, k_ref, v_ref, logit_ref, decay_ref, out_ref):
+def pack_kernel(q_ref, k_ref, v_ref, logit_ref, decay_ref, key_out_ref, out_ref):
     heads = out_ref.shape[0]
-    row, column = iotas(heads, heads)
-    eye = jnp.where(row == column, 1.0, 0.0).astype(BF16)
-    logits = dot_nt(eye, logit_ref[0])
-    decays = dot_nt(eye, decay_ref[0])
+    logits = logit_ref[0].astype(F32)
+    decays = decay_ref[0].astype(F32)
     extra_row, _unused = iotas(EXTRA, C)
     for h in range(heads):
         columns = slice(h * C, (h + 1) * C)
-        out_ref[h, 0:C] = k_ref[0, :, columns]
-        out_ref[h, C : 2 * C] = q_ref[0, :, columns]
-        out_ref[h, 2 * C : 3 * C] = v_ref[0, :, columns]
+        key_out_ref[h, 0:C] = k_ref[0, :, columns]
         extra = jnp.where(extra_row == 0, logits[h : h + 1], decays[h : h + 1])
-        out_ref[h, 3 * C : 3 * C + EXTRA] = extra.astype(BF16)
+        key_out_ref[h, C : C + EXTRA] = extra.astype(BF16)
+        out_ref[h, 0:C] = q_ref[0, :, columns]
+        out_ref[h, C : 2 * C] = v_ref[0, :, columns]
 
 
 def pack(query, key, value, logit, decay_input):
-    heads = logit.shape[2]
+    heads = logit.shape[1]
     return pl.pallas_call(
         pack_kernel,
-        out_shape=jax.ShapeDtypeStruct((heads, 3 * C + EXTRA, C), BF16),
+        out_shape=(
+            jax.ShapeDtypeStruct((heads, C + EXTRA, C), BF16),
+            jax.ShapeDtypeStruct((heads, 2 * C, C), BF16),
+        ),
         in_specs=[VMEM] * 5,
-        out_specs=VMEM,
+        out_specs=(VMEM, VMEM),
         name="pack",
     )(query, key, value, logit, decay_input)
 
@@ -79,9 +80,23 @@
 GROUP = 4
 
 
-def delta_kernel(
-    x_ref, added_ref, rate_ref, out_ref,
-    a_ref, b_ref, qe_ref, su_ref, cum_col_ref, cum_row_ref, write_col_ref, write_row_ref,
+def column_of(ref, n):
+    lane = lax.broadcasted_iota(jnp.int32, ref.shape, 1)
+    return jnp.sum(jnp.where(lane == n, ref[...], 0.0), axis=1, keepdims=True)
+
+
+def beside(a, b):
+    return jnp.concatenate([a, b], axis=1)
+
+
+def above(a, b):
+    return jnp.concatenate([a, b], axis=0)
+
+
+def inverse_kernel(
+    x_ref, added_ref, rate_ref,
+    base_ref, weight_ref, a_ref, cum_col_ref, cum_row_ref, key_col_ref, key_row_ref,
+    write_col_ref, write_row_ref,
 ):
     chunks = x_ref.shape[0]
     row, column = iotas(C, C)
@@ -93,134 +108,178 @@
     logits = jnp.zeros((chunks, C), F32)
     decays = jnp.zeros((chunks, C), F32)
     for n in range(chunks):
-        extra = x_ref[n, 3 * C : 3 * C + EXTRA].astype(F32)
+        extra = x_ref[n, C : C + EXTRA].astype(F32)
         logits = jnp.where(chunk_row == n, extra[0:1], logits)
         decays = jnp.where(chunk_row == n, extra[1:2], decays)
     softplus = jnp.maximum(decays, 0.0) + jnp.log(1.0 + jnp.exp(-jnp.abs(decays)))
     log_decay = added_ref[...] - rate_ref[0] * softplus
     upper = jnp.where(row <= column, 1.0, 0.0)
-    lower = jnp.where(row >= column, 1.0, 0.0)
+    lower = jnp.where(inclusive, 1.0, 0.0)
     eye = jnp.where(diagonal, 1.0, 0.0)
     cum_row_ref[...] = jnp.dot(log_decay, upper, precision=HIGHEST, preferred_element_type=F32)
     cum_col_ref[...] = dot_nt(lower, log_decay, precision=HIGHEST)
     write = 1.0 / (1.0 + jnp.exp(-logits))
     write_row_ref[...] = write
     write_col_ref[...] = dot_nt(eye, write, precision=HIGHEST)
-
-    def column_of(ref, n):
-        lane = lax.broadcasted_iota(jnp.int32, (C, ref.shape[1]), 1)
-        return jnp.sum(jnp.where(lane == n, ref[...], 0.0), axis=1, keepdims=True)
-
-    def prepare(n):
-        keys = x_ref[n, 0:C]
-        queries = x_ref[n, C : 2 * C]
-        values = x_ref[n, 2 * C : 3 * C]
-        cum_c = column_of(cum_col_ref, n)
-        write_c = column_of(write_col_ref, n)
-        cum_r = cum_row_ref[pl.ds(n, 1), :]
-        write_r = write_row_ref[pl.ds(n, 1), :]
-        products = dot_nt(jnp.concatenate([keys, queries], axis=0), keys)
-        keys_dot, scores = products[:C], products[C:]
-        squares = jnp.where(diagonal, keys_dot, 0.0)
-        key_c = lax.rsqrt(jnp.sum(squares, axis=1, keepdims=True) + 1e-06)
-        key_r = lax.rsqrt(jnp.sum(squares, axis=0, keepdims=True) + 1e-06)
-        q32 = queries.astype(F32)
-        query_c = lax.rsqrt(jnp.sum(q32 * q32, axis=1, keepdims=True) + 1e-06) * C ** (-0.5)
-        within = jnp.exp(jnp.where(inclusive, cum_c - cum_r, -jnp.inf)) * key_r
-        lower_part = jnp.where(strict, keys_dot * within * (write_c * key_c), 0.0)
-        scores = scores * within * query_c
-
-        high, low = halves(lower_part)
-        left = jnp.concatenate([high, low], axis=1)
+    lane = lax.broadcasted_iota(jnp.int32, (C, chunks), 1)
+
+    def group(g, key_columns):
+        ns = [g * GROUP + k for k in range(GROUP)]
+        keys = [x_ref[n, 0:C] for n in ns]
+        products = [dot_nt(k, k) for k in keys]
+        cum_c = [column_of(cum_col_ref, n) for n in ns]
+        write_c = [column_of(write_col_ref, n) for n in ns]
+        cum_r = [cum_row_ref[pl.ds(n, 1), :] for n in ns]
+        write_r = [write_row_ref[pl.ds(n, 1), :] for n in ns]
+        squares = [jnp.where(diagonal, p, 0.0) for p in products]
+        key_c = [lax.rsqrt(jnp.sum(s, axis=1, keepdims=True) + 1e-06) for s in squares]
+        key_r = [lax.rsqrt(jnp.sum(s, axis=0, keepdims=True) + 1e-06) for s in squares]
+        for n, c, r in zip(ns, key_c, key_r):
+            key_columns = jnp.where(lane == n, c, key_columns)
+            key_row_ref[pl.ds(n, 1), :] = r
+        lower_part = [
+            jnp.where(
+                strict,
+                p * jnp.exp(jnp.where(inclusive, cc - cr, -jnp.inf)) * (wc * kc) * kr,
+                0.0,
+            )
+            for p, cc, cr, wc, kc, kr in zip(products, cum_c, cum_r, write_c, key_c, key_r)
+        ]
+
+        left = [beside(*halves(part)) for part in lower_part]
         pair = (row // 2 == column // 2) & strict
-        inverse = jnp.where(pair, -lower_part, eye)
+        inverse = [jnp.where(pair, -part, eye) for part in lower_part]
         size = 2
         while size < C:
-            high, low = halves(inverse)
-            first = dot(left, jnp.concatenate([high, high], axis=0))
-            first_high, first_low = halves(first)
-            second = dot(
-                jnp.concatenate([high, high], axis=1),
-                jnp.concatenate([first_high, first_low], axis=0),
-            )
+            highs = [i.astype(BF16) for i in inverse]
+            first = [dot(f, above(h, h)) for f, h in zip(left, highs)]
+            first = [above(*halves(f)) for f in first]
+            second = [dot(beside(h, h), f) for h, f in zip(highs, first)]
             joined = (row // (2 * size) == column // (2 * size)) & (row // size > column // size)
-            inverse = jnp.where(joined, -second, inverse)
+            inverse = [jnp.where(joined, -s, i) for s, i in zip(second, inverse)]
             size *= 2
 
-        decay_r = jnp.exp(cum_r)
-        base_high, base_low = halves(inverse * write_r)
-        base = dot(
-            jnp.concatenate([base_high, base_low], axis=1),
-            jnp.concatenate([values, values], axis=0),
-        )
-        weight_high, weight_low = halves(inverse * (write_r * decay_r * key_r))
-        weight = dot(
-            jnp.concatenate([weight_high, weight_low], axis=1),
-            jnp.concatenate([keys, keys], axis=0),
-        )
-        last = cum_c[C - 1 : C]
-        both = jnp.concatenate([base, weight], axis=1)
-        carried_high, carried_low = halves(both * (key_c * jnp.exp(last - cum_c)))
-        keys_t = keys.T
-        update = dot(
-            jnp.concatenate([keys_t, keys_t], axis=1),
-            jnp.concatenate([carried_high, carried_low], axis=0),
-        )
-        b_ref[n] = update[:, :C]
-        a_ref[n] = jnp.where(diagonal, jnp.exp(last), 0.0) - update[:, C:]
-        score_high, score_low = halves(scores)
-        both = both.astype(BF16)
-        seen = dot(
-            jnp.concatenate([score_high, score_low], axis=1),
-            jnp.concatenate([both, both], axis=0),
-        )
-        su_ref[n] = seen[:, :C]
-        qe_ref[n] = q32 * (query_c * jnp.exp(cum_c)) - seen[:, C:]
-
-    def group(g, carry):
+        for n, i, w in zip(ns, inverse, write_r):
+            base_ref[n] = beside(*halves(i * w))
+        weight = [
+            beside(*halves(i * (w * jnp.exp(c) * k)))
+            for i, w, c, k in zip(inverse, write_r, cum_r, key_r)
+        ]
+        weight = [dot(w, above(k, k)) for w, k in zip(weight, keys)]
+        for n, w in zip(ns, weight):
+            weight_ref[n] = w.astype(BF16)
+        last = [c[C - 1 : C] for c in cum_c]
+        carried = [
+            above(*halves(w * (k * jnp.exp(end - c))))
+            for w, k, end, c in zip(weight, key_c, last, cum_c)
+        ]
+        turned = [k.T for k in keys]
+        update = [dot(beside(t, t), c) for t, c in zip(turned, carried)]
+        for n, u, end in zip(ns, update, last):
+            a_ref[n] = beside(*halves(jnp.where(diagonal, jnp.exp(end), 0.0) - u))
+        return key_columns
+
+    key_col_ref[...] = lax.fori_loop(
+        0, chunks // GROUP, group, jnp.zeros((C, chunks), F32)
+    )
+
+
+def chunk_inverse(blocks, added, decay_rate):
+    chunks = blocks.shape[0]
+    wide = jax.ShapeDtypeStruct((chunks, C, 2 * C), BF16)
+    columns = jax.ShapeDtypeStruct((C, chunks), F32)
+    rows = jax.ShapeDtypeStruct((chunks, C), F32)
+    return pl.pallas_call(
+        inverse_kernel,
+        out_shape=(
+            wide, jax.ShapeDtypeStruct((chunks, C, C), BF16), wide, columns, rows, columns, rows,
+        ),
+        in_specs=[VMEM, VMEM, SMEM],
+        out_specs=(VMEM,) * 7,
+        scratch_shapes=[pltpu.VMEM((C, chunks), F32), pltpu.VMEM((chunks, C), F32)],
+        cost_estimate=pl.CostEstimate(flops=4 * 10**9, bytes_accessed=2**21, transcendentals=0),
+        name="inverse",
+    )(blocks, added, decay_rate)
+
+
+def delta_kernel(
+    key_ref, x_ref, base_ref, weight_ref, a_ref, cum_col_ref, cum_row_ref, key_col_ref,
+    key_row_ref, out_ref, b_ref, qe_ref, su_ref,
+):
+    chunks = x_ref.shape[0]
+    row, column = iotas(C, C)
+    inclusive = row >= column
+
+    def prepare(g):
+        ns = [g * GROUP + k for k in range(GROUP)]
+        keys = [key_ref[n, 0:C] for n in ns]
+        queries = [x_ref[n, 0:C] for n in ns]
+        values = [x_ref[n, C : 2 * C] for n in ns]
+        scores = [dot_nt(q, k) for q, k in zip(queries, keys)]
+        base = [dot(base_ref[n], above(v, v)) for n, v in zip(ns, values)]
+        cum_c = [column_of(cum_col_ref, n) for n in ns]
+        key_c = [column_of(key_col_ref, n) for n in ns]
+        cum_r = [cum_row_ref[pl.ds(n, 1), :] for n in ns]
+        key_r = [key_row_ref[pl.ds(n, 1), :] for n in ns]
+        q32 = [q.astype(F32) for q in queries]
+        query_c = [
+            lax.rsqrt(jnp.sum(q * q, axis=1, keepdims=True) + 1e-06) * C ** (-0.5) for q in q32
+        ]
+        scores = [
+            s * jnp.exp(jnp.where(inclusive, cc - cr, -jnp.inf)) * kr * qc
+            for s, cc, cr, kr, qc in zip(scores, cum_c, cum_r, key_r, query_c)
+        ]
+        carried = [
+            above(*halves(b * (k * jnp.exp(c[C - 1 : C] - c))))
+            for b, k, c in zip(base, key_c, cum_c)
+        ]
+        turned = [k.T for k in keys]
+        update = [dot(beside(t, t), c) for t, c in zip(turned, carried)]
+        both = [beside(b.astype(BF16), weight_ref[n]) for n, b in zip(ns, base)]
+        seen = [dot(beside(*halves(s)), above(b, b)) for s, b in zip(scores, both)]
+        for n, u, s, q, qc, c in zip(ns, update, seen, q32, query_c, cum_c):
+            b_ref[n] = u
+            su_ref[n] = s[:, :C]
+            qe_ref[n] = beside(*halves(q * (qc * jnp.exp(c)) - s[:, C:]))
+
+    def advance(g, state):
         for k in range(GROUP):
-            prepare(g * GROUP + k)
-        return carry
-
-    lax.fori_loop(0, chunks // GROUP, group, 0)
-
-    def advance(n, state):
-        high, low = halves(state)
-        both = jnp.concatenate([high, low], axis=0)
-        q_high, q_low = halves(qe_ref[n])
-        out = dot(jnp.concatenate([q_high, q_high], axis=1), both) + su_ref[n]
-        scale = lax.rsqrt(jnp.mean(out * out, axis=1, keepdims=True) + 1e-05)
-        out_ref[n] = (out * scale).astype(BF16)
-        a_high, a_low = halves(a_ref[n])
-        return (
-            dot(jnp.concatenate([a_high, a_high], axis=1), both) + dot(a_low, high) + b_ref[n]
-        )
-
-    def steps(g, state):
-        for k in range(2):
-            state = advance(g * 2 + k, state)
+            n = g * GROUP + k
+            high, low = halves(state)
+            queries = qe_ref[n]
+            out = dot(queries, above(high, high)) + su_ref[n]
+            scale = lax.rsqrt(jnp.mean(out * out, axis=1, keepdims=True) + 1e-05)
+            out_ref[n] = (out * scale).astype(BF16)
+            a_high, a_low = a_ref[n, :, :C], a_ref[n, :, C:]
+            state = dot(beside(a_high, a_high), above(high, low)) + dot(a_low, high) + b_ref[n]
         return state
 
-    lax.fori_loop(0, chunks // 2, steps, jnp.zeros((C, C), F32))
-
-
-def delta(blocks, added, decay_rate):
+    prepare(0)
+
+    def step(g, state):
+        state = advance(g - 1, state)
+        prepare(g)
+        return state
+
+    state = lax.fori_loop(1, chunks // GROUP, step, jnp.zeros((C, C), F32))
+    advance(chunks // GROUP - 1, state)
+
+
+def delta(keys, blocks, parts):
     chunks = blocks.shape[0]
     return pl.pallas_call(
         delta_kernel,
         out_shape=jax.ShapeDtypeStruct((chunks, C, C), BF16),
-        in_specs=[VMEM, VMEM, SMEM],
+        in_specs=[VMEM] * 9,
         out_specs=VMEM,
-        scratch_shapes=[pltpu.VMEM((chunks, C, C), F32)] * 4
-        + [
-            pltpu.VMEM((C, chunks), F32),
-            pltpu.VMEM((chunks, C), F32),
-            pltpu.VMEM((C, chunks), F32),
-            pltpu.VMEM((chunks, C), F32),
+        scratch_shapes=[
+            pltpu.VMEM((chunks, C, C), F32),
+            pltpu.VMEM((chunks, C, 2 * C), BF16),
+            pltpu.VMEM((chunks, C, C), F32),
         ],
         cost_estimate=pl.CostEstimate(flops=4 * 10**9, bytes_accessed=2**21, transcendentals=0),
         name="delta",
-    )(blocks, added, decay_rate)
+    )(keys, blocks, *parts)
 
 
 def slots_kernel(index_ref, dest_ref, source_ref, count_ref):
@@ -235,17 +294,20 @@
 
     lax.fori_loop(0, experts, clear, 0)
 
+    tokens = index_ref.shape[0] // 4
+
     def place(t, carry):
         for k in range(4):
-            e = index_ref[t * 4 + k]
+            at = k * tokens + t
+            e = index_ref[at]
             used = count_ref[e]
             count_ref[e] = used + 1
             slot = e * capacity + used
-            dest_ref[t * 4 + k] = slot
+            dest_ref[at] = slot
             source_ref[slot] = t
         return carry
 
-    lax.fori_loop(0, index_ref.shape[0] // 4, place, 0)
+    lax.fori_loop(0, tokens, place, 0)
 
 
 def slots(index, experts, capacity):
@@ -343,11 +405,20 @@
         swap = swap_matrix()
 
         def turn(i, carry):
-            for k in range(4):
-                start = pl.multiple_of((i * 4 + k) * 16, 16)
-                turned = dot(swap, x_ref[pl.ds(start, 16)].reshape(16 * tiles, C)).astype(BF16)
+            for k in range(2):
+                start = pl.multiple_of((i * 4 + k * 2) * 16, 16)
+                other = pl.multiple_of(start + 16, 16)
+                turned = dot(
+                    swap,
+                    beside(
+                        x_ref[pl.ds(start, 16)].reshape(16 * tiles, C),
+                        x_ref[pl.ds(other, 16)].reshape(16 * tiles, C),
+                    ),
+                ).astype(BF16)
                 for j in range(tiles):
-                    rows_ref[pl.ds(start, 16), j * C : (j + 1) * C] = turned[j * 16 : (j + 1) * 16]
+                    part = turned[j * 16 : (j + 1) * 16]
+                    rows_ref[pl.ds(start, 16), j * C : (j + 1) * C] = part[:, :C]
+                    rows_ref[pl.ds(other, 16), j * C : (j + 1) * C] = part[:, C:]
             return carry
 
         lax.fori_loop(0, groups // 4, turn, 0)
@@ -372,18 +443,23 @@
         swap = swap_matrix()
         down_steps, _rows, width = made_ref.shape
 
+        def stacked(start):
+            pieces = []
+            for d in range(down_steps):
+                piece = made_ref[d, pl.ds(start, 16), :]
+                pieces += [piece[:, j * C : (j + 1) * C] for j in range(width // C)]
+            return jnp.concatenate(pieces, axis=0)
+
         def turn(i, carry):
             for k in range(2):
-                start = pl.multiple_of((i * 2 + k) * 16, 16)
-                pieces = []
-                for d in range(down_steps):
-                    piece = made_ref[d, pl.ds(start, 16), :]
-                    pieces += [piece[:, j * C : (j + 1) * C] for j in range(width // C)]
-                turned = dot(swap, jnp.concatenate(pieces, axis=0)).astype(BF16)
-                out_ref[pl.ds(start, 16)] = turned.reshape(16, tiles, C)
+                start = pl.multiple_of((i * 4 + k * 2) * 16, 16)
+                other = pl.multiple_of(start + 16, 16)
+                turned = dot(swap, beside(stacked(start), stacked(other))).astype(BF16)
+                out_ref[pl.ds(start, 16)] = turned[:, :C].reshape(16, tiles, C)
+                out_ref[pl.ds(other, 16)] = turned[:, C:].reshape(16, tiles, C)
             return carry
 
-        lax.fori_loop(0, groups // 2, turn, 0)
+        lax.fori_loop(0, groups // 4, turn, 0)
 
 
 def expert(rows, gate_weight, up_weight, down_weight):
@@ -416,34 +492,37 @@
 
 def combine_kernel(back_ref, normed_ref, gain_ref, dest_ref, weight_ref, out_ref, z_ref):
     tokens, tiles, _lanes = normed_ref.shape
-    features = tiles * C
+    swap = swap_matrix()
     gain = gain_ref[...]
 
-    def token(t):
-        total = normed_ref[t].astype(F32)
-        for k in range(4):
-            slot = dest_ref[t * 4 + k]
-            total = total + weight_ref[t * 4 + k] * back_ref[slot].astype(F32)
-        centred = total - jnp.sum(total, keepdims=True) * (1.0 / features)
-        variance = jnp.sum(centred * centred, keepdims=True) * (1.0 / features)
-        z_ref[t] = centred * lax.rsqrt(variance + 1e-05) * gain
-
     def some(i, carry):
-        for k in range(8):
-            token(i * 8 + k)
+        for k in range(16):
+            t = i * 16 + k
+            total = normed_ref[t].astype(F32)
+            for pick in range(4):
+                at = pick * tokens + t
+                total = total + weight_ref[at] * back_ref[dest_ref[at]].astype(F32)
+            z_ref[t] = total
         return carry
 
-    lax.fori_loop(0, tokens // 8, some, 0)
-    swap = swap_matrix()
-    for g in range(tokens // 16):
-        z = z_ref[g * 16 : (g + 1) * 16].reshape(16 * tiles, C)
+    lax.fori_loop(0, tokens // 16, some, 0)
+
+    def finish(i, carry):
+        start = pl.multiple_of(i * 16, 16)
+        z = z_ref[pl.ds(start, 16)].reshape(16 * tiles, C)
         high = z.astype(BF16)
         rest = z - high.astype(F32)
         middle = rest.astype(BF16)
         low = (rest - middle.astype(F32)).astype(BF16)
-        turned = dot(swap, high) + dot(swap, middle) + dot(swap, low)
-        for j in range(tiles):
-            out_ref[0, g * 16 : (g + 1) * 16, j * C : (j + 1) * C] = turned[j * 16 : (j + 1) * 16]
+        turned = dot(swap, beside(high, middle))
+        turned = turned[:, :C] + turned[:, C:] + dot(swap, low)
+        total = jnp.concatenate([turned[j * 16 : (j + 1) * 16] for j in range(tiles)], axis=1)
+        centred = total - jnp.mean(total, axis=1, keepdims=True)
+        variance = jnp.mean(centred * centred, axis=1, keepdims=True)
+        out_ref[0, pl.ds(start, 16), :] = centred * lax.rsqrt(variance + 1e-05) * gain
+        return carry
+
+    lax.fori_loop(0, tokens // 16, finish, 0, unroll=2)
 
 
 def combine(back, normed, gain, dest, weight):
@@ -466,9 +545,8 @@
         pairs = [(i, (i + shift) % y_size) for i in range(y_size)]
         found.append(lax.ppermute(block, "dp_0", pairs))
     places = [((y - shift) % y_size) * core_size + core for shift in range(y_size)]
-    swapped = [lax.ppermute(b, "dp_1", [(0, 1), (1, 0)]) for b in found]
     others = [((y - shift) % y_size) * core_size + 1 - core for shift in range(y_size)]
-    return found + swapped, jnp.stack(places + others).astype(jnp.int32)
+    return found, jnp.stack(places + others).astype(jnp.int32)
 
 
 def per_device(
@@ -496,12 +574,22 @@
     picks = token_expert_index.shape[2]
     capacity = tokens * picks * 3 // (2 * experts)
     tiles = features // C
-    weights, places = gathered(output_projection)
-    dest, source = slots(token_expert_index.reshape(-1), experts, capacity)
-    blocks = pack(query, key, value, write_strength_logit, decay_head_input)
+    found, places = gathered(output_projection)
+    dest, source = slots(token_expert_index[0].T.reshape(-1), experts, capacity)
+    keys, blocks = pack(
+        query,
+        key,
+        value,
+        write_strength_logit.transpose(0, 2, 1),
+        decay_head_input.transpose(0, 2, 1),
+    )
+    keys = lax.all_to_all(keys, "sp", split_axis=0, concat_axis=0, tiled=True)
     blocks = lax.all_to_all(blocks, "sp", split_axis=0, concat_axis=0, tiled=True)
-    recurrent = delta(blocks, added_log_decay.reshape(-1, C), head_decay_rate)
+    parts = chunk_inverse(keys, added_log_decay.reshape(-1, C), head_decay_rate)
+    recurrent = delta(keys, blocks, parts)
+    recurrent, found = lax.optimization_barrier((recurrent, found))
     returned = lax.all_to_all(recurrent, "sp", split_axis=0, concat_axis=0, tiled=True)
+    weights = found + [lax.ppermute(b, "dp_1", [(0, 1), (1, 0)]) for b in found]
     normed, rows = project(
         returned,
         output_gate_input,
@@ -525,9 +613,9 @@
     return combine(
         back.reshape(experts * capacity, tiles, C),
         normed,
-        feedforward_norm_gain.reshape(tiles, C),
+        feedforward_norm_gain.reshape(1, features),
         dest,
-        token_expert_weight.reshape(-1),
+        token_expert_weight[0].T.reshape(-1),
     )
 
 

time: 282 us -> 230 us (0.82)
  blocking collectives: 48.2 us -> 115 us
  waiting for transfers between devices: 83.9 us -> 24.2 us
  Pallas kernels: 109 us -> 69.2 us
  starting transfers between devices: 30.3 us -> 17.3 us
  local copies, waits for them, and re-layouts: 8.66 us -> 2.71 us
    all_to_all x0 -> x2, blocking collectives: none -> 67.1 us  [the longest x1 47.2 us: per_device(): back = lax.all_to_all(made, SP_DP, split_axis=0, concat_axis=0, tiled=True)]
    all_to_all x1 -> x0, waiting for transfers between devices: 41 us -> none  [per_device(): back = lax.all_to_all(made, SP_DP, split_axis=0, concat_axis=0, tiled=True)]
    pallas_call x1, Pallas kernels: 43 us -> 7.91 us  [delta(): pl.pallas_call(delta_kernel, out_shape=jax.ShapeDtypeStruct((chunks, C, C...]
    ppermute x3, waiting for transfers between devices: 40 us -> 20.4 us  [gathered(): found.append(lax.ppermute(block, 'dp_0', pairs))]
    pallas_call x1, Pallas kernels: 21.5 us -> 5.82 us  [combine(): pl.pallas_call(combine_kernel, out_shape=jax.ShapeDtypeStruct((1, tokens,...]
    pallas_call x1 -> x2, Pallas kernels: 2.93 us -> 16.5 us  [the longest x1 13.6 us: chunk_inverse(): pl.pallas_call(inverse_kernel, out_shape=(wide, jax.ShapeDtypeStruct((chu...]
    all_to_all x1, starting transfers between devices: 8.42 us -> 3.66 us  [per_device(): lax.all_to_all(blocks, 'sp', split_axis=0, concat_axis=0, tiled=True)]
    all_to_all x1 -> x0, starting transfers between devices: 4.62 us -> none  [per_device(): back = lax.all_to_all(made, SP_DP, split_axis=0, concat_axis=0, tiled=True)]
  transfers between devices with their start and end apart: 10 -> 9, of which waited for: 4 -> 2; matrix products, arithmetic and copies ran while one was open for 1% -> 0% of each run, Pallas kernels for 17% -> 12%
where the time goes in v1:
time: 230 us
  blocking collectives  115 us (50%)
  Pallas kernels  69.2 us (30%)
  waiting for transfers between devices  24.2 us (11%)
  starting transfers between devices  17.3 us (8%)
  local copies, waits for them, and re-layouts  2.71 us (1%)
    all_to_all x1, blocking collectives, per_device(): rows = lax.all_to_all(rows, SP_DP, split_axis=0, concat_axis=0, tiled=True)  48.4 us
    all_to_all x1, blocking collectives, per_device(): back = lax.all_to_all(made, SP_DP, split_axis=0, concat_axis=0, tiled=True)  47.2 us
    pallas_call x1, Pallas kernels, expert(): pl.pallas_call(expert_kernel, grid=(ff_steps + down_steps,), out_shape=ja...  23.1 us
    ppermute x3, waiting for transfers between devices, gathered(): found.append(lax.ppermute(block, 'dp_0', pairs))  20.4 us
    all_to_all x1, blocking collectives, per_device(): keys = lax.all_to_all(keys, 'sp', split_axis=0, concat_axis=0, tiled=True)  19.8 us
    pallas_call x1, Pallas kernels, chunk_inverse(): pl.pallas_call(inverse_kernel, out_shape=(wide, jax.ShapeDtypeStruct((chu...  13.6 us
    pallas_call x1, Pallas kernels, project(): pl.pallas_call(project_kernel, out_shape=(jax.ShapeDtypeStruct((tokens, t...  9.78 us
    pallas_call x1, Pallas kernels, delta(): pl.pallas_call(delta_kernel, out_shape=jax.ShapeDtypeStruct((chunks, C, C...  7.91 us
  transfers between devices with their start and end apart: 9, of which 2 were waited for; matrix products, arithmetic and copies ran while one was open for 0% of the time, Pallas kernels for 12%

profile of v1, /device:TPU:1, one launch (start us, length us, event | category | flops | bytes accessed | tf_op | source)
XLA Modules:
  0.0 229.7 jit_solution(1104967903773659352)
XLA Ops:
  0.0 0.0 copy-start.2
  0.0 2.9 %pack.1 = (bf16[16,144,128]{2,1,0:T(8,128)(2,1)}, bf16[16,256,128]{2,1,0:T(8,128)(2,1)}) custom-call(bf16[1,128,2048]{2,1,0:T(8,128)(2,1)} %q_ref.1, bf16[1,128,2048]{2,1,0:T(8,128)(2,1)} %k_ref.1, bf16[1,128,2048]{2,1,0:T(8,128)(2,1)} %v_ref.1, bf16[1,16,128]{2,1,0:T(8,128)(2,1)} %bitcast.37, bf16[1,16,128]{2,1,0:T(8,128)(2,1)} %bitcast.38), custom_call_target="tpu_custom_call" | custom-call | tf_op jit(solution)/shard_map/pack/pallas_call | solution.py:68
  2.9 19.8 %all_to_all.25.x_ref.key_ref = bf16[16,144,128]{2,1,0:T(8,128)(2,1)} all-to-all(bf16[16,144,128]{2,1,0:T(8,128)(2,1)} %get-tuple-element.23), channel_id=1, replica_groups=mesh['sp'=16,'dp_0'=4,'dp_1'=2] {'sp'}, dimensions={0} | all-to-all | bytes 1179648 | tf_op jit(solution)/shard_map/all_to_all | solution.py:586
  22.7 3.7 %all-to-all-start.1 = ((bf16[16,256,128]{2,1,0:T(8,128)(2,1)}), bf16[16,256,128]{2,1,0:T(8,128)(2,1)S(1)}, u32[]{:S(2)}, u32[]{:S(2)}) async-start(bf16[16,256,128]{2,1,0:T(8,128)(2,1)} %get-tuple-element.24), calls=%async_computation.1 | async-start | bytes 2097152 | tf_op jit(solution)/shard_map/all_to_all | solution.py:587
  26.4 0.0 copy-done.2
  26.4 3.0 %collective-permute-start.1 = (bf16[2048,256]{1,0:T(8,128)(2,1)S(1)}, bf16[2048,256]{1,0:T(8,128)(2,1)}, u32[]{:S(2)}, u32[]{:S(2)}) collective-permute-start(bf16[2048,256]{1,0:T(8,128)(2,1)S(1)} %copy-done.2), channel_id=1, source_target_pairs={{0,4},{2,6},{4,0},{6,2},{1,5},{3,7},{5,1},{7,3},{8,12},{10,14},{12... | collective-permute-start | bytes 3145736 | tf_op jit(solution)/shard_map/ppermute | solution.py:546
  29.4 0.4 collective-permute-start
  29.8 2.3 collective-permute-start.2
  32.7 13.6 %inverse.1 = (bf16[16,128,256]{2,1,0:T(8,128)(2,1)}, bf16[16,128,128]{2,1,0:T(8,128)(2,1)}, bf16[16,128,256]{2,1,0:T(8,128)(2,1)}, f32[128,16]{1,0:T(8,128)}, f3...) custom-call(bf16[16,144,128]{2,1,0:T(8,128)(2,1)} %all_to_all.25.x_ref.key_ref, f32[16,128]{1,0:T(8,128)} %bitcast.45, ...), custom_call_target="tpu_custom_call" | custom-call | flops 4000000000 | bytes 2097152 | tf_op jit(solution)/shard_map/inverse/pallas_call | solution.py:192
  46.3 0.0 all-to-all-done.1.x_ref
  46.3 0.0 copy-start.1
  46.3 1.0 copy-done.1
  47.3 7.9 %delta.1 = bf16[16,128,128]{2,1,0:T(8,128)(2,1)} custom-call(bf16[16,144,128]{2,1,0:T(8,128)(2,1)} %all_to_all.25.x_ref.key_ref, bf16[16,256,128]{2,1,0:T(8,128)(2,1)} %copy-done.1, bf16[16,128,256]{2,1,0:T(8,128)(2,1)} %get-tuple-element.25.base_ref, bf16[16,128,128]{2,1,0:T(8,128)(2,1)} %get-tuple-element.26.weight_ref, ...), custom_call_target="tpu_custom_call" | custom-call | flops 4000000000 | bytes 2097152 | tf_op jit(solution)/shard_map/delta/pallas_call | solution.py:270
  55.2 0.0 collective-permute-done.1.rest_2_
  55.2 20.4 %collective-permute-done.rest_1_ = bf16[2048,256]{1,0:T(8,128)(2,1)} collective-permute-done((bf16[2048,256]{1,0:T(8,128)(2,1)S(1)}, bf16[2048,256]{1,0:T(8,128)(2,1)}, u32[]{:S(2)}, u32[]{:S(2)}) %collective-permute-start) | collective-permute-done | bytes 1048608 | tf_op jit(solution)/shard_map/ppermute | solution.py:546
  75.7 0.0 collective-permute-done.2.rest_3_
  75.7 0.9 collective-permute-start.3
  76.5 0.0 collective-permute-start.4
  76.5 0.5 collective-permute-start.5
  77.0 0.0 collective-permute-start.6
  77.1 6.6 %all-to-all-start.2 = ((bf16[16,128,128]{2,1,0:T(8,128)(2,1)}), bf16[16,128,128]{2,1,0:T(8,128)(2,1)S(1)}, u32[]{:S(2)}, u32[]{:S(2)}) async-start(bf16[16,128,128]{2,1,0:T(8,128)(2,1)} %delta.1), calls=%async_computation.2 | async-start | bytes 1048576 | tf_op jit(solution)/shard_map/all_to_all | solution.py:591
  83.7 6.1 %slots.1 = (s32[512]{0:T(512)}, s32[768]{0:T(1024)}) custom-call(s32[512]{0:T(512)} %bitcast.40), custom_call_target="tpu_custom_call" | custom-call | tf_op jit(solution)/shard_map/slots/pallas_call | solution.py:314
  89.8 0.6 stack.35.place_ref
  90.5 3.8 %all-to-all-done.2.rec_ref = bf16[16,128,128]{2,1,0:T(8,128)(2,1)S(1)} async-done(((bf16[16,128,128]{2,1,0:T(8,128)(2,1)}), bf16[16,128,128]{2,1,0:T(8,128)(2,1)S(1)}, u32[]{:S(2)}, u32[]{:S(2)}) %all-to-all-start.2) | async-done | bytes 524320 | tf_op jit(solution)/shard_map/all_to_all | solution.py:591
  94.2 0.0 copy-start
  94.2 0.0 collective-permute-done.3.rest_4_
  94.3 0.0 copy-start.3
  94.3 0.0 collective-permute-done.4.rest_5_
  94.3 0.0 collective-permute-done.5.rest_6_
  94.3 0.0 collective-permute-done.6.rest_7_
  94.3 0.8 copy-done
  95.1 0.3 copy-done.3
  95.4 9.8 %project.1 = (bf16[128,16,128]{2,1,0:T(8,128)(2,1)}, bf16[768,16,128]{2,1,0:T(8,128)(2,1)}) custom-call(bf16[16,128,128]{2,1,0:T(8,128)(2,1)} %copy-done, bf16[1,128,2048]{2,1,0:T(8,128)(2,1)} %gate_ref.1, f32[1,128]{1,0:T(1,128)} %bitcast.41, bf16[1,128,2048]{2,1,0:T(8,128)(2,1)} %residual_ref.1, f32[1,2048]{1,0:T(1,128)} %bitcast.36, ...), custom_call_target="tpu_custom_call" | custom-call | flops 1000000000 | bytes 16777216 | tf_op jit(solution)/shard_map/project/pallas_call | solution.py:374
  105.2 48.4 %all_to_all.26 = bf16[128,96,128]{2,1,0:T(8,128)(2,1)} all-to-all(bf16[128,96,128]{2,1,0:T(8,128)(2,1)} %bitcast.32), channel_id=1, replica_groups=mesh['sp'=16,'dp_0'=4,'dp_1'=2] {'sp','dp_0','dp_1'}, dimensions={0} | all-to-all | bytes 6291456 | tf_op jit(solution)/shard_map/all_to_all | solution.py:604
  153.6 23.1 %expert.1 = bf16[768,16,128]{2,1,0:T(8,128)(2,1)} custom-call(bf16[768,16,128]{2,1,0:T(8,128)(2,1)} %bitcast.33, bf16[2048,1024]{1,0:T(8,128)(2,1)} %bitcast.42, bf16[2048,1024]{1,0:T(8,128)(2,1)} %bitcast.43, bf16[1024,2048]{1,0:T(8,128)(2,1)} %bitcast.44), custom_call_target="tpu_custom_call" | custom-call | flops 10000000000 | bytes 16777216 | tf_op jit(solution)/shard_map/expert/pallas_call | solution.py:471
  176.7 47.2 %all_to_all.27 = bf16[128,96,128]{2,1,0:T(8,128)(2,1)} all-to-all(bf16[128,96,128]{2,1,0:T(8,128)(2,1)} %bitcast.34), channel_id=1, replica_groups=mesh['sp'=16,'dp_0'=4,'dp_1'=2] {'sp','dp_0','dp_1'}, dimensions={0} | all-to-all | bytes 6291456 | tf_op jit(solution)/shard_map/all_to_all | solution.py:612
  223.9 5.8 %combine.1 = f32[1,128,2048]{2,1,0:T(8,128)} custom-call(bf16[768,16,128]{2,1,0:T(8,128)(2,1)} %bitcast.31, bf16[128,16,128]{2,1,0:T(8,128)(2,1)} %get-tuple-element.39.normed_ref, f32[1,2048]{1,0:T(1,128)} %bitcast.35, s32[512]{0:T(512)} %get-tuple-element.40.dest_ref, f32[512]{0:T(512)} %bitcast.39), custom_call_target="tpu_custom_call" | custom-call | tf_op jit(solution)/shard_map/combine/pallas_call | solution.py:530
Async XLA Ops:
  0.0 26.4 %copy-start.2 = (bf16[2048,256]{1,0:T(8,128)(2,1)S(1)}, bf16[2048,256]{1,0:T(8,128)(2,1)}, u32[]{:S(2)}) copy-start(bf16[2048,256]{1,0:T(8,128)(2,1)} %rest_0_) | copy-start | bytes 3145732
  22.7 23.6 %all-to-all-start.1 = ((bf16[16,256,128]{2,1,0:T(8,128)(2,1)}), bf16[16,256,128]{2,1,0:T(8,128)(2,1)S(1)}, u32[]{:S(2)}, u32[]{:S(2)}) async-start(bf16[16,256,128]{2,1,0:T(8,128)(2,1)} %get-tuple-element.24), calls=%async_computation.1 | async-start | bytes 2097152 | tf_op jit(solution)/shard_map/all_to_all | solution.py:587
  26.4 28.8 %collective-permute-start.1 = (bf16[2048,256]{1,0:T(8,128)(2,1)S(1)}, bf16[2048,256]{1,0:T(8,128)(2,1)}, u32[]{:S(2)}, u32[]{:S(2)}) collective-permute-start(bf16[2048,256]{1,0:T(8,128)(2,1)S(1)} %copy-done.2), channel_id=1, source_target_pairs={{0,4},{2,6},{4,0},{6,2},{1,5},{3,7},{5,1},{7,3},{8,12},{10,14},{12... | collective-permute-start | bytes 3145736 | tf_op jit(solution)/shard_map/ppermute | solution.py:546
  29.4 46.2 %collective-permute-start = (bf16[2048,256]{1,0:T(8,128)(2,1)S(1)}, bf16[2048,256]{1,0:T(8,128)(2,1)}, u32[]{:S(2)}, u32[]{:S(2)}) collective-permute-start(bf16[2048,256]{1,0:T(8,128)(2,1)S(1)} %copy-done.2), channel_id=1, source_target_pairs={{0,2},{2,4},{4,6},{6,0},{1,3},{3,5},{5,7},{7,1},{8,10},{10,12},{12... | collective-permute-start | bytes 3145736 | tf_op jit(solution)/shard_map/ppermute | solution.py:546
  29.8 45.9 %collective-permute-start.2 = (bf16[2048,256]{1,0:T(8,128)(2,1)S(1)}, bf16[2048,256]{1,0:T(8,128)(2,1)}, u32[]{:S(2)}, u32[]{:S(2)}) collective-permute-start(bf16[2048,256]{1,0:T(8,128)(2,1)S(1)} %copy-done.2), channel_id=1, source_target_pairs={{0,6},{2,0},{4,2},{6,4},{1,7},{3,1},{5,3},{7,5},{8,14},{10,8},{12,... | collective-permute-start | bytes 3145736 | tf_op jit(solution)/shard_map/ppermute | solution.py:546
  46.3 1.0 copy-start.1
  75.7 18.6 %collective-permute-start.3 = (bf16[2048,256]{1,0:T(8,128)(2,1)S(1)}, bf16[2048,256]{1,0:T(8,128)(2,1)S(1)}, u32[]{:S(2)}, u32[]{:S(2)}) collective-permute-start(bf16[2048,256]{1,0:T(8,128)(2,1)S(1)} %copy-done.2), channel_id=1, source_target_pairs={{0,1},{1,0},{2,3},{3,2},{4,5},{5,4},{6,7},{7,6},{8,9},{9,8},{10,11... | collective-permute-start | bytes 3145736 | tf_op jit(solution)/shard_map/ppermute | solution.py:592
  76.5 17.7 %collective-permute-start.4 = (bf16[2048,256]{1,0:T(8,128)(2,1)}, bf16[2048,256]{1,0:T(8,128)(2,1)}, u32[]{:S(2)}, u32[]{:S(2)}) collective-permute-start(bf16[2048,256]{1,0:T(8,128)(2,1)} %collective-permute-done.rest_1_), channel_id=1, source_target_pairs={{0,1},{1,0},{2,3},{3,2},{4,5},{5,4},{6,7},{7,6},{8,9},{9,8},{10,11... | collective-permute-start | bytes 3145736 | tf_op jit(solution)/shard_map/ppermute | solution.py:592
  76.5 17.7 %collective-permute-start.5 = (bf16[2048,256]{1,0:T(8,128)(2,1)}, bf16[2048,256]{1,0:T(8,128)(2,1)}, u32[]{:S(2)}, u32[]{:S(2)}) collective-permute-start(bf16[2048,256]{1,0:T(8,128)(2,1)} %collective-permute-done.1.rest_2_), channel_id=1, source_target_pairs={{0,1},{1,0},{2,3},{3,2},{4,5},{5,4},{6,7},{7,6},{8,9},{9,8},{10,11... | collective-permute-start | bytes 3145736 | tf_op jit(solution)/shard_map/ppermute | solution.py:592
  77.0 17.2 %collective-permute-start.6 = (bf16[2048,256]{1,0:T(8,128)(2,1)}, bf16[2048,256]{1,0:T(8,128)(2,1)}, u32[]{:S(2)}, u32[]{:S(2)}) collective-permute-start(bf16[2048,256]{1,0:T(8,128)(2,1)} %collective-permute-done.2.rest_3_), channel_id=1, source_target_pairs={{0,1},{1,0},{2,3},{3,2},{4,5},{5,4},{6,7},{7,6},{8,9},{9,8},{10,11... | collective-permute-start | bytes 3145736 | tf_op jit(solution)/shard_map/ppermute | solution.py:592
  77.1 17.2 %all-to-all-start.2 = ((bf16[16,128,128]{2,1,0:T(8,128)(2,1)}), bf16[16,128,128]{2,1,0:T(8,128)(2,1)S(1)}, u32[]{:S(2)}, u32[]{:S(2)}) async-start(bf16[16,128,128]{2,1,0:T(8,128)(2,1)} %delta.1), calls=%async_computation.2 | async-start | bytes 1048576 | tf_op jit(solution)/shard_map/all_to_all | solution.py:591
  94.2 0.8 copy-start
  94.3 1.1 copy-start.3

commit v2 on v1

--- a/solution.py
+++ b/solution.py
@@ -5,6 +5,7 @@
 from jax.experimental.pallas import tpu as pltpu
 from jax.sharding import Mesh
 from jax.sharding import PartitionSpec as P
+
 
 DP = ("dp_0", "dp_1")
 SP_DP = ("sp", "dp_0", "dp_1")
@@ -17,7 +18,15 @@
 EXTRA = 16
 VMEM = pl.BlockSpec(memory_space=pltpu.VMEM)
 SMEM = pl.BlockSpec(memory_space=pltpu.SMEM)
-HBM = pl.BlockSpec(memory_space=pl.ANY)
+HBM = pl.BlockSpec(memory_space=pltpu.HBM)
+
+
+def near(x):
+    return pltpu.with_memory_space_constraint(x, pltpu.VMEM)
+
+
+def far(x):
+    return pltpu.with_memory_space_constraint(x, pltpu.HBM)
 
 
 def dot(a, b):
@@ -30,10 +39,6 @@
     )
 
 
-def dot_tn(a, b):
-    return lax.dot_general(a, b, (((0,), (0,)), ((), ())), preferred_element_type=F32)
-
-
 def halves(x):
     high = x.astype(BF16)
     return high, (x - high.astype(F32)).astype(BF16)
@@ -49,18 +54,27 @@
     return jnp.where((row % 16) * 16 + row // 16 == column, 1.0, 0.0).astype(BF16)
 
 
-def pack_kernel(q_ref, k_ref, v_ref, logit_ref, decay_ref, key_out_ref, out_ref):
+def pack_kernel(q_ref, k_ref, v_ref, logit_ref, decay_ref, key_out_ref, out_ref, sems):
     heads = out_ref.shape[0]
+    copies = []
+    for h in range(heads):
+        columns = slice(h * C, (h + 1) * C)
+        for source, target in (
+            (k_ref, key_out_ref.at[h, 0:C]),
+            (q_ref, out_ref.at[h, 0:C]),
+            (v_ref, out_ref.at[h, C : 2 * C]),
+        ):
+            copy = pltpu.make_async_copy(source.at[0, :, columns], target, sems.at[len(copies)])
+            copy.start()
+            copies.append(copy)
     logits = logit_ref[0].astype(F32)
     decays = decay_ref[0].astype(F32)
-    extra_row, _unused = iotas(EXTRA, C)
+    extra_row, _ = iotas(EXTRA, C)
     for h in range(heads):
-        columns = slice(h * C, (h + 1) * C)
-        key_out_ref[h, 0:C] = k_ref[0, :, columns]
         extra = jnp.where(extra_row == 0, logits[h : h + 1], decays[h : h + 1])
         key_out_ref[h, C : C + EXTRA] = extra.astype(BF16)
-        out_ref[h, 0:C] = q_ref[0, :, columns]
-        out_ref[h, C : 2 * C] = v_ref[0, :, columns]
+    for copy in copies:
+        copy.wait()
 
 
 def pack(query, key, value, logit, decay_input):
@@ -71,10 +85,12 @@
             jax.ShapeDtypeStruct((heads, C + EXTRA, C), BF16),
             jax.ShapeDtypeStruct((heads, 2 * C, C), BF16),
         ),
-        in_specs=[VMEM] * 5,
+        in_specs=[HBM] * 3 + [VMEM] * 2,
         out_specs=(VMEM, VMEM),
+        scratch_shapes=[pltpu.SemaphoreType.DMA((3 * heads,))],
+        compiler_params=pltpu.CompilerParams(vmem_limit_bytes=12 * 2**20),
         name="pack",
-    )(query, key, value, logit, decay_input)
+    )(far(query), far(key), far(value), far(logit), far(decay_input))
 
 
 GROUP = 4
@@ -93,18 +109,27 @@
     return jnp.concatenate([a, b], axis=0)
 
 
+def group_copies(pairs, sems, g):
+    part = pl.ds(g * GROUP, GROUP)
+    return [
+        pltpu.make_async_copy(source.at[part], target.at[part], sems.at[k, g])
+        for k, (source, target) in enumerate(pairs)
+    ]
+
+
 def inverse_kernel(
     x_ref, added_ref, rate_ref,
-    base_ref, weight_ref, a_ref, cum_col_ref, cum_row_ref, key_col_ref, key_row_ref,
-    write_col_ref, write_row_ref,
+    base_hbm, weight_hbm, a_hbm, cum_col_ref, cum_row_ref, key_col_ref, key_row_ref,
+    base_ref, weight_ref, a_ref, write_col_ref, write_row_ref, sems,
 ):
+    pairs = ((base_ref, base_hbm), (weight_ref, weight_hbm), (a_ref, a_hbm))
     chunks = x_ref.shape[0]
     row, column = iotas(C, C)
     inclusive = row >= column
     strict = row > column
     diagonal = row == column
 
-    chunk_row, _unused = iotas(chunks, C)
+    chunk_row, _ = iotas(chunks, C)
     logits = jnp.zeros((chunks, C), F32)
     decays = jnp.zeros((chunks, C), F32)
     for n in range(chunks):
@@ -177,40 +202,61 @@
         update = [dot(beside(t, t), c) for t, c in zip(turned, carried)]
         for n, u, end in zip(ns, update, last):
             a_ref[n] = beside(*halves(jnp.where(diagonal, jnp.exp(end), 0.0) - u))
+        for copy in group_copies(pairs, sems, g):
+            copy.start()
         return key_columns
 
     key_col_ref[...] = lax.fori_loop(
         0, chunks // GROUP, group, jnp.zeros((C, chunks), F32)
     )
+    for g in range(chunks // GROUP):
+        for copy in group_copies(pairs, sems, g):
+            copy.wait()
 
 
 def chunk_inverse(blocks, added, decay_rate):
     chunks = blocks.shape[0]
-    wide = jax.ShapeDtypeStruct((chunks, C, 2 * C), BF16)
+    wide = pltpu.HBM((chunks, C, 2 * C), BF16)
     columns = jax.ShapeDtypeStruct((C, chunks), F32)
     rows = jax.ShapeDtypeStruct((chunks, C), F32)
     return pl.pallas_call(
         inverse_kernel,
         out_shape=(
-            wide, jax.ShapeDtypeStruct((chunks, C, C), BF16), wide, columns, rows, columns, rows,
+            wide, pltpu.HBM((chunks, C, C), BF16), wide, columns, rows, columns, rows,
         ),
         in_specs=[VMEM, VMEM, SMEM],
-        out_specs=(VMEM,) * 7,
-        scratch_shapes=[pltpu.VMEM((C, chunks), F32), pltpu.VMEM((chunks, C), F32)],
+        out_specs=(HBM,) * 3 + (VMEM,) * 4,
+        scratch_shapes=[
+            pltpu.VMEM((chunks, C, 2 * C), BF16),
+            pltpu.VMEM((chunks, C, C), BF16),
+            pltpu.VMEM((chunks, C, 2 * C), BF16),
+            pltpu.VMEM((C, chunks), F32),
+            pltpu.VMEM((chunks, C), F32),
+            pltpu.SemaphoreType.DMA((3, chunks // GROUP)),
+        ],
+        compiler_params=pltpu.CompilerParams(vmem_limit_bytes=16 * 2**20),
         cost_estimate=pl.CostEstimate(flops=4 * 10**9, bytes_accessed=2**21, transcendentals=0),
         name="inverse",
-    )(blocks, added, decay_rate)
+    )(near(blocks), added, decay_rate)
 
 
 def delta_kernel(
-    key_ref, x_ref, base_ref, weight_ref, a_ref, cum_col_ref, cum_row_ref, key_col_ref,
-    key_row_ref, out_ref, b_ref, qe_ref, su_ref,
+    key_hbm, x_ref, base_hbm, weight_hbm, a_hbm, cum_col_ref, cum_row_ref, key_col_ref,
+    key_row_ref, out_ref, key_ref, base_ref, weight_ref, a_ref, b_ref, qe_ref, su_ref, sems,
 ):
     chunks = x_ref.shape[0]
+    pairs = (
+        (key_hbm, key_ref), (base_hbm, base_ref), (weight_hbm, weight_ref), (a_hbm, a_ref),
+    )
+    for g in range(chunks // GROUP):
+        for copy in group_copies(pairs, sems, g):
+            copy.start()
     row, column = iotas(C, C)
     inclusive = row >= column
 
     def prepare(g):
+        for copy in group_copies(pairs, sems, g):
+            copy.wait()
         ns = [g * GROUP + k for k in range(GROUP)]
         keys = [key_ref[n, 0:C] for n in ns]
         queries = [x_ref[n, 0:C] for n in ns]
@@ -270,16 +316,22 @@
     return pl.pallas_call(
         delta_kernel,
         out_shape=jax.ShapeDtypeStruct((chunks, C, C), BF16),
-        in_specs=[VMEM] * 9,
+        in_specs=[HBM, VMEM, HBM, HBM, HBM] + [VMEM] * 4,
         out_specs=VMEM,
         scratch_shapes=[
+            pltpu.VMEM(keys.shape, BF16),
+            pltpu.VMEM((chunks, C, 2 * C), BF16),
+            pltpu.VMEM((chunks, C, C), BF16),
+            pltpu.VMEM((chunks, C, 2 * C), BF16),
             pltpu.VMEM((chunks, C, C), F32),
             pltpu.VMEM((chunks, C, 2 * C), BF16),
             pltpu.VMEM((chunks, C, C), F32),
+            pltpu.SemaphoreType.DMA((4, chunks // GROUP)),
         ],
+        compiler_params=pltpu.CompilerParams(vmem_limit_bytes=16 * 2**20),
         cost_estimate=pl.CostEstimate(flops=4 * 10**9, bytes_accessed=2**21, transcendentals=0),
         name="delta",
-    )(keys, blocks, *parts)
+    )(far(keys), near(blocks), *[far(p) for p in parts[:3]], *parts[3:])
 
 
 def slots_kernel(index_ref, dest_ref, source_ref, count_ref):
@@ -320,21 +372,27 @@
         in_specs=[SMEM],
         out_specs=(SMEM, SMEM),
         scratch_shapes=[pltpu.SMEM((experts,), jnp.int32)],
+        compiler_params=pltpu.CompilerParams(vmem_limit_bytes=2**20),
         name="slots",
     )(index)
 
 
 def project_kernel(
-    rec_ref, gate_ref, head_gain_ref, residual_ref, gain_ref, source_ref, place_ref,
+    rec_ref, gate_hbm, head_gain_ref, residual_hbm, gain_ref, source_ref, place_ref,
     *rest,
 ):
     weight_refs = rest[:8]
-    normed_ref, out_ref, gated_ref, mixed_ref, w_ref, sems = rest[8:]
+    normed_ref, out_ref, gate_ref, residual_ref, gated_ref, mixed_ref, w_ref, sems = rest[8:]
+    gate_copy = pltpu.make_async_copy(gate_hbm, gate_ref, sems.at[8])
+    gate_copy.start()
     copies = [
         pltpu.make_async_copy(weight_refs[k], w_ref.at[k], sems.at[k]) for k in range(8)
     ]
     for copy in copies:
         copy.start()
+    residual_copy = pltpu.make_async_copy(residual_hbm, residual_ref, sems.at[9])
+    residual_copy.start()
+    gate_copy.wait()
     heads = rec_ref.shape[0]
     head_gain = head_gain_ref[...]
     for h in range(heads):
@@ -346,6 +404,7 @@
         copies[k].wait()
         mixed_ref[place_ref[k]] = dot(gated_ref[...], w_ref[k])
     total = jnp.concatenate([mixed_ref[k] for k in range(8)], axis=1)
+    residual_copy.wait()
     total = total + residual_ref[0].astype(F32)
     centred = total - jnp.mean(total, axis=1, keepdims=True)
     variance = jnp.mean(centred * centred, axis=1, keepdims=True)
@@ -377,121 +436,114 @@
             jax.ShapeDtypeStruct((tokens, tiles, C), BF16),
             jax.ShapeDtypeStruct((source.shape[0], tiles, C), BF16),
         ),
-        in_specs=[VMEM] * 5 + [SMEM] * 2 + [HBM] * 8,
+        in_specs=[VMEM, HBM, VMEM, HBM, VMEM] + [SMEM] * 2 + [HBM] * 8,
         out_specs=(VMEM, VMEM),
         scratch_shapes=[
+            pltpu.VMEM((1, tokens, features), BF16),
+            pltpu.VMEM((1, tokens, features), BF16),
             pltpu.VMEM((tokens, features), BF16),
             pltpu.VMEM((8, tokens, features // 8), F32),
             pltpu.VMEM((8, features, features // 8), BF16),
-            pltpu.SemaphoreType.DMA((8,)),
+            pltpu.SemaphoreType.DMA((10,)),
         ],
+        compiler_params=pltpu.CompilerParams(vmem_limit_bytes=24 * 2**20),
         cost_estimate=pl.CostEstimate(flops=10**9, bytes_accessed=2**24, transcendentals=0),
         name="project",
-    )(recurrent, gate, head_gain, residual, gain, source, place, *weights)
-
-
-FF_BLOCK = 256
-
-
-def expert_kernel(x_ref, gate_ref, up_ref, down_ref, out_ref, rows_ref, hidden_ref, made_ref):
-    step = pl.program_id(0)
-    slots_ = x_ref.shape[0]
-    tiles = x_ref.shape[1]
-    groups = slots_ // 16
-    ff_steps = hidden_ref.shape[0]
-
-    @pl.when(step == 0)
-    def _():
-        swap = swap_matrix()
-
-        def turn(i, carry):
-            for k in range(2):
-                start = pl.multiple_of((i * 4 + k * 2) * 16, 16)
-                other = pl.multiple_of(start + 16, 16)
-                turned = dot(
-                    swap,
-                    beside(
-                        x_ref[pl.ds(start, 16)].reshape(16 * tiles, C),
-                        x_ref[pl.ds(other, 16)].reshape(16 * tiles, C),
-                    ),
-                ).astype(BF16)
-                for j in range(tiles):
-                    part = turned[j * 16 : (j + 1) * 16]
-                    rows_ref[pl.ds(start, 16), j * C : (j + 1) * C] = part[:, :C]
-                    rows_ref[pl.ds(other, 16), j * C : (j + 1) * C] = part[:, C:]
-            return carry
-
-        lax.fori_loop(0, groups // 4, turn, 0)
-
-    @pl.when(step < ff_steps)
-    def _():
+    )(
+        near(recurrent), far(gate), head_gain, far(residual), gain, source, place,
+        *[far(w) for w in weights],
+    )
+
+
+FF_BLOCK = 512
+DOWN_ROWS = 384
+TURN_UNROLL = 6
+
+
+def expert_kernel(
+    x_ref, gate_hbm, up_hbm, down_hbm, out_ref, gate_ref, up_ref, down_ref, rows_ref, hidden_ref,
+    sems,
+):
+    slots_, tiles, _ = x_ref.shape
+    copies = [
+        pltpu.make_async_copy(source, target, sems.at[k])
+        for k, (source, target) in enumerate(
+            ((gate_hbm, gate_ref), (up_hbm, up_ref), (down_hbm, down_ref))
+        )
+    ]
+    for copy in copies:
+        copy.start()
+    swap = swap_matrix()
+
+    def turn(i, carry):
+        for k in range(TURN_UNROLL):
+            start = pl.multiple_of((i * TURN_UNROLL + k) * 32, 32)
+            pieces = [x_ref[pl.ds(start + o, 16)].reshape(16 * tiles, C) for o in (0, 16)]
+            turned = dot(swap, beside(*pieces)).astype(BF16)
+            for j in range(tiles):
+                part = turned[j * 16 : (j + 1) * 16]
+                rows_ref[pl.ds(start, 16), j * C : (j + 1) * C] = part[:, :C]
+                rows_ref[pl.ds(start + 16, 16), j * C : (j + 1) * C] = part[:, C:]
+        return carry
+
+    lax.fori_loop(0, slots_ // (32 * TURN_UNROLL), turn, 0)
+    copies[0].wait()
+    copies[1].wait()
+
+    def widen(f, carry):
+        columns = pl.ds(pl.multiple_of(f * FF_BLOCK, FF_BLOCK), FF_BLOCK)
         rows = rows_ref[...]
-        gate = jnp.minimum(dot(rows, gate_ref[...]), CLAMP_LIMIT)
-        up = jnp.clip(dot(rows, up_ref[...]), -CLAMP_LIMIT, CLAMP_LIMIT)
+        gate = jnp.minimum(dot(rows, gate_ref[:, columns]), CLAMP_LIMIT)
+        up = jnp.clip(dot(rows, up_ref[:, columns]), -CLAMP_LIMIT, CLAMP_LIMIT)
         hidden = gate / (1.0 + jnp.exp(-SWISH_SLOPE * gate)) * (up + 1.0)
-        hidden_ref[step] = hidden.astype(BF16)
-
-    @pl.when(step >= ff_steps)
-    def _():
-        total = dot(hidden_ref[0], down_ref[0:FF_BLOCK])
-        for k in range(1, ff_steps):
-            total = total + dot(hidden_ref[k], down_ref[k * FF_BLOCK : (k + 1) * FF_BLOCK])
-        made_ref[step - ff_steps] = total.astype(BF16)
-
-    @pl.when(step == pl.num_programs(0) - 1)
-    def _():
-        swap = swap_matrix()
-        down_steps, _rows, width = made_ref.shape
-
-        def stacked(start):
-            pieces = []
-            for d in range(down_steps):
-                piece = made_ref[d, pl.ds(start, 16), :]
-                pieces += [piece[:, j * C : (j + 1) * C] for j in range(width // C)]
-            return jnp.concatenate(pieces, axis=0)
-
-        def turn(i, carry):
-            for k in range(2):
-                start = pl.multiple_of((i * 4 + k * 2) * 16, 16)
-                other = pl.multiple_of(start + 16, 16)
-                turned = dot(swap, beside(stacked(start), stacked(other))).astype(BF16)
-                out_ref[pl.ds(start, 16)] = turned[:, :C].reshape(16, tiles, C)
-                out_ref[pl.ds(other, 16)] = turned[:, C:].reshape(16, tiles, C)
-            return carry
-
-        lax.fori_loop(0, groups // 4, turn, 0)
+        hidden_ref[:, columns] = hidden.astype(BF16)
+        return carry
+
+    lax.fori_loop(0, hidden_ref.shape[1] // FF_BLOCK, widen, 0)
+    copies[2].wait()
+
+    def narrow(i, carry):
+        start = pl.multiple_of(i * DOWN_ROWS, DOWN_ROWS)
+        made = dot(hidden_ref[pl.ds(start, DOWN_ROWS)], down_ref[...]).astype(BF16)
+        for g in range(0, DOWN_ROWS, 32):
+            stacked = [
+                jnp.concatenate(
+                    [made[k : k + 16, j * C : (j + 1) * C] for j in range(tiles)], axis=0
+                )
+                for k in (g, g + 16)
+            ]
+            turned = dot(swap, beside(*stacked)).astype(BF16)
+            out_ref[pl.ds(start + g, 16)] = turned[:, :C].reshape(16, tiles, C)
+            out_ref[pl.ds(start + g + 16, 16)] = turned[:, C:].reshape(16, tiles, C)
+        return carry
+
+    lax.fori_loop(0, slots_ // DOWN_ROWS, narrow, 0)
 
 
 def expert(rows, gate_weight, up_weight, down_weight):
-    slots_, tiles, _lanes = rows.shape
+    slots_, _, _ = rows.shape
     features, hidden = gate_weight.shape
-    ff_steps = hidden // FF_BLOCK
-    width = 512
-    down_steps = features // width
     return pl.pallas_call(
         expert_kernel,
-        grid=(ff_steps + down_steps,),
         out_shape=jax.ShapeDtypeStruct(rows.shape, BF16),
-        in_specs=[
-            pl.BlockSpec(rows.shape, lambda i: (0, 0, 0), pipeline_mode=pl.Buffered(1)),
-            pl.BlockSpec((features, FF_BLOCK), lambda i: (0, jnp.minimum(i, ff_steps - 1))),
-            pl.BlockSpec((features, FF_BLOCK), lambda i: (0, jnp.minimum(i, ff_steps - 1))),
-            pl.BlockSpec((hidden, width), lambda i: (0, jnp.maximum(i - ff_steps, 0))),
+        in_specs=[VMEM, HBM, HBM, HBM],
+        out_specs=VMEM,
+        scratch_shapes=[
+            pltpu.VMEM(gate_weight.shape, BF16),
+            pltpu.VMEM(up_weight.shape, BF16),
+            pltpu.VMEM(down_weight.shape, BF16),
+            pltpu.VMEM((slots_, features), BF16),
+            pltpu.VMEM((slots_, hidden), BF16),
+            pltpu.SemaphoreType.DMA((3,)),
         ],
-        out_specs=pl.BlockSpec(rows.shape, lambda i: (0, 0, 0), pipeline_mode=pl.Buffered(1)),
-        scratch_shapes=[
-            pltpu.VMEM((slots_, features), BF16),
-            pltpu.VMEM((ff_steps, slots_, FF_BLOCK), BF16),
-            pltpu.VMEM((down_steps, slots_, width), BF16),
-        ],
-        compiler_params=pltpu.CompilerParams(dimension_semantics=("arbitrary",)),
+        compiler_params=pltpu.CompilerParams(vmem_limit_bytes=36 * 2**20),
         cost_estimate=pl.CostEstimate(flops=10**10, bytes_accessed=2**24, transcendentals=0),
         name="expert",
-    )(rows, gate_weight, up_weight, down_weight)
+    )(near(rows), far(gate_weight), far(up_weight), far(down_weight))
 
 
 def combine_kernel(back_ref, normed_ref, gain_ref, dest_ref, weight_ref, out_ref, z_ref):
-    tokens, tiles, _lanes = normed_ref.shape
+    tokens, tiles, _ = normed_ref.shape
     swap = swap_matrix()
     gain = gain_ref[...]
 
@@ -526,15 +578,16 @@
 
 
 def combine(back, normed, gain, dest, weight):
-    tokens, tiles, _lanes = normed.shape
+    tokens, tiles, _ = normed.shape
     return pl.pallas_call(
         combine_kernel,
         out_shape=jax.ShapeDtypeStruct((1, tokens, tiles * C), F32),
         in_specs=[VMEM] * 3 + [SMEM] * 2,
         out_specs=VMEM,
         scratch_shapes=[pltpu.VMEM((tokens, tiles, C), F32)],
+        compiler_params=pltpu.CompilerParams(vmem_limit_bytes=12 * 2**20),
         name="combine",
-    )(back, normed, gain, dest, weight)
+    )(near(back), near(normed), gain, dest, weight)
 
 
 def gathered(block):
@@ -549,7 +602,7 @@
     return found, jnp.stack(places + others).astype(jnp.int32)
 
 
-def per_device(
+def layer(
     residual,
     query,
     key,
@@ -589,7 +642,9 @@
     recurrent = delta(keys, blocks, parts)
     recurrent, found = lax.optimization_barrier((recurrent, found))
     returned = lax.all_to_all(recurrent, "sp", split_axis=0, concat_axis=0, tiled=True)
-    weights = found + [lax.ppermute(b, "dp_1", [(0, 1), (1, 0)]) for b in found]
+    weights = list(found)
+    for b in found:
+        weights.append(lax.ppermute(b, "dp_1", [(0, 1), (1, 0)]))
     normed, rows = project(
         returned,
         output_gate_input,
@@ -622,7 +677,7 @@
 def solution(mesh):
     torus = Mesh(mesh.devices.reshape(mesh.shape["sp"], 4, 2), ("sp", "dp_0", "dp_1"))
     return jax.shard_map(
-        per_device,
+        layer,
         mesh=torus,
         in_specs=(
             P(DP, "sp", None),

time: 230 us -> 216 us (0.939)
  Pallas kernels: 69.2 us -> 56.3 us
  waiting for transfers between devices: 24.2 us -> 27.3 us
  local copies, waits for them, and re-layouts: 2.71 us -> 0.13 us
    pallas_call x2, Pallas kernels: 36.7 us -> 27.2 us  [the longest x1 15.1 us: expert(): pl.pallas_call(expert_kernel, out_shape=jax.ShapeDtypeStruct(rows.shape,...]
    ppermute x3, waiting for transfers between devices: 20.4 us -> 22.8 us  [gathered(): found.append(lax.ppermute(block, 'dp_0', pairs))]
    pallas_call x1, Pallas kernels: 9.78 us -> 7.4 us  [project(): pl.pallas_call(project_kernel, out_shape=(jax.ShapeDtypeStruct((tokens, t...]
where the time goes in v2:
time: 216 us; the launch traced here: 215 us
  blocking collectives  113 us (52%)
  Pallas kernels  56.3 us (26%)
  waiting for transfers between devices  27.3 us (13%)
  starting transfers between devices  17.3 us (8%)
    all_to_all x1, blocking collectives, layer(): rows = lax.all_to_all(rows, SP_DP, split_axis=0, concat_axis=0, tiled=True)  48.1 us
    all_to_all x1, blocking collectives, layer(): back = lax.all_to_all(made, SP_DP, split_axis=0, concat_axis=0, tiled=True)  45.6 us
    ppermute x3, waiting for transfers between devices, gathered(): found.append(lax.ppermute(block, 'dp_0', pairs))  22.8 us
    all_to_all x1, blocking collectives, layer(): keys = lax.all_to_all(keys, 'sp', split_axis=0, concat_axis=0, tiled=True)  19.5 us
    pallas_call x1, Pallas kernels, expert(): pl.pallas_call(expert_kernel, out_shape=jax.ShapeDtypeStruct(rows.shape,...  15.1 us
    pallas_call x1, Pallas kernels, chunk_inverse(): pl.pallas_call(inverse_kernel, out_shape=(wide, pltpu.HBM((chunks, C, C),...  12.1 us
    pallas_call x1, Pallas kernels, delta(): pl.pallas_call(delta_kernel, out_shape=jax.ShapeDtypeStruct((chunks, C, C...  7.85 us
    pallas_call x1, Pallas kernels, project(): pl.pallas_call(project_kernel, out_shape=(jax.ShapeDtypeStruct((tokens, t...  7.4 us
  transfers between devices with their start and end apart: 9, of which 2 were waited for; matrix products, arithmetic and copies ran while one was open for 0% of the time, Pallas kernels for 12%

profile of v2, /device:TPU:1, one launch (start us, length us, event | category | flops | bytes accessed | tf_op | source)
XLA Modules:
  0.0 215.2 jit_solution(4054853713130734779)
XLA Ops:
  0.0 0.0 copy-start.7
  0.0 0.0 copy-start.6
  0.0 3.5 %pack.1 = (bf16[16,144,128]{2,1,0:T(8,128)(2,1)S(1)}, bf16[16,256,128]{2,1,0:T(8,128)(2,1)}) custom-call(bf16[1,128,2048]{2,1,0:T(8,128)(2,1)} %q_ref.1, bf16[1,128,2048]{2,1,0:T(8,128)(2,1)} %k_ref.1, bf16[1,128,2048]{2,1,0:T(8,128)(2,1)} %v_ref.1, bf16[1,16,128]{2,1,0:T(8,128)(2,1)} %bitcast.41, bf16[1,16,128]{2,1,0:T(8,128)(2,1)} %bitcast.42), custom_call_target="tpu_custom_call" | custom-call | tf_op jit(solution)/shard_map/pack/pallas_call | solution.py:82
  3.6 19.5 %all_to_all.25.x_ref.key_hbm = bf16[16,144,128]{2,1,0:T(8,128)(2,1)S(1)} all-to-all(bf16[16,144,128]{2,1,0:T(8,128)(2,1)S(1)} %get-tuple-element.23), channel_id=1, replica_groups=mesh['sp'=16,'dp_0'=4,'dp_1'=2] {'sp'}, dimensions={0} | all-to-all | bytes 1179648 | tf_op jit(solution)/shard_map/all_to_all | solution.py:639
  23.1 0.0 copy-start
  23.1 3.7 %all-to-all-start.1 = ((bf16[16,256,128]{2,1,0:T(8,128)(2,1)}), bf16[16,256,128]{2,1,0:T(8,128)(2,1)S(1)}, u32[]{:S(2)}, u32[]{:S(2)}) async-start(bf16[16,256,128]{2,1,0:T(8,128)(2,1)} %get-tuple-element.24), calls=%async_computation.1 | async-start | bytes 2097152 | tf_op jit(solution)/shard_map/all_to_all | solution.py:640
  26.8 0.0 copy-done.7
  26.8 3.0 %collective-permute-start.1 = (bf16[2048,256]{1,0:T(8,128)(2,1)S(1)}, bf16[2048,256]{1,0:T(8,128)(2,1)}, u32[]{:S(2)}, u32[]{:S(2)}) collective-permute-start(bf16[2048,256]{1,0:T(8,128)(2,1)S(1)} %copy-done.7), channel_id=1, source_target_pairs={{0,4},{2,6},{4,0},{6,2},{1,5},{3,7},{5,1},{7,3},{8,12},{10,14},{12... | collective-permute-start | bytes 3145736 | tf_op jit(solution)/shard_map/ppermute | solution.py:599
  29.8 0.4 collective-permute-start
  30.2 2.3 %collective-permute-start.2 = (bf16[2048,256]{1,0:T(8,128)(2,1)S(1)}, bf16[2048,256]{1,0:T(8,128)(2,1)}, u32[]{:S(2)}, u32[]{:S(2)}) collective-permute-start(bf16[2048,256]{1,0:T(8,128)(2,1)S(1)} %copy-done.7), channel_id=1, source_target_pairs={{0,6},{2,0},{4,2},{6,4},{1,7},{3,1},{5,3},{7,5},{8,14},{10,8},{12,... | collective-permute-start | bytes 3145736 | tf_op jit(solution)/shard_map/ppermute | solution.py:599
  33.1 0.0 copy-done.6
  33.1 12.1 %inverse.1 = (bf16[16,128,256]{2,1,0:T(8,128)(2,1)}, bf16[16,128,128]{2,1,0:T(8,128)(2,1)}, bf16[16,128,256]{2,1,0:T(8,128)(2,1)}, f32[128,16]{1,0:T(8,128)S(1)}...) custom-call(bf16[16,144,128]{2,1,0:T(8,128)(2,1)S(1)} %all_to_all.25.x_ref.key_hbm, ...), custom_call_target="tpu_custom_call" | custom-call | flops 4000000000 | bytes 2097152 | tf_op jit(solution)/shard_map/inverse/pallas_call | solution.py:222
  45.3 0.0 copy-done
  45.3 0.0 all-to-all-done.1.x_ref
  45.3 0.0 copy-start.4
  45.3 0.0 copy-start.2
  45.3 0.0 copy-start.5
  45.3 7.8 %delta.1 = bf16[16,128,128]{2,1,0:T(8,128)(2,1)} custom-call(bf16[16,144,128]{2,1,0:T(8,128)(2,1)} %copy-done, bf16[16,256,128]{2,1,0:T(8,128)(2,1)S(1)} %all-to-all-done.1.x_ref, bf16[16,128,256]{2,1,0:T(8,128)(2,1)} %get-tuple-element.25.base_hbm, bf16[16,128,128]{2,1,0:T(8,128)(2,1)} %get-tuple-element.26.weight_hbm, ...), custom_call_target="tpu_custom_call" | custom-call | flops 4000000000 | bytes 2097152 | tf_op jit(solution)/shard_map/delta/pallas_call | solution.py:316
  53.2 0.0 collective-permute-done.1.rest_2_
  53.2 22.8 %collective-permute-done.rest_1_ = bf16[2048,256]{1,0:T(8,128)(2,1)} collective-permute-done((bf16[2048,256]{1,0:T(8,128)(2,1)S(1)}, bf16[2048,256]{1,0:T(8,128)(2,1)}, u32[]{:S(2)}, u32[]{:S(2)}) %collective-permute-start) | collective-permute-done | bytes 1048608 | tf_op jit(solution)/shard_map/ppermute | solution.py:599
  76.0 0.0 collective-permute-done.2.rest_3_
  76.0 0.9 collective-permute-start.3
  76.9 0.0 collective-permute-start.4
  76.9 0.5 collective-permute-start.5
  77.4 0.0 collective-permute-start.6
  77.4 6.6 %all-to-all-start.2 = ((bf16[16,128,128]{2,1,0:T(8,128)(2,1)}), bf16[16,128,128]{2,1,0:T(8,128)(2,1)S(1)}, u32[]{:S(2)}, u32[]{:S(2)}) async-start(bf16[16,128,128]{2,1,0:T(8,128)(2,1)} %delta.1), calls=%async_computation.2 | async-start | bytes 1048576 | tf_op jit(solution)/shard_map/all_to_all | solution.py:644
  84.1 0.0 copy-done.4
  84.1 6.0 %slots.1 = (s32[512]{0:T(512)S(1)}, s32[768]{0:T(1024)S(1)}) custom-call(s32[512]{0:T(512)S(1)} %bitcast.38), custom_call_target="tpu_custom_call" | custom-call | tf_op jit(solution)/shard_map/slots/pallas_call | solution.py:366
  90.1 0.1 stack.35.place_ref
  90.2 4.4 %all-to-all-done.2.rec_ref = bf16[16,128,128]{2,1,0:T(8,128)(2,1)S(1)} async-done(((bf16[16,128,128]{2,1,0:T(8,128)(2,1)}), bf16[16,128,128]{2,1,0:T(8,128)(2,1)S(1)}, u32[]{:S(2)}, u32[]{:S(2)}) %all-to-all-start.2) | async-done | bytes 524320 | tf_op jit(solution)/shard_map/all_to_all | solution.py:644
  94.6 0.0 collective-permute-done.3.rest_4_
  94.6 0.0 collective-permute-done.4.rest_5_
  94.6 0.0 collective-permute-done.5.rest_6_
  94.6 0.0 collective-permute-done.6.rest_7_
  94.6 0.0 copy-done.2
  94.6 0.0 copy-done.5
  94.6 7.4 %project.1 = (bf16[128,16,128]{2,1,0:T(8,128)(2,1)S(1)}, bf16[768,16,128]{2,1,0:T(8,128)(2,1)S(1)}) custom-call(bf16[16,128,128]{2,1,0:T(8,128)(2,1)S(1)} %all-to-all-done.2.rec_ref, bf16[1,128,2048]{2,1,0:T(8,128)(2,1)} %gate_hbm.1, f32[1,128]{1,0:T(1,128)S(1)} %bitcast.39, bf16[1,128,2048]{2,1,0:T(8,128)(2,1)} %residual_hbm.1, f32[1,2048]{1,0:T(1,128)S(1)} %bitcast.36, ...), custom_call_target="tpu_custom_call" | custom-call | flops 1000000000 | bytes 16777216 | tf_op jit(solution)/shard_map/project/pallas_call | solution.py:433
  102.1 48.1 %all_to_all.26 = bf16[128,96,128]{2,1,0:T(8,128)(2,1)S(1)} all-to-all(bf16[128,96,128]{2,1,0:T(8,128)(2,1)S(1)} %bitcast.32), channel_id=1, replica_groups=mesh['sp'=16,'dp_0'=4,'dp_1'=2] {'sp','dp_0','dp_1'}, dimensions={0} | all-to-all | bytes 6291456 | tf_op jit(solution)/shard_map/all_to_all | solution.py:659
  150.1 15.1 %expert.1 = bf16[768,16,128]{2,1,0:T(8,128)(2,1)S(1)} custom-call(bf16[768,16,128]{2,1,0:T(8,128)(2,1)S(1)} %bitcast.33, bf16[2048,1024]{1,0:T(8,128)(2,1)} %bitcast.43, bf16[2048,1024]{1,0:T(8,128)(2,1)} %bitcast.44, bf16[1024,2048]{1,0:T(8,128)(2,1)} %bitcast.45), custom_call_target="tpu_custom_call" | custom-call | flops 10000000000 | bytes 16777216 | tf_op jit(solution)/shard_map/expert/pallas_call | solution.py:526
  165.2 0.0 copy-start.1
  165.2 0.0 copy-start.3
  165.2 45.6 %all_to_all.27 = bf16[128,96,128]{2,1,0:T(8,128)(2,1)S(1)} all-to-all(bf16[128,96,128]{2,1,0:T(8,128)(2,1)S(1)} %bitcast.34), channel_id=1, replica_groups=mesh['sp'=16,'dp_0'=4,'dp_1'=2] {'sp','dp_0','dp_1'}, dimensions={0} | all-to-all | bytes 6291456 | tf_op jit(solution)/shard_map/all_to_all | solution.py:667
  210.9 0.0 copy-done.1
  210.9 0.0 copy-done.3
  210.9 4.3 %combine.1 = f32[1,128,2048]{2,1,0:T(8,128)} custom-call(bf16[768,16,128]{2,1,0:T(8,128)(2,1)S(1)} %bitcast.31, bf16[128,16,128]{2,1,0:T(8,128)(2,1)S(1)} %get-tuple-element.39.normed_ref, f32[1,2048]{1,0:T(1,128)S(1)} %bitcast.35, s32[512]{0:T(512)S(1)} %get-tuple-element.40.dest_ref, f32[512]{0:T(512)S(1)} %bitcast.37), custom_call_target="tpu_custom_call" | custom-call | tf_op jit(solution)/shard_map/combine/pallas_call | solution.py:582
Async XLA Ops:
  0.0 26.8 %copy-start.7 = (bf16[2048,256]{1,0:T(8,128)(2,1)S(1)}, bf16[2048,256]{1,0:T(8,128)(2,1)}, u32[]{:S(2)}) copy-start(bf16[2048,256]{1,0:T(8,128)(2,1)} %rest_0_) | copy-start | bytes 3145732
  0.0 33.1 %copy-start.6 = (f32[1,1,2048]{2,1,0:T(1,128)S(1)}, f32[1,1,2048]{2,1,0:T(1,128)}, u32[]{:S(2)}) copy-start(f32[1,1,2048]{2,1,0:T(1,128)} %param.25) | copy-start | bytes 24580
  23.1 22.2 %copy-start = (bf16[16,144,128]{2,1,0:T(8,128)(2,1)}, bf16[16,144,128]{2,1,0:T(8,128)(2,1)S(1)}, u32[]{:S(2)}) copy-start(bf16[16,144,128]{2,1,0:T(8,128)(2,1)S(1)} %all_to_all.25.x_ref.key_hbm) | copy-start | bytes 1769476
  23.1 22.2 %all-to-all-start.1 = ((bf16[16,256,128]{2,1,0:T(8,128)(2,1)}), bf16[16,256,128]{2,1,0:T(8,128)(2,1)S(1)}, u32[]{:S(2)}, u32[]{:S(2)}) async-start(bf16[16,256,128]{2,1,0:T(8,128)(2,1)} %get-tuple-element.24), calls=%async_computation.1 | async-start | bytes 2097152 | tf_op jit(solution)/shard_map/all_to_all | solution.py:640
  26.8 26.4 %collective-permute-start.1 = (bf16[2048,256]{1,0:T(8,128)(2,1)S(1)}, bf16[2048,256]{1,0:T(8,128)(2,1)}, u32[]{:S(2)}, u32[]{:S(2)}) collective-permute-start(bf16[2048,256]{1,0:T(8,128)(2,1)S(1)} %copy-done.7), channel_id=1, source_target_pairs={{0,4},{2,6},{4,0},{6,2},{1,5},{3,7},{5,1},{7,3},{8,12},{10,14},{12... | collective-permute-start | bytes 3145736 | tf_op jit(solution)/shard_map/ppermute | solution.py:599
  29.8 46.2 %collective-permute-start = (bf16[2048,256]{1,0:T(8,128)(2,1)S(1)}, bf16[2048,256]{1,0:T(8,128)(2,1)}, u32[]{:S(2)}, u32[]{:S(2)}) collective-permute-start(bf16[2048,256]{1,0:T(8,128)(2,1)S(1)} %copy-done.7), channel_id=1, source_target_pairs={{0,2},{2,4},{4,6},{6,0},{1,3},{3,5},{5,7},{7,1},{8,10},{10,12},{12... | collective-permute-start | bytes 3145736 | tf_op jit(solution)/shard_map/ppermute | solution.py:599
  30.2 45.9 %collective-permute-start.2 = (bf16[2048,256]{1,0:T(8,128)(2,1)S(1)}, bf16[2048,256]{1,0:T(8,128)(2,1)}, u32[]{:S(2)}, u32[]{:S(2)}) collective-permute-start(bf16[2048,256]{1,0:T(8,128)(2,1)S(1)} %copy-done.7), channel_id=1, source_target_pairs={{0,6},{2,0},{4,2},{6,4},{1,7},{3,1},{5,3},{7,5},{8,14},{10,8},{12,... | collective-permute-start | bytes 3145736 | tf_op jit(solution)/shard_map/ppermute | solution.py:599
  45.3 38.8 %copy-start.4 = (s32[1,128,4]{1,2,0:T(4,128)S(1)}, s32[1,128,4]{1,2,0:T(4,128)}, u32[]{:S(2)}) copy-start(s32[1,128,4]{1,2,0:T(4,128)} %param.30) | copy-start | bytes 6148
  45.3 49.3 %copy-start.2 = (f32[2048]{0:T(1024)S(1)}, f32[2048]{0:T(1024)}, u32[]{:S(2)}) copy-start(f32[2048]{0:T(1024)} %param.29) | copy-start | bytes 24580
  45.3 49.3 %copy-start.5 = (f32[128]{0:T(128)S(1)}, f32[128]{0:T(128)}, u32[]{:S(2)}) copy-start(f32[128]{0:T(128)} %param.27) | copy-start | bytes 1540
  76.0 18.6 %collective-permute-start.3 = (bf16[2048,256]{1,0:T(8,128)(2,1)S(1)}, bf16[2048,256]{1,0:T(8,128)(2,1)}, u32[]{:S(2)}, u32[]{:S(2)}) collective-permute-start(bf16[2048,256]{1,0:T(8,128)(2,1)S(1)} %copy-done.7), channel_id=1, source_target_pairs={{0,1},{1,0},{2,3},{3,2},{4,5},{5,4},{6,7},{7,6},{8,9},{9,8},{10,11... | collective-permute-start | bytes 3145736 | tf_op jit(solution)/shard_map/ppermute | solution.py:647
  76.9 17.7 %collective-permute-start.4 = (bf16[2048,256]{1,0:T(8,128)(2,1)}, bf16[2048,256]{1,0:T(8,128)(2,1)}, u32[]{:S(2)}, u32[]{:S(2)}) collective-permute-start(bf16[2048,256]{1,0:T(8,128)(2,1)} %collective-permute-done.rest_1_), channel_id=1, source_target_pairs={{0,1},{1,0},{2,3},{3,2},{4,5},{5,4},{6,7},{7,6},{8,9},{9,8},{10,11... | collective-permute-start | bytes 3145736 | tf_op jit(solution)/shard_map/ppermute | solution.py:647
  76.9 17.7 %collective-permute-start.5 = (bf16[2048,256]{1,0:T(8,128)(2,1)}, bf16[2048,256]{1,0:T(8,128)(2,1)}, u32[]{:S(2)}, u32[]{:S(2)}) collective-permute-start(bf16[2048,256]{1,0:T(8,128)(2,1)} %collective-permute-done.1.rest_2_), channel_id=1, source_target_pairs={{0,1},{1,0},{2,3},{3,2},{4,5},{5,4},{6,7},{7,6},{8,9},{9,8},{10,11... | collective-permute-start | bytes 3145736 | tf_op jit(solution)/shard_map/ppermute | solution.py:647
  77.4 17.2 %collective-permute-start.6 = (bf16[2048,256]{1,0:T(8,128)(2,1)}, bf16[2048,256]{1,0:T(8,128)(2,1)}, u32[]{:S(2)}, u32[]{:S(2)}) collective-permute-start(bf16[2048,256]{1,0:T(8,128)(2,1)} %collective-permute-done.2.rest_3_), channel_id=1, source_target_pairs={{0,1},{1,0},{2,3},{3,2},{4,5},{5,4},{6,7},{7,6},{8,9},{9,8},{10,11... | collective-permute-start | bytes 3145736 | tf_op jit(solution)/shard_map/ppermute | solution.py:647
  77.4 17.2 %all-to-all-start.2 = ((bf16[16,128,128]{2,1,0:T(8,128)(2,1)}), bf16[16,128,128]{2,1,0:T(8,128)(2,1)S(1)}, u32[]{:S(2)}, u32[]{:S(2)}) async-start(bf16[16,128,128]{2,1,0:T(8,128)(2,1)} %delta.1), calls=%async_computation.2 | async-start | bytes 1048576 | tf_op jit(solution)/shard_map/all_to_all | solution.py:644
  165.2 45.7 %copy-start.1 = (f32[2048]{0:T(1024)S(1)}, f32[2048]{0:T(1024)}, u32[]{:S(2)}) copy-start(f32[2048]{0:T(1024)} %param.35) | copy-start | bytes 24580
  165.2 45.6 %copy-start.3 = (f32[1,128,4]{1,2,0:T(4,128)S(1)}, f32[1,128,4]{1,2,0:T(4,128)}, u32[]{:S(2)}) copy-start(f32[1,128,4]{1,2,0:T(4,128)} %param.31) | copy-start | bytes 6148

commit v3 on v2

--- a/solution.py
+++ b/solution.py
@@ -54,17 +54,17 @@
     return jnp.where((row % 16) * 16 + row // 16 == column, 1.0, 0.0).astype(BF16)
 
 
-def pack_kernel(q_ref, k_ref, v_ref, logit_ref, decay_ref, key_out_ref, out_ref, sems):
+def pack_kernel(q_ref, k_ref, v_ref, logit_ref, decay_ref, out_ref, sems):
     heads = out_ref.shape[0]
     copies = []
     for h in range(heads):
         columns = slice(h * C, (h + 1) * C)
-        for source, target in (
-            (k_ref, key_out_ref.at[h, 0:C]),
-            (q_ref, out_ref.at[h, 0:C]),
-            (v_ref, out_ref.at[h, C : 2 * C]),
-        ):
-            copy = pltpu.make_async_copy(source.at[0, :, columns], target, sems.at[len(copies)])
+        for k, source in enumerate((k_ref, q_ref, v_ref)):
+            copy = pltpu.make_async_copy(
+                source.at[0, :, columns],
+                out_ref.at[h, k * C : (k + 1) * C],
+                sems.at[len(copies)],
+            )
             copy.start()
             copies.append(copy)
     logits = logit_ref[0].astype(F32)
@@ -72,7 +72,7 @@
     extra_row, _ = iotas(EXTRA, C)
     for h in range(heads):
         extra = jnp.where(extra_row == 0, logits[h : h + 1], decays[h : h + 1])
-        key_out_ref[h, C : C + EXTRA] = extra.astype(BF16)
+        out_ref[h, 3 * C : 3 * C + EXTRA] = extra.astype(BF16)
     for copy in copies:
         copy.wait()
 
@@ -81,19 +81,16 @@
     heads = logit.shape[1]
     return pl.pallas_call(
         pack_kernel,
-        out_shape=(
-            jax.ShapeDtypeStruct((heads, C + EXTRA, C), BF16),
-            jax.ShapeDtypeStruct((heads, 2 * C, C), BF16),
-        ),
+        out_shape=jax.ShapeDtypeStruct((heads, 3 * C + EXTRA, C), BF16),
         in_specs=[HBM] * 3 + [VMEM] * 2,
-        out_specs=(VMEM, VMEM),
+        out_specs=VMEM,
         scratch_shapes=[pltpu.SemaphoreType.DMA((3 * heads,))],
         compiler_params=pltpu.CompilerParams(vmem_limit_bytes=12 * 2**20),
         name="pack",
     )(far(query), far(key), far(value), far(logit), far(decay_input))
 
 
-GROUP = 4
+GROUP = 8
 
 
 def column_of(ref, n):
@@ -109,20 +106,24 @@
     return jnp.concatenate([a, b], axis=0)
 
 
-def group_copies(pairs, sems, g):
-    part = pl.ds(g * GROUP, GROUP)
-    return [
-        pltpu.make_async_copy(source.at[part], target.at[part], sems.at[k, g])
-        for k, (source, target) in enumerate(pairs)
-    ]
-
-
-def inverse_kernel(
-    x_ref, added_ref, rate_ref,
-    base_hbm, weight_hbm, a_hbm, cum_col_ref, cum_row_ref, key_col_ref, key_row_ref,
-    base_ref, weight_ref, a_ref, write_col_ref, write_row_ref, sems,
+def recurrence_kernel(
+    x_ref, added_ref, rate_ref, out_ref, base_ref, weight_ref, a_ref, b_ref, qe_ref, su_ref,
+    cum_col_ref, cum_row_ref, key_col_ref, key_row_ref, write_col_ref, write_row_ref,
 ):
-    pairs = ((base_ref, base_hbm), (weight_ref, weight_hbm), (a_ref, a_hbm))
+    inverse_part(
+        x_ref, added_ref, rate_ref, base_ref, weight_ref, a_ref,
+        cum_col_ref, cum_row_ref, key_col_ref, key_row_ref, write_col_ref, write_row_ref,
+    )
+    delta_part(
+        x_ref, base_ref, weight_ref, a_ref, cum_col_ref, cum_row_ref, key_col_ref, key_row_ref,
+        out_ref, b_ref, qe_ref, su_ref,
+    )
+
+
+def inverse_part(
+    x_ref, added_ref, rate_ref, base_ref, weight_ref, a_ref,
+    cum_col_ref, cum_row_ref, key_col_ref, key_row_ref, write_col_ref, write_row_ref,
+):
     chunks = x_ref.shape[0]
     row, column = iotas(C, C)
     inclusive = row >= column
@@ -133,7 +134,7 @@
     logits = jnp.zeros((chunks, C), F32)
     decays = jnp.zeros((chunks, C), F32)
     for n in range(chunks):
-        extra = x_ref[n, C : C + EXTRA].astype(F32)
+        extra = x_ref[n, 3 * C : 3 * C + EXTRA].astype(F32)
         logits = jnp.where(chunk_row == n, extra[0:1], logits)
         decays = jnp.where(chunk_row == n, extra[1:2], decays)
     softplus = jnp.maximum(decays, 0.0) + jnp.log(1.0 + jnp.exp(-jnp.abs(decays)))
@@ -202,65 +203,26 @@
         update = [dot(beside(t, t), c) for t, c in zip(turned, carried)]
         for n, u, end in zip(ns, update, last):
             a_ref[n] = beside(*halves(jnp.where(diagonal, jnp.exp(end), 0.0) - u))
-        for copy in group_copies(pairs, sems, g):
-            copy.start()
         return key_columns
 
     key_col_ref[...] = lax.fori_loop(
         0, chunks // GROUP, group, jnp.zeros((C, chunks), F32)
     )
-    for g in range(chunks // GROUP):
-        for copy in group_copies(pairs, sems, g):
-            copy.wait()
-
-
-def chunk_inverse(blocks, added, decay_rate):
-    chunks = blocks.shape[0]
-    wide = pltpu.HBM((chunks, C, 2 * C), BF16)
-    columns = jax.ShapeDtypeStruct((C, chunks), F32)
-    rows = jax.ShapeDtypeStruct((chunks, C), F32)
-    return pl.pallas_call(
-        inverse_kernel,
-        out_shape=(
-            wide, pltpu.HBM((chunks, C, C), BF16), wide, columns, rows, columns, rows,
-        ),
-        in_specs=[VMEM, VMEM, SMEM],
-        out_specs=(HBM,) * 3 + (VMEM,) * 4,
-        scratch_shapes=[
-            pltpu.VMEM((chunks, C, 2 * C), BF16),
-            pltpu.VMEM((chunks, C, C), BF16),
-            pltpu.VMEM((chunks, C, 2 * C), BF16),
-            pltpu.VMEM((C, chunks), F32),
-            pltpu.VMEM((chunks, C), F32),
-            pltpu.SemaphoreType.DMA((3, chunks // GROUP)),
-        ],
-        compiler_params=pltpu.CompilerParams(vmem_limit_bytes=16 * 2**20),
-        cost_estimate=pl.CostEstimate(flops=4 * 10**9, bytes_accessed=2**21, transcendentals=0),
-        name="inverse",
-    )(near(blocks), added, decay_rate)
-
-
-def delta_kernel(
-    key_hbm, x_ref, base_hbm, weight_hbm, a_hbm, cum_col_ref, cum_row_ref, key_col_ref,
-    key_row_ref, out_ref, key_ref, base_ref, weight_ref, a_ref, b_ref, qe_ref, su_ref, sems,
+
+
+def delta_part(
+    x_ref, base_ref, weight_ref, a_ref, cum_col_ref, cum_row_ref, key_col_ref, key_row_ref,
+    out_ref, b_ref, qe_ref, su_ref,
 ):
     chunks = x_ref.shape[0]
-    pairs = (
-        (key_hbm, key_ref), (base_hbm, base_ref), (weight_hbm, weight_ref), (a_hbm, a_ref),
-    )
-    for g in range(chunks // GROUP):
-        for copy in group_copies(pairs, sems, g):
-            copy.start()
     row, column = iotas(C, C)
     inclusive = row >= column
 
     def prepare(g):
-        for copy in group_copies(pairs, sems, g):
-            copy.wait()
         ns = [g * GROUP + k for k in range(GROUP)]
-        keys = [key_ref[n, 0:C] for n in ns]
-        queries = [x_ref[n, 0:C] for n in ns]
-        values = [x_ref[n, C : 2 * C] for n in ns]
+        keys = [x_ref[n, 0:C] for n in ns]
+        queries = [x_ref[n, C : 2 * C] for n in ns]
+        values = [x_ref[n, 2 * C : 3 * C] for n in ns]
         scores = [dot_nt(q, k) for q, k in zip(queries, keys)]
         base = [dot(base_ref[n], above(v, v)) for n, v in zip(ns, values)]
         cum_c = [column_of(cum_col_ref, n) for n in ns]
@@ -311,27 +273,25 @@
     advance(chunks // GROUP - 1, state)
 
 
-def delta(keys, blocks, parts):
+def recurrence(blocks, added, decay_rate):
     chunks = blocks.shape[0]
+    square = pltpu.VMEM((chunks, C, C), F32)
+    wide = pltpu.VMEM((chunks, C, 2 * C), BF16)
+    columns = pltpu.VMEM((C, chunks), F32)
+    rows = pltpu.VMEM((chunks, C), F32)
     return pl.pallas_call(
-        delta_kernel,
+        recurrence_kernel,
         out_shape=jax.ShapeDtypeStruct((chunks, C, C), BF16),
-        in_specs=[HBM, VMEM, HBM, HBM, HBM] + [VMEM] * 4,
+        in_specs=[VMEM, VMEM, SMEM],
         out_specs=VMEM,
         scratch_shapes=[
-            pltpu.VMEM(keys.shape, BF16),
-            pltpu.VMEM((chunks, C, 2 * C), BF16),
-            pltpu.VMEM((chunks, C, C), BF16),
-            pltpu.VMEM((chunks, C, 2 * C), BF16),
-            pltpu.VMEM((chunks, C, C), F32),
-            pltpu.VMEM((chunks, C, 2 * C), BF16),
-            pltpu.VMEM((chunks, C, C), F32),
-            pltpu.SemaphoreType.DMA((4, chunks // GROUP)),
+            wide, pltpu.VMEM((chunks, C, C), BF16), wide, square, wide, square,
+            columns, rows, columns, rows, columns, rows,
         ],
-        compiler_params=pltpu.CompilerParams(vmem_limit_bytes=16 * 2**20),
-        cost_estimate=pl.CostEstimate(flops=4 * 10**9, bytes_accessed=2**21, transcendentals=0),
-        name="delta",
-    )(far(keys), near(blocks), *[far(p) for p in parts[:3]], *parts[3:])
+        compiler_params=pltpu.CompilerParams(vmem_limit_bytes=24 * 2**20),
+        cost_estimate=pl.CostEstimate(flops=8 * 10**9, bytes_accessed=2**21, transcendentals=0),
+        name="recurrence",
+    )(near(blocks), added, decay_rate)
 
 
 def slots_kernel(index_ref, dest_ref, source_ref, count_ref):
@@ -629,17 +589,15 @@
     tiles = features // C
     found, places = gathered(output_projection)
     dest, source = slots(token_expert_index[0].T.reshape(-1), experts, capacity)
-    keys, blocks = pack(
+    blocks = pack(
         query,
         key,
         value,
         write_strength_logit.transpose(0, 2, 1),
         decay_head_input.transpose(0, 2, 1),
     )
-    keys = lax.all_to_all(keys, "sp", split_axis=0, concat_axis=0, tiled=True)
     blocks = lax.all_to_all(blocks, "sp", split_axis=0, concat_axis=0, tiled=True)
-    parts = chunk_inverse(keys, added_log_decay.reshape(-1, C), head_decay_rate)
-    recurrent = delta(keys, blocks, parts)
+    recurrent = recurrence(blocks, added_log_decay.reshape(-1, C), head_decay_rate)
     recurrent, found = lax.optimization_barrier((recurrent, found))
     returned = lax.all_to_all(recurrent, "sp", split_axis=0, concat_axis=0, tiled=True)
     weights = list(found)

time: 216 us -> 202 us (0.935)
  blocking collectives: 113 us -> 93.7 us
  waiting for transfers between devices: 27.3 us -> 35.7 us
  Pallas kernels: 56.3 us -> 48.2 us
  starting transfers between devices: 17.3 us -> 22.1 us
    all_to_all x1 -> x0, blocking collectives: 19.5 us -> none  [layer(): keys = lax.all_to_all(keys, 'sp', split_axis=0, concat_axis=0, tiled=True)]
    all_to_all x1, waiting for transfers between devices: 0.01 us -> 17.6 us  [layer(): lax.all_to_all(blocks, 'sp', split_axis=0, concat_axis=0, tiled=True)]
    ppermute x3, waiting for transfers between devices: 22.8 us -> 13.6 us  [gathered(): found.append(lax.ppermute(block, 'dp_0', pairs))]
    pallas_call x3 -> x2, Pallas kernels: 23.5 us -> 15.4 us  [the longest x1 11.6 us: recurrence(): pl.pallas_call(recurrence_kernel, out_shape=jax.ShapeDtypeStruct((chunks,...]
    all_to_all x1, starting transfers between devices: 3.66 us -> 8.43 us  [layer(): lax.all_to_all(blocks, 'sp', split_axis=0, concat_axis=0, tiled=True)]
  transfers between devices with their start and end apart: 9 -> 9, of which waited for: 2 -> 3; matrix products, arithmetic and copies ran while one was open for 0% -> 0% of each run, Pallas kernels for 12% -> 9%
where the time goes in v3:
time: 202 us
  blocking collectives  93.7 us (46%)
  Pallas kernels  48.2 us (24%)
  waiting for transfers between devices  35.7 us (18%)
  starting transfers between devices  22.1 us (11%)
    all_to_all x1, blocking collectives, layer(): rows = lax.all_to_all(rows, SP_DP, split_axis=0, concat_axis=0, tiled=True)  48.1 us
    all_to_all x1, blocking collectives, layer(): back = lax.all_to_all(made, SP_DP, split_axis=0, concat_axis=0, tiled=True)  45.6 us
    all_to_all x1, waiting for transfers between devices, layer(): lax.all_to_all(blocks, 'sp', split_axis=0, concat_axis=0, tiled=True)  17.6 us
    pallas_call x1, Pallas kernels, expert(): pl.pallas_call(expert_kernel, out_shape=jax.ShapeDtypeStruct(rows.shape,...  15.1 us
    ppermute x3, waiting for transfers between devices, gathered(): found.append(lax.ppermute(block, 'dp_0', pairs))  13.6 us
    pallas_call x1, Pallas kernels, recurrence(): pl.pallas_call(recurrence_kernel, out_shape=jax.ShapeDtypeStruct((chunks,...  11.6 us
    all_to_all x1, starting transfers between devices, layer(): lax.all_to_all(blocks, 'sp', split_axis=0, concat_axis=0, tiled=True)  8.43 us
    pallas_call x1, Pallas kernels, project(): pl.pallas_call(project_kernel, out_shape=(jax.ShapeDtypeStruct((tokens, t...  7.39 us
  transfers between devices with their start and end apart: 9, of which 3 were waited for; matrix products, arithmetic and copies ran while one was open for 0% of the time, Pallas kernels for 9%

profile of v3, /device:TPU:1, one launch (start us, length us, event | category | flops | bytes accessed | tf_op | source)
XLA Modules:
  0.0 201.6 jit_solution(3167155412854126930)
XLA Ops:
  0.0 0.0 copy-start.6
  0.0 0.0 copy-start.5
  0.0 3.8 %pack.1 = bf16[16,400,128]{2,1,0:T(8,128)(2,1)} custom-call(bf16[1,128,2048]{2,1,0:T(8,128)(2,1)} %q_ref.1, bf16[1,128,2048]{2,1,0:T(8,128)(2,1)} %k_ref.1, bf16[1,128,2048]{2,1,0:T(8,128)(2,1)} %v_ref.1, bf16[1,16,128]{2,1,0:T(8,128)(2,1)} %bitcast.41, bf16[1,16,128]{2,1,0:T(8,128)(2,1)} %bitcast.42), custom_call_target="tpu_custom_call" | custom-call | tf_op jit(solution)/shard_map/pack/pallas_call | solution.py:82
  3.8 8.4 %all-to-all-start = ((bf16[16,400,128]{2,1,0:T(8,128)(2,1)}), bf16[16,400,128]{2,1,0:T(8,128)(2,1)S(1)}, u32[]{:S(2)}, u32[]{:S(2)}) async-start(bf16[16,400,128]{2,1,0:T(8,128)(2,1)} %pack.1), calls=%async_computation | async-start | bytes 3276800 | tf_op jit(solution)/shard_map/all_to_all | solution.py:599
  12.2 0.0 copy-done.6
  12.2 3.0 %collective-permute-start.1 = (bf16[2048,256]{1,0:T(8,128)(2,1)S(1)}, bf16[2048,256]{1,0:T(8,128)(2,1)}, u32[]{:S(2)}, u32[]{:S(2)}) collective-permute-start(bf16[2048,256]{1,0:T(8,128)(2,1)S(1)} %copy-done.6), channel_id=1, source_target_pairs={{0,4},{2,6},{4,0},{6,2},{1,5},{3,7},{5,1},{7,3},{8,12},{10,14},{12... | collective-permute-start | bytes 3145736 | tf_op jit(solution)/shard_map/ppermute | solution.py:559
  15.2 0.4 collective-permute-start
  15.6 2.3 %collective-permute-start.2 = (bf16[2048,256]{1,0:T(8,128)(2,1)S(1)}, bf16[2048,256]{1,0:T(8,128)(2,1)}, u32[]{:S(2)}, u32[]{:S(2)}) collective-permute-start(bf16[2048,256]{1,0:T(8,128)(2,1)S(1)} %copy-done.6), channel_id=1, source_target_pairs={{0,6},{2,0},{4,2},{6,4},{1,7},{3,1},{5,3},{7,5},{8,14},{10,8},{12,... | collective-permute-start | bytes 3145736 | tf_op jit(solution)/shard_map/ppermute | solution.py:559
  18.6 17.6 %all-to-all-done.x_ref = bf16[16,400,128]{2,1,0:T(8,128)(2,1)S(1)} async-done(((bf16[16,400,128]{2,1,0:T(8,128)(2,1)}), bf16[16,400,128]{2,1,0:T(8,128)(2,1)S(1)}, u32[]{:S(2)}, u32[]{:S(2)}) %all-to-all-start) | async-done | bytes 1638432 | tf_op jit(solution)/shard_map/all_to_all | solution.py:599
  36.2 0.0 copy-done.5
  36.2 0.0 copy-start.3
  36.2 0.0 copy-start.1
  36.2 0.0 copy-start.4
  36.2 11.6 %recurrence.1 = bf16[16,128,128]{2,1,0:T(8,128)(2,1)} custom-call(bf16[16,400,128]{2,1,0:T(8,128)(2,1)S(1)} %all-to-all-done.x_ref, f32[16,128]{1,0:T(8,128)S(1)} %bitcast.40, f32[1]{0:T(128)S(6)} %copy.19.rate_ref), custom_call_target="tpu_custom_call" | custom-call | flops 8000000000 | bytes 2097152 | tf_op jit(solution)/shard_map/recurrence/pallas_call | solution.py:282
  47.9 0.0 collective-permute-done.1.rest_2_
  47.9 13.6 %collective-permute-done.rest_1_ = bf16[2048,256]{1,0:T(8,128)(2,1)} collective-permute-done((bf16[2048,256]{1,0:T(8,128)(2,1)S(1)}, bf16[2048,256]{1,0:T(8,128)(2,1)}, u32[]{:S(2)}, u32[]{:S(2)}) %collective-permute-start) | collective-permute-done | bytes 1048608 | tf_op jit(solution)/shard_map/ppermute | solution.py:559
  61.5 0.0 collective-permute-done.2.rest_3_
  61.5 0.9 collective-permute-start.3
  62.3 0.0 collective-permute-start.4
  62.4 0.5 collective-permute-start.5
  62.9 0.0 collective-permute-start.6
  62.9 6.7 %all-to-all-start.1 = ((bf16[16,128,128]{2,1,0:T(8,128)(2,1)}), bf16[16,128,128]{2,1,0:T(8,128)(2,1)S(1)}, u32[]{:S(2)}, u32[]{:S(2)}) async-start(bf16[16,128,128]{2,1,0:T(8,128)(2,1)} %recurrence.1), calls=%async_computation.1 | async-start | bytes 1048576 | tf_op jit(solution)/shard_map/all_to_all | solution.py:602
  69.6 0.0 copy-done.3
  69.6 6.0 %slots.1 = (s32[512]{0:T(512)S(1)}, s32[768]{0:T(1024)S(1)}) custom-call(s32[512]{0:T(512)S(1)} %bitcast.38), custom_call_target="tpu_custom_call" | custom-call | tf_op jit(solution)/shard_map/slots/pallas_call | solution.py:326
  75.6 0.1 stack.35.place_ref
  75.7 4.4 %all-to-all-done.1.rec_ref = bf16[16,128,128]{2,1,0:T(8,128)(2,1)S(1)} async-done(((bf16[16,128,128]{2,1,0:T(8,128)(2,1)}), bf16[16,128,128]{2,1,0:T(8,128)(2,1)S(1)}, u32[]{:S(2)}, u32[]{:S(2)}) %all-to-all-start.1) | async-done | bytes 524320 | tf_op jit(solution)/shard_map/all_to_all | solution.py:602
  80.1 0.0 collective-permute-done.3.rest_4_
  80.1 0.0 copy-start.7
  80.1 0.0 collective-permute-done.4.rest_5_
  80.1 0.0 collective-permute-done.5.rest_6_
  80.1 0.0 collective-permute-done.6.rest_7_
  80.2 0.9 copy-done.7
  81.1 0.0 copy-done.1
  81.1 0.0 copy-done.4
  81.1 7.4 %project.1 = (bf16[128,16,128]{2,1,0:T(8,128)(2,1)S(1)}, bf16[768,16,128]{2,1,0:T(8,128)(2,1)S(1)}) custom-call(bf16[16,128,128]{2,1,0:T(8,128)(2,1)S(1)} %all-to-all-done.1.rec_ref, bf16[1,128,2048]{2,1,0:T(8,128)(2,1)} %gate_hbm.1, f32[1,128]{1,0:T(1,128)S(1)} %bitcast.39, bf16[1,128,2048]{2,1,0:T(8,128)(2,1)} %residual_hbm.1, f32[1,2048]{1,0:T(1,128)S(1)} %bitcast.36, ...), custom_call_target="tpu_custom_call" | custom-call | flops 1000000000 | bytes 16777216 | tf_op jit(solution)/shard_map/project/pallas_call | solution.py:393
  88.5 48.1 %all_to_all.20 = bf16[128,96,128]{2,1,0:T(8,128)(2,1)S(1)} all-to-all(bf16[128,96,128]{2,1,0:T(8,128)(2,1)S(1)} %bitcast.32), channel_id=1, replica_groups=mesh['sp'=16,'dp_0'=4,'dp_1'=2] {'sp','dp_0','dp_1'}, dimensions={0} | all-to-all | bytes 6291456 | tf_op jit(solution)/shard_map/all_to_all | solution.py:617
  136.6 15.1 %expert.1 = bf16[768,16,128]{2,1,0:T(8,128)(2,1)S(1)} custom-call(bf16[768,16,128]{2,1,0:T(8,128)(2,1)S(1)} %bitcast.33, bf16[2048,1024]{1,0:T(8,128)(2,1)} %bitcast.43, bf16[2048,1024]{1,0:T(8,128)(2,1)} %bitcast.44, bf16[1024,2048]{1,0:T(8,128)(2,1)} %bitcast.45), custom_call_target="tpu_custom_call" | custom-call | flops 10000000000 | bytes 16777216 | tf_op jit(solution)/shard_map/expert/pallas_call | solution.py:486
  151.6 0.0 copy-start
  151.7 0.0 copy-start.2
  151.7 45.6 %all_to_all.21 = bf16[128,96,128]{2,1,0:T(8,128)(2,1)S(1)} all-to-all(bf16[128,96,128]{2,1,0:T(8,128)(2,1)S(1)} %bitcast.34), channel_id=1, replica_groups=mesh['sp'=16,'dp_0'=4,'dp_1'=2] {'sp','dp_0','dp_1'}, dimensions={0} | all-to-all | bytes 6291456 | tf_op jit(solution)/shard_map/all_to_all | solution.py:625
  197.3 0.0 copy-done
  197.3 0.0 copy-done.2
  197.3 4.3 %combine.1 = f32[1,128,2048]{2,1,0:T(8,128)} custom-call(bf16[768,16,128]{2,1,0:T(8,128)(2,1)S(1)} %bitcast.31, bf16[128,16,128]{2,1,0:T(8,128)(2,1)S(1)} %get-tuple-element.21.normed_ref, f32[1,2048]{1,0:T(1,128)S(1)} %bitcast.35, s32[512]{0:T(512)S(1)} %get-tuple-element.22.dest_ref, f32[512]{0:T(512)S(1)} %bitcast.37), custom_call_target="tpu_custom_call" | custom-call | tf_op jit(solution)/shard_map/combine/pallas_call | solution.py:542
Async XLA Ops:
  0.0 12.2 %copy-start.6 = (bf16[2048,256]{1,0:T(8,128)(2,1)S(1)}, bf16[2048,256]{1,0:T(8,128)(2,1)}, u32[]{:S(2)}) copy-start(bf16[2048,256]{1,0:T(8,128)(2,1)} %rest_0_) | copy-start | bytes 3145732
  0.0 36.2 %copy-start.5 = (f32[1,1,2048]{2,1,0:T(1,128)S(1)}, f32[1,1,2048]{2,1,0:T(1,128)}, u32[]{:S(2)}) copy-start(f32[1,1,2048]{2,1,0:T(1,128)} %param.25) | copy-start | bytes 24580
  3.8 32.4 %all-to-all-start = ((bf16[16,400,128]{2,1,0:T(8,128)(2,1)}), bf16[16,400,128]{2,1,0:T(8,128)(2,1)S(1)}, u32[]{:S(2)}, u32[]{:S(2)}) async-start(bf16[16,400,128]{2,1,0:T(8,128)(2,1)} %pack.1), calls=%async_computation | async-start | bytes 3276800 | tf_op jit(solution)/shard_map/all_to_all | solution.py:599
  12.2 35.6 %collective-permute-start.1 = (bf16[2048,256]{1,0:T(8,128)(2,1)S(1)}, bf16[2048,256]{1,0:T(8,128)(2,1)}, u32[]{:S(2)}, u32[]{:S(2)}) collective-permute-start(bf16[2048,256]{1,0:T(8,128)(2,1)S(1)} %copy-done.6), channel_id=1, source_target_pairs={{0,4},{2,6},{4,0},{6,2},{1,5},{3,7},{5,1},{7,3},{8,12},{10,14},{12... | collective-permute-start | bytes 3145736 | tf_op jit(solution)/shard_map/ppermute | solution.py:559
  15.2 46.2 %collective-permute-start = (bf16[2048,256]{1,0:T(8,128)(2,1)S(1)}, bf16[2048,256]{1,0:T(8,128)(2,1)}, u32[]{:S(2)}, u32[]{:S(2)}) collective-permute-start(bf16[2048,256]{1,0:T(8,128)(2,1)S(1)} %copy-done.6), channel_id=1, source_target_pairs={{0,2},{2,4},{4,6},{6,0},{1,3},{3,5},{5,7},{7,1},{8,10},{10,12},{12... | collective-permute-start | bytes 3145736 | tf_op jit(solution)/shard_map/ppermute | solution.py:559
  15.6 45.9 %collective-permute-start.2 = (bf16[2048,256]{1,0:T(8,128)(2,1)S(1)}, bf16[2048,256]{1,0:T(8,128)(2,1)}, u32[]{:S(2)}, u32[]{:S(2)}) collective-permute-start(bf16[2048,256]{1,0:T(8,128)(2,1)S(1)} %copy-done.6), channel_id=1, source_target_pairs={{0,6},{2,0},{4,2},{6,4},{1,7},{3,1},{5,3},{7,5},{8,14},{10,8},{12,... | collective-permute-start | bytes 3145736 | tf_op jit(solution)/shard_map/ppermute | solution.py:559
  36.2 33.4 %copy-start.3 = (s32[1,128,4]{1,2,0:T(4,128)S(1)}, s32[1,128,4]{1,2,0:T(4,128)}, u32[]{:S(2)}) copy-start(s32[1,128,4]{1,2,0:T(4,128)} %param.30) | copy-start | bytes 6148
  36.2 44.9 %copy-start.1 = (f32[2048]{0:T(1024)S(1)}, f32[2048]{0:T(1024)}, u32[]{:S(2)}) copy-start(f32[2048]{0:T(1024)} %param.29) | copy-start | bytes 24580
  36.2 44.9 %copy-start.4 = (f32[128]{0:T(128)S(1)}, f32[128]{0:T(128)}, u32[]{:S(2)}) copy-start(f32[128]{0:T(128)} %param.27) | copy-start | bytes 1540
  61.5 18.6 %collective-permute-start.3 = (bf16[2048,256]{1,0:T(8,128)(2,1)S(1)}, bf16[2048,256]{1,0:T(8,128)(2,1)S(1)}, u32[]{:S(2)}, u32[]{:S(2)}) collective-permute-start(bf16[2048,256]{1,0:T(8,128)(2,1)S(1)} %copy-done.6), channel_id=1, source_target_pairs={{0,1},{1,0},{2,3},{3,2},{4,5},{5,4},{6,7},{7,6},{8,9},{9,8},{10,11... | collective-permute-start | bytes 3145736 | tf_op jit(solution)/shard_map/ppermute | solution.py:605
  62.3 17.8 %collective-permute-start.4 = (bf16[2048,256]{1,0:T(8,128)(2,1)}, bf16[2048,256]{1,0:T(8,128)(2,1)}, u32[]{:S(2)}, u32[]{:S(2)}) collective-permute-start(bf16[2048,256]{1,0:T(8,128)(2,1)} %collective-permute-done.rest_1_), channel_id=1, source_target_pairs={{0,1},{1,0},{2,3},{3,2},{4,5},{5,4},{6,7},{7,6},{8,9},{9,8},{10,11... | collective-permute-start | bytes 3145736 | tf_op jit(solution)/shard_map/ppermute | solution.py:605
  62.4 17.8 %collective-permute-start.5 = (bf16[2048,256]{1,0:T(8,128)(2,1)}, bf16[2048,256]{1,0:T(8,128)(2,1)}, u32[]{:S(2)}, u32[]{:S(2)}) collective-permute-start(bf16[2048,256]{1,0:T(8,128)(2,1)} %collective-permute-done.1.rest_2_), channel_id=1, source_target_pairs={{0,1},{1,0},{2,3},{3,2},{4,5},{5,4},{6,7},{7,6},{8,9},{9,8},{10,11... | collective-permute-start | bytes 3145736 | tf_op jit(solution)/shard_map/ppermute | solution.py:605
  62.9 17.3 %collective-permute-start.6 = (bf16[2048,256]{1,0:T(8,128)(2,1)}, bf16[2048,256]{1,0:T(8,128)(2,1)}, u32[]{:S(2)}, u32[]{:S(2)}) collective-permute-start(bf16[2048,256]{1,0:T(8,128)(2,1)} %collective-permute-done.2.rest_3_), channel_id=1, source_target_pairs={{0,1},{1,0},{2,3},{3,2},{4,5},{5,4},{6,7},{7,6},{8,9},{9,8},{10,11... | collective-permute-start | bytes 3145736 | tf_op jit(solution)/shard_map/ppermute | solution.py:605
  62.9 17.3 %all-to-all-start.1 = ((bf16[16,128,128]{2,1,0:T(8,128)(2,1)}), bf16[16,128,128]{2,1,0:T(8,128)(2,1)S(1)}, u32[]{:S(2)}, u32[]{:S(2)}) async-start(bf16[16,128,128]{2,1,0:T(8,128)(2,1)} %recurrence.1), calls=%async_computation.1 | async-start | bytes 1048576 | tf_op jit(solution)/shard_map/all_to_all | solution.py:602
  80.1 1.0 copy-start.7
  151.6 45.7 %copy-start = (f32[2048]{0:T(1024)S(1)}, f32[2048]{0:T(1024)}, u32[]{:S(2)}) copy-start(f32[2048]{0:T(1024)} %param.35) | copy-start | bytes 24580
  151.7 45.6 %copy-start.2 = (f32[1,128,4]{1,2,0:T(4,128)S(1)}, f32[1,128,4]{1,2,0:T(4,128)}, u32[]{:S(2)}) copy-start(f32[1,128,4]{1,2,0:T(4,128)} %param.31) | copy-start | bytes 6148

commit v4 on v3

--- a/solution.py
+++ b/solution.py
@@ -54,7 +54,7 @@
     return jnp.where((row % 16) * 16 + row // 16 == column, 1.0, 0.0).astype(BF16)
 
 
-def pack_kernel(q_ref, k_ref, v_ref, logit_ref, decay_ref, out_ref, sems):
+def pack_kernel(q_ref, k_ref, v_ref, logit_ref, decay_ref, out_hbm, out_ref, sems, out_sems):
     heads = out_ref.shape[0]
     copies = []
     for h in range(heads):
@@ -73,7 +73,13 @@
     for h in range(heads):
         extra = jnp.where(extra_row == 0, logits[h : h + 1], decays[h : h + 1])
         out_ref[h, 3 * C : 3 * C + EXTRA] = extra.astype(BF16)
-    for copy in copies:
+    sent = []
+    for h in range(heads):
+        for copy in copies[3 * h : 3 * h + 3]:
+            copy.wait()
+        sent.append(pltpu.make_async_copy(out_ref.at[h], out_hbm.at[h], out_sems.at[h]))
+        sent[h].start()
+    for copy in sent:
         copy.wait()
 
 
@@ -81,16 +87,21 @@
     heads = logit.shape[1]
     return pl.pallas_call(
         pack_kernel,
-        out_shape=jax.ShapeDtypeStruct((heads, 3 * C + EXTRA, C), BF16),
+        out_shape=pltpu.HBM((heads, 3 * C + EXTRA, C), BF16),
         in_specs=[HBM] * 3 + [VMEM] * 2,
-        out_specs=VMEM,
-        scratch_shapes=[pltpu.SemaphoreType.DMA((3 * heads,))],
+        out_specs=HBM,
+        scratch_shapes=[
+            pltpu.VMEM((heads, 3 * C + EXTRA, C), BF16),
+            pltpu.SemaphoreType.DMA((3 * heads,)),
+            pltpu.SemaphoreType.DMA((heads,)),
+        ],
         compiler_params=pltpu.CompilerParams(vmem_limit_bytes=12 * 2**20),
         name="pack",
     )(far(query), far(key), far(value), far(logit), far(decay_input))
 
 
 GROUP = 8
+WIDE_GROUP = 16
 
 
 def column_of(ref, n):
@@ -150,7 +161,7 @@
     lane = lax.broadcasted_iota(jnp.int32, (C, chunks), 1)
 
     def group(g, key_columns):
-        ns = [g * GROUP + k for k in range(GROUP)]
+        ns = [g * WIDE_GROUP + k for k in range(WIDE_GROUP)]
         keys = [x_ref[n, 0:C] for n in ns]
         products = [dot_nt(k, k) for k in keys]
         cum_c = [column_of(cum_col_ref, n) for n in ns]
@@ -206,7 +217,7 @@
         return key_columns
 
     key_col_ref[...] = lax.fori_loop(
-        0, chunks // GROUP, group, jnp.zeros((C, chunks), F32)
+        0, chunks // WIDE_GROUP, group, jnp.zeros((C, chunks), F32)
     )
 
 
@@ -502,12 +513,18 @@
     )(near(rows), far(gate_weight), far(up_weight), far(down_weight))
 
 
-def combine_kernel(back_ref, normed_ref, gain_ref, dest_ref, weight_ref, out_ref, z_ref):
+def combine_kernel(
+    back_ref, normed_ref, gain_ref, dest_ref, weight_ref, out_hbm, z_ref, out_ref, sems
+):
     tokens, tiles, _ = normed_ref.shape
     swap = swap_matrix()
     gain = gain_ref[...]
 
-    def some(i, carry):
+    def copy_of(i):
+        part = pl.ds(pl.multiple_of(i * 16, 16), 16)
+        return pltpu.make_async_copy(out_ref.at[part], out_hbm.at[0, part], sems.at[i])
+
+    def add(i):
         for k in range(16):
             t = i * 16 + k
             total = normed_ref[t].astype(F32)
@@ -515,11 +532,8 @@
                 at = pick * tokens + t
                 total = total + weight_ref[at] * back_ref[dest_ref[at]].astype(F32)
             z_ref[t] = total
-        return carry
-
-    lax.fori_loop(0, tokens // 16, some, 0)
-
-    def finish(i, carry):
+
+    def finish(i):
         start = pl.multiple_of(i * 16, 16)
         z = z_ref[pl.ds(start, 16)].reshape(16 * tiles, C)
         high = z.astype(BF16)
@@ -531,20 +545,35 @@
         total = jnp.concatenate([turned[j * 16 : (j + 1) * 16] for j in range(tiles)], axis=1)
         centred = total - jnp.mean(total, axis=1, keepdims=True)
         variance = jnp.mean(centred * centred, axis=1, keepdims=True)
-        out_ref[0, pl.ds(start, 16), :] = centred * lax.rsqrt(variance + 1e-05) * gain
+        out_ref[pl.ds(start, 16), :] = centred * lax.rsqrt(variance + 1e-05) * gain
+        copy_of(i).start()
+
+    add(0)
+
+    def step(i, carry):
+        finish(i - 1)
+        add(i)
         return carry
 
-    lax.fori_loop(0, tokens // 16, finish, 0, unroll=2)
+    groups = tokens // 16
+    lax.fori_loop(1, groups, step, 0)
+    finish(groups - 1)
+    for i in range(groups):
+        copy_of(i).wait()
 
 
 def combine(back, normed, gain, dest, weight):
     tokens, tiles, _ = normed.shape
     return pl.pallas_call(
         combine_kernel,
-        out_shape=jax.ShapeDtypeStruct((1, tokens, tiles * C), F32),
+        out_shape=pltpu.HBM((1, tokens, tiles * C), F32),
         in_specs=[VMEM] * 3 + [SMEM] * 2,
-        out_specs=VMEM,
-        scratch_shapes=[pltpu.VMEM((tokens, tiles, C), F32)],
+        out_specs=HBM,
+        scratch_shapes=[
+            pltpu.VMEM((tokens, tiles, C), F32),
+            pltpu.VMEM((tokens, tiles * C), F32),
+            pltpu.SemaphoreType.DMA((tokens // 16,)),
+        ],
         compiler_params=pltpu.CompilerParams(vmem_limit_bytes=12 * 2**20),
         name="combine",
     )(near(back), near(normed), gain, dest, weight)
@@ -598,7 +627,6 @@
     )
     blocks = lax.all_to_all(blocks, "sp", split_axis=0, concat_axis=0, tiled=True)
     recurrent = recurrence(blocks, added_log_decay.reshape(-1, C), head_decay_rate)
-    recurrent, found = lax.optimization_barrier((recurrent, found))
     returned = lax.all_to_all(recurrent, "sp", split_axis=0, concat_axis=0, tiled=True)
     weights = list(found)
     for b in found:

time: 202 us -> 213 us (1.054)
  starting transfers between devices: 22.1 us -> 44.5 us
  waiting for transfers between devices: 35.7 us -> 27.3 us
    ppermute x4, starting transfers between devices: 1.39 us -> 25.5 us  [layer(): weights.append(lax.ppermute(b, 'dp_1', [(0, 1), (1, 0)]))]
    all_to_all x1, waiting for transfers between devices: 17.6 us -> 0.01 us  [layer(): lax.all_to_all(blocks, 'sp', split_axis=0, concat_axis=0, tiled=True)]
    ppermute x3, waiting for transfers between devices: 13.6 us -> 22.4 us  [gathered(): found.append(lax.ppermute(block, 'dp_0', pairs))]
  transfers between devices with their start and end apart: 9 -> 9, of which waited for: 3 -> 3; matrix products, arithmetic and copies ran while one was open for 0% -> 0% of each run, Pallas kernels for 9% -> 8%
where the time goes in v4:
time: 213 us; the launch traced here: 212 us
  blocking collectives  91.7 us (43%)
  Pallas kernels  47.7 us (22%)
  starting transfers between devices  44.5 us (21%)
  waiting for transfers between devices  27.3 us (13%)
    all_to_all x1, blocking collectives, layer(): rows = lax.all_to_all(rows, SP_DP, split_axis=0, concat_axis=0, tiled=True)  46.1 us
    all_to_all x1, blocking collectives, layer(): back = lax.all_to_all(made, SP_DP, split_axis=0, concat_axis=0, tiled=True)  45.6 us
    ppermute x4, starting transfers between devices, layer(): weights.append(lax.ppermute(b, 'dp_1', [(0, 1), (1, 0)]))  25.5 us
    ppermute x3, waiting for transfers between devices, gathered(): found.append(lax.ppermute(block, 'dp_0', pairs))  22.4 us
    pallas_call x1, Pallas kernels, expert(): pl.pallas_call(expert_kernel, out_shape=jax.ShapeDtypeStruct(rows.shape,...  15.1 us
    pallas_call x1, Pallas kernels, recurrence(): pl.pallas_call(recurrence_kernel, out_shape=jax.ShapeDtypeStruct((chunks,...  10.6 us
    all_to_all x1, starting transfers between devices, layer(): lax.all_to_all(blocks, 'sp', split_axis=0, concat_axis=0, tiled=True)  8.43 us
    pallas_call x1, Pallas kernels, project(): pl.pallas_call(project_kernel, out_shape=(jax.ShapeDtypeStruct((tokens, t...  7.4 us
  transfers between devices with their start and end apart: 9, of which 3 were waited for; matrix products, arithmetic and copies ran while one was open for 0% of the time, Pallas kernels for 8%

profile of v4, /device:TPU:1, one launch (start us, length us, event | category | flops | bytes accessed | tf_op | source)
XLA Modules:
  0.0 212.3 jit_solution(14000905872134536730)
XLA Ops:
  0.0 0.0 copy-start.6
  0.0 0.0 copy-start.5
  0.0 3.4 %pack.1 = bf16[16,400,128]{2,1,0:T(8,128)(2,1)} custom-call(bf16[1,128,2048]{2,1,0:T(8,128)(2,1)} %q_ref.1, bf16[1,128,2048]{2,1,0:T(8,128)(2,1)} %k_ref.1, bf16[1,128,2048]{2,1,0:T(8,128)(2,1)} %v_ref.1, bf16[1,16,128]{2,1,0:T(8,128)(2,1)} %bitcast.41, bf16[1,16,128]{2,1,0:T(8,128)(2,1)} %bitcast.42), custom_call_target="tpu_custom_call" | custom-call | tf_op jit(solution)/shard_map/pack/pallas_call | solution.py:88
  3.4 8.4 %all-to-all-start = ((bf16[16,400,128]{2,1,0:T(8,128)(2,1)}), bf16[16,400,128]{2,1,0:T(8,128)(2,1)S(1)}, u32[]{:S(2)}, u32[]{:S(2)}) async-start(bf16[16,400,128]{2,1,0:T(8,128)(2,1)} %pack.1), calls=%async_computation | async-start | bytes 3276800 | tf_op jit(solution)/shard_map/all_to_all | solution.py:628
  11.9 0.0 copy-done.6
  11.9 2.8 %collective-permute-start.2 = (bf16[2048,256]{1,0:T(8,128)(2,1)S(1)}, bf16[2048,256]{1,0:T(8,128)(2,1)}, u32[]{:S(2)}, u32[]{:S(2)}) collective-permute-start(bf16[2048,256]{1,0:T(8,128)(2,1)S(1)} %copy-done.6), channel_id=1, source_target_pairs={{0,6},{2,0},{4,2},{6,4},{1,7},{3,1},{5,3},{7,5},{8,14},{10,8},{12,... | collective-permute-start | bytes 3145736 | tf_op jit(solution)/shard_map/ppermute | solution.py:588
  14.7 0.3 collective-permute-start.1
  15.0 0.7 collective-permute-start
  15.7 1.8 collective-permute-start.3
  18.2 19.1 %collective-permute-done.2.rest_3_ = bf16[2048,256]{1,0:T(8,128)(2,1)} collective-permute-done((bf16[2048,256]{1,0:T(8,128)(2,1)S(1)}, bf16[2048,256]{1,0:T(8,128)(2,1)}, u32[]{:S(2)}, u32[]{:S(2)}) %collective-permute-start.2) | collective-permute-done | bytes 1048608 | tf_op jit(solution)/shard_map/ppermute | solution.py:588
  37.3 23.2 %collective-permute-start.6 = (bf16[2048,256]{1,0:T(8,128)(2,1)}, bf16[2048,256]{1,0:T(8,128)(2,1)}, u32[]{:S(2)}, u32[]{:S(2)}) collective-permute-start(bf16[2048,256]{1,0:T(8,128)(2,1)} %collective-permute-done.2.rest_3_), channel_id=1, source_target_pairs={{0,1},{1,0},{2,3},{3,2},{4,5},{5,4},{6,7},{7,6},{8,9},{9,8},{10,11... | collective-permute-start | bytes 3145736 | tf_op jit(solution)/shard_map/ppermute | solution.py:633
  60.5 0.0 collective-permute-done.1.rest_2_
  60.5 0.0 collective-permute-start.5
  60.5 3.3 %collective-permute-done.rest_1_ = bf16[2048,256]{1,0:T(8,128)(2,1)} collective-permute-done((bf16[2048,256]{1,0:T(8,128)(2,1)S(1)}, bf16[2048,256]{1,0:T(8,128)(2,1)}, u32[]{:S(2)}, u32[]{:S(2)}) %collective-permute-start) | collective-permute-done | bytes 1048608 | tf_op jit(solution)/shard_map/ppermute | solution.py:588
  63.9 0.5 collective-permute-start.4
  64.3 0.0 all-to-all-done.x_ref
  64.3 0.0 copy-done.5
  64.4 0.0 copy-start.3
  64.4 0.0 copy-start.1
  64.4 0.0 copy-start.4
  64.4 10.6 %recurrence.1 = bf16[16,128,128]{2,1,0:T(8,128)(2,1)} custom-call(bf16[16,400,128]{2,1,0:T(8,128)(2,1)S(1)} %all-to-all-done.x_ref, f32[16,128]{1,0:T(8,128)S(1)} %bitcast.40, f32[1]{0:T(128)S(6)} %copy.19.rate_ref), custom_call_target="tpu_custom_call" | custom-call | flops 8000000000 | bytes 2097152 | tf_op jit(solution)/shard_map/recurrence/pallas_call | solution.py:293
  74.9 6.7 %all-to-all-start.1 = ((bf16[16,128,128]{2,1,0:T(8,128)(2,1)}), bf16[16,128,128]{2,1,0:T(8,128)(2,1)S(1)}, u32[]{:S(2)}, u32[]{:S(2)}) async-start(bf16[16,128,128]{2,1,0:T(8,128)(2,1)} %recurrence.1), calls=%async_computation.1 | async-start | bytes 1048576 | tf_op jit(solution)/shard_map/all_to_all | solution.py:630
  81.7 0.0 copy-done.3
  81.7 6.0 %slots.1 = (s32[512]{0:T(512)S(1)}, s32[768]{0:T(1024)S(1)}) custom-call(s32[512]{0:T(512)S(1)} %bitcast.38), custom_call_target="tpu_custom_call" | custom-call | tf_op jit(solution)/shard_map/slots/pallas_call | solution.py:337
  87.7 0.1 stack.35.place_ref
  87.8 0.0 collective-permute-done.3.rest_4_
  87.8 4.8 %all-to-all-done.1.rec_ref = bf16[16,128,128]{2,1,0:T(8,128)(2,1)S(1)} async-done(((bf16[16,128,128]{2,1,0:T(8,128)(2,1)}), bf16[16,128,128]{2,1,0:T(8,128)(2,1)S(1)}, u32[]{:S(2)}, u32[]{:S(2)}) %all-to-all-start.1) | async-done | bytes 524320 | tf_op jit(solution)/shard_map/all_to_all | solution.py:630
  92.6 0.0 collective-permute-done.6.rest_7_
  92.6 0.0 collective-permute-done.5.rest_6_
  92.6 0.0 collective-permute-done.4.rest_5_
  92.6 0.0 copy-done.1
  92.6 0.0 copy-done.4
  92.7 7.4 %project.1 = (bf16[128,16,128]{2,1,0:T(8,128)(2,1)S(1)}, bf16[768,16,128]{2,1,0:T(8,128)(2,1)S(1)}) custom-call(bf16[16,128,128]{2,1,0:T(8,128)(2,1)S(1)} %all-to-all-done.1.rec_ref, bf16[1,128,2048]{2,1,0:T(8,128)(2,1)} %gate_hbm.1, f32[1,128]{1,0:T(1,128)S(1)} %bitcast.39, bf16[1,128,2048]{2,1,0:T(8,128)(2,1)} %residual_hbm.1, f32[1,2048]{1,0:T(1,128)S(1)} %bitcast.36, ...), custom_call_target="tpu_custom_call" | custom-call | flops 1000000000 | bytes 16777216 | tf_op jit(solution)/shard_map/project/pallas_call | solution.py:404
  100.1 46.1 %all_to_all.20 = bf16[128,96,128]{2,1,0:T(8,128)(2,1)S(1)} all-to-all(bf16[128,96,128]{2,1,0:T(8,128)(2,1)S(1)} %bitcast.32), channel_id=1, replica_groups=mesh['sp'=16,'dp_0'=4,'dp_1'=2] {'sp','dp_0','dp_1'}, dimensions={0} | all-to-all | bytes 6291456 | tf_op jit(solution)/shard_map/all_to_all | solution.py:645
  146.1 15.1 %expert.1 = bf16[768,16,128]{2,1,0:T(8,128)(2,1)S(1)} custom-call(bf16[768,16,128]{2,1,0:T(8,128)(2,1)S(1)} %bitcast.33, bf16[2048,1024]{1,0:T(8,128)(2,1)} %bitcast.43, bf16[2048,1024]{1,0:T(8,128)(2,1)} %bitcast.44, bf16[1024,2048]{1,0:T(8,128)(2,1)} %bitcast.45), custom_call_target="tpu_custom_call" | custom-call | flops 10000000000 | bytes 16777216 | tf_op jit(solution)/shard_map/expert/pallas_call | solution.py:497
  161.2 0.0 copy-start
  161.3 0.0 copy-start.2
  161.3 45.6 %all_to_all.21 = bf16[128,96,128]{2,1,0:T(8,128)(2,1)S(1)} all-to-all(bf16[128,96,128]{2,1,0:T(8,128)(2,1)S(1)} %bitcast.34), channel_id=1, replica_groups=mesh['sp'=16,'dp_0'=4,'dp_1'=2] {'sp','dp_0','dp_1'}, dimensions={0} | all-to-all | bytes 6291456 | tf_op jit(solution)/shard_map/all_to_all | solution.py:653
  206.9 0.0 copy-done
  206.9 0.0 copy-done.2
  206.9 5.2 %combine.1 = f32[1,128,2048]{2,1,0:T(8,128)} custom-call(bf16[768,16,128]{2,1,0:T(8,128)(2,1)S(1)} %bitcast.31, bf16[128,16,128]{2,1,0:T(8,128)(2,1)S(1)} %get-tuple-element.11.normed_ref, f32[1,2048]{1,0:T(1,128)S(1)} %bitcast.35, s32[512]{0:T(512)S(1)} %get-tuple-element.12.dest_ref, f32[512]{0:T(512)S(1)} %bitcast.37), custom_call_target="tpu_custom_call" | custom-call | tf_op jit(solution)/shard_map/combine/pallas_call | solution.py:567
Async XLA Ops:
  0.0 11.9 %copy-start.6 = (bf16[2048,256]{1,0:T(8,128)(2,1)S(1)}, bf16[2048,256]{1,0:T(8,128)(2,1)}, u32[]{:S(2)}) copy-start(bf16[2048,256]{1,0:T(8,128)(2,1)} %rest_0_.1) | copy-start | bytes 3145732
  0.0 64.3 %copy-start.5 = (f32[1,1,2048]{2,1,0:T(1,128)S(1)}, f32[1,1,2048]{2,1,0:T(1,128)}, u32[]{:S(2)}) copy-start(f32[1,1,2048]{2,1,0:T(1,128)} %param.25) | copy-start | bytes 24580
  3.4 60.9 %all-to-all-start = ((bf16[16,400,128]{2,1,0:T(8,128)(2,1)}), bf16[16,400,128]{2,1,0:T(8,128)(2,1)S(1)}, u32[]{:S(2)}, u32[]{:S(2)}) async-start(bf16[16,400,128]{2,1,0:T(8,128)(2,1)} %pack.1), calls=%async_computation | async-start | bytes 3276800 | tf_op jit(solution)/shard_map/all_to_all | solution.py:628
  11.9 25.4 %collective-permute-start.2 = (bf16[2048,256]{1,0:T(8,128)(2,1)S(1)}, bf16[2048,256]{1,0:T(8,128)(2,1)}, u32[]{:S(2)}, u32[]{:S(2)}) collective-permute-start(bf16[2048,256]{1,0:T(8,128)(2,1)S(1)} %copy-done.6), channel_id=1, source_target_pairs={{0,6},{2,0},{4,2},{6,4},{1,7},{3,1},{5,3},{7,5},{8,14},{10,8},{12,... | collective-permute-start | bytes 3145736 | tf_op jit(solution)/shard_map/ppermute | solution.py:588
  14.7 45.8 %collective-permute-start.1 = (bf16[2048,256]{1,0:T(8,128)(2,1)S(1)}, bf16[2048,256]{1,0:T(8,128)(2,1)}, u32[]{:S(2)}, u32[]{:S(2)}) collective-permute-start(bf16[2048,256]{1,0:T(8,128)(2,1)S(1)} %copy-done.6), channel_id=1, source_target_pairs={{0,4},{2,6},{4,0},{6,2},{1,5},{3,7},{5,1},{7,3},{8,12},{10,14},{12... | collective-permute-start | bytes 3145736 | tf_op jit(solution)/shard_map/ppermute | solution.py:588
  15.0 48.8 %collective-permute-start = (bf16[2048,256]{1,0:T(8,128)(2,1)S(1)}, bf16[2048,256]{1,0:T(8,128)(2,1)}, u32[]{:S(2)}, u32[]{:S(2)}) collective-permute-start(bf16[2048,256]{1,0:T(8,128)(2,1)S(1)} %copy-done.6), channel_id=1, source_target_pairs={{0,2},{2,4},{4,6},{6,0},{1,3},{3,5},{5,7},{7,1},{8,10},{10,12},{12... | collective-permute-start | bytes 3145736 | tf_op jit(solution)/shard_map/ppermute | solution.py:588
  15.7 72.1 %collective-permute-start.3 = (bf16[2048,256]{1,0:T(8,128)(2,1)S(1)}, bf16[2048,256]{1,0:T(8,128)(2,1)}, u32[]{:S(2)}, u32[]{:S(2)}) collective-permute-start(bf16[2048,256]{1,0:T(8,128)(2,1)S(1)} %copy-done.6), channel_id=1, source_target_pairs={{0,1},{1,0},{2,3},{3,2},{4,5},{5,4},{6,7},{7,6},{8,9},{9,8},{10,11... | collective-permute-start | bytes 3145736 | tf_op jit(solution)/shard_map/ppermute | solution.py:633
  37.3 55.3 %collective-permute-start.6 = (bf16[2048,256]{1,0:T(8,128)(2,1)}, bf16[2048,256]{1,0:T(8,128)(2,1)}, u32[]{:S(2)}, u32[]{:S(2)}) collective-permute-start(bf16[2048,256]{1,0:T(8,128)(2,1)} %collective-permute-done.2.rest_3_), channel_id=1, source_target_pairs={{0,1},{1,0},{2,3},{3,2},{4,5},{5,4},{6,7},{7,6},{8,9},{9,8},{10,11... | collective-permute-start | bytes 3145736 | tf_op jit(solution)/shard_map/ppermute | solution.py:633
  60.5 32.1 %collective-permute-start.5 = (bf16[2048,256]{1,0:T(8,128)(2,1)}, bf16[2048,256]{1,0:T(8,128)(2,1)}, u32[]{:S(2)}, u32[]{:S(2)}) collective-permute-start(bf16[2048,256]{1,0:T(8,128)(2,1)} %collective-permute-done.1.rest_2_), channel_id=1, source_target_pairs={{0,1},{1,0},{2,3},{3,2},{4,5},{5,4},{6,7},{7,6},{8,9},{9,8},{10,11... | collective-permute-start | bytes 3145736 | tf_op jit(solution)/shard_map/ppermute | solution.py:633
  63.9 28.8 %collective-permute-start.4 = (bf16[2048,256]{1,0:T(8,128)(2,1)}, bf16[2048,256]{1,0:T(8,128)(2,1)}, u32[]{:S(2)}, u32[]{:S(2)}) collective-permute-start(bf16[2048,256]{1,0:T(8,128)(2,1)} %collective-permute-done.rest_1_), channel_id=1, source_target_pairs={{0,1},{1,0},{2,3},{3,2},{4,5},{5,4},{6,7},{7,6},{8,9},{9,8},{10,11... | collective-permute-start | bytes 3145736 | tf_op jit(solution)/shard_map/ppermute | solution.py:633
  64.4 17.3 %copy-start.3 = (s32[1,128,4]{1,2,0:T(4,128)S(1)}, s32[1,128,4]{1,2,0:T(4,128)}, u32[]{:S(2)}) copy-start(s32[1,128,4]{1,2,0:T(4,128)} %param.30) | copy-start | bytes 6148
  64.4 28.3 %copy-start.1 = (f32[2048]{0:T(1024)S(1)}, f32[2048]{0:T(1024)}, u32[]{:S(2)}) copy-start(f32[2048]{0:T(1024)} %param.29) | copy-start | bytes 24580
  64.4 28.3 %copy-start.4 = (f32[128]{0:T(128)S(1)}, f32[128]{0:T(128)}, u32[]{:S(2)}) copy-start(f32[128]{0:T(128)} %param.27) | copy-start | bytes 1540
  74.9 17.7 %all-to-all-start.1 = ((bf16[16,128,128]{2,1,0:T(8,128)(2,1)}), bf16[16,128,128]{2,1,0:T(8,128)(2,1)S(1)}, u32[]{:S(2)}, u32[]{:S(2)}) async-start(bf16[16,128,128]{2,1,0:T(8,128)(2,1)} %recurrence.1), calls=%async_computation.1 | async-start | bytes 1048576 | tf_op jit(solution)/shard_map/all_to_all | solution.py:630
  161.2 45.7 %copy-start = (f32[2048]{0:T(1024)S(1)}, f32[2048]{0:T(1024)}, u32[]{:S(2)}) copy-start(f32[2048]{0:T(1024)} %param.35) | copy-start | bytes 24580
  161.3 45.6 %copy-start.2 = (f32[1,128,4]{1,2,0:T(4,128)S(1)}, f32[1,128,4]{1,2,0:T(4,128)}, u32[]{:S(2)}) copy-start(f32[1,128,4]{1,2,0:T(4,128)} %param.31) | copy-start | bytes 6148

commit v5 on v3

--- a/solution.py
+++ b/solution.py
@@ -54,7 +54,7 @@
     return jnp.where((row % 16) * 16 + row // 16 == column, 1.0, 0.0).astype(BF16)
 
 
-def pack_kernel(q_ref, k_ref, v_ref, logit_ref, decay_ref, out_ref, sems):
+def pack_kernel(q_ref, k_ref, v_ref, logit_ref, decay_ref, out_hbm, out_ref, sems, out_sems):
     heads = out_ref.shape[0]
     copies = []
     for h in range(heads):
@@ -73,7 +73,13 @@
     for h in range(heads):
         extra = jnp.where(extra_row == 0, logits[h : h + 1], decays[h : h + 1])
         out_ref[h, 3 * C : 3 * C + EXTRA] = extra.astype(BF16)
-    for copy in copies:
+    sent = []
+    for h in range(heads):
+        for copy in copies[3 * h : 3 * h + 3]:
+            copy.wait()
+        sent.append(pltpu.make_async_copy(out_ref.at[h], out_hbm.at[h], out_sems.at[h]))
+        sent[h].start()
+    for copy in sent:
         copy.wait()
 
 
@@ -81,16 +87,21 @@
     heads = logit.shape[1]
     return pl.pallas_call(
         pack_kernel,
-        out_shape=jax.ShapeDtypeStruct((heads, 3 * C + EXTRA, C), BF16),
+        out_shape=pltpu.HBM((heads, 3 * C + EXTRA, C), BF16),
         in_specs=[HBM] * 3 + [VMEM] * 2,
-        out_specs=VMEM,
-        scratch_shapes=[pltpu.SemaphoreType.DMA((3 * heads,))],
+        out_specs=HBM,
+        scratch_shapes=[
+            pltpu.VMEM((heads, 3 * C + EXTRA, C), BF16),
+            pltpu.SemaphoreType.DMA((3 * heads,)),
+            pltpu.SemaphoreType.DMA((heads,)),
+        ],
         compiler_params=pltpu.CompilerParams(vmem_limit_bytes=12 * 2**20),
         name="pack",
     )(far(query), far(key), far(value), far(logit), far(decay_input))
 
 
 GROUP = 8
+WIDE_GROUP = 16
 
 
 def column_of(ref, n):
@@ -150,7 +161,7 @@
     lane = lax.broadcasted_iota(jnp.int32, (C, chunks), 1)
 
     def group(g, key_columns):
-        ns = [g * GROUP + k for k in range(GROUP)]
+        ns = [g * WIDE_GROUP + k for k in range(WIDE_GROUP)]
         keys = [x_ref[n, 0:C] for n in ns]
         products = [dot_nt(k, k) for k in keys]
         cum_c = [column_of(cum_col_ref, n) for n in ns]
@@ -206,7 +217,7 @@
         return key_columns
 
     key_col_ref[...] = lax.fori_loop(
-        0, chunks // GROUP, group, jnp.zeros((C, chunks), F32)
+        0, chunks // WIDE_GROUP, group, jnp.zeros((C, chunks), F32)
     )
 
 
@@ -598,7 +609,6 @@
     )
     blocks = lax.all_to_all(blocks, "sp", split_axis=0, concat_axis=0, tiled=True)
     recurrent = recurrence(blocks, added_log_decay.reshape(-1, C), head_decay_rate)
-    recurrent, found = lax.optimization_barrier((recurrent, found))
     returned = lax.all_to_all(recurrent, "sp", split_axis=0, concat_axis=0, tiled=True)
     weights = list(found)
     for b in found:

time: 202 us -> 212 us (1.050)
  starting transfers between devices: 22.1 us -> 44.5 us
  waiting for transfers between devices: 35.7 us -> 27.3 us
    ppermute x4, starting transfers between devices: 1.39 us -> 25.5 us  [layer(): weights.append(lax.ppermute(b, 'dp_1', [(0, 1), (1, 0)]))]
    all_to_all x1, waiting for transfers between devices: 17.6 us -> 0.01 us  [layer(): lax.all_to_all(blocks, 'sp', split_axis=0, concat_axis=0, tiled=True)]
    ppermute x3, waiting for transfers between devices: 13.6 us -> 22.4 us  [gathered(): found.append(lax.ppermute(block, 'dp_0', pairs))]
  transfers between devices with their start and end apart: 9 -> 9, of which waited for: 3 -> 3; matrix products, arithmetic and copies ran while one was open for 0% -> 0% of each run, Pallas kernels for 9% -> 8%
where the time goes in v5:
time: 212 us; the launch traced here: 211 us
  blocking collectives  91.7 us (43%)
  Pallas kernels  46.8 us (22%)
  starting transfers between devices  44.5 us (21%)
  waiting for transfers between devices  27.3 us (13%)
    all_to_all x1, blocking collectives, layer(): rows = lax.all_to_all(rows, SP_DP, split_axis=0, concat_axis=0, tiled=True)  46.1 us
    all_to_all x1, blocking collectives, layer(): back = lax.all_to_all(made, SP_DP, split_axis=0, concat_axis=0, tiled=True)  45.6 us
    ppermute x4, starting transfers between devices, layer(): weights.append(lax.ppermute(b, 'dp_1', [(0, 1), (1, 0)]))  25.5 us
    ppermute x3, waiting for transfers between devices, gathered(): found.append(lax.ppermute(block, 'dp_0', pairs))  22.4 us
    pallas_call x1, Pallas kernels, expert(): pl.pallas_call(expert_kernel, out_shape=jax.ShapeDtypeStruct(rows.shape,...  15.1 us
    pallas_call x1, Pallas kernels, recurrence(): pl.pallas_call(recurrence_kernel, out_shape=jax.ShapeDtypeStruct((chunks,...  10.6 us
    all_to_all x1, starting transfers between devices, layer(): lax.all_to_all(blocks, 'sp', split_axis=0, concat_axis=0, tiled=True)  8.43 us
    pallas_call x1, Pallas kernels, project(): pl.pallas_call(project_kernel, out_shape=(jax.ShapeDtypeStruct((tokens, t...  7.4 us
  transfers between devices with their start and end apart: 9, of which 3 were waited for; matrix products, arithmetic and copies ran while one was open for 0% of the time, Pallas kernels for 8%

profile of v5, /device:TPU:1, one launch (start us, length us, event | category | flops | bytes accessed | tf_op | source)
XLA Modules:
  0.0 211.2 jit_solution(11583040603054172215)
XLA Ops:
  0.0 0.0 copy-start.6
  0.0 0.0 copy-start.5
  0.0 3.4 %pack.1 = bf16[16,400,128]{2,1,0:T(8,128)(2,1)} custom-call(bf16[1,128,2048]{2,1,0:T(8,128)(2,1)} %q_ref.1, bf16[1,128,2048]{2,1,0:T(8,128)(2,1)} %k_ref.1, bf16[1,128,2048]{2,1,0:T(8,128)(2,1)} %v_ref.1, bf16[1,16,128]{2,1,0:T(8,128)(2,1)} %bitcast.41, bf16[1,16,128]{2,1,0:T(8,128)(2,1)} %bitcast.42), custom_call_target="tpu_custom_call" | custom-call | tf_op jit(solution)/shard_map/pack/pallas_call | solution.py:88
  3.4 8.4 %all-to-all-start = ((bf16[16,400,128]{2,1,0:T(8,128)(2,1)}), bf16[16,400,128]{2,1,0:T(8,128)(2,1)S(1)}, u32[]{:S(2)}, u32[]{:S(2)}) async-start(bf16[16,400,128]{2,1,0:T(8,128)(2,1)} %pack.1), calls=%async_computation | async-start | bytes 3276800 | tf_op jit(solution)/shard_map/all_to_all | solution.py:610
  11.9 0.0 copy-done.6
  11.9 2.8 %collective-permute-start.2 = (bf16[2048,256]{1,0:T(8,128)(2,1)S(1)}, bf16[2048,256]{1,0:T(8,128)(2,1)}, u32[]{:S(2)}, u32[]{:S(2)}) collective-permute-start(bf16[2048,256]{1,0:T(8,128)(2,1)S(1)} %copy-done.6), channel_id=1, source_target_pairs={{0,6},{2,0},{4,2},{6,4},{1,7},{3,1},{5,3},{7,5},{8,14},{10,8},{12,... | collective-permute-start | bytes 3145736 | tf_op jit(solution)/shard_map/ppermute | solution.py:570
  14.7 0.3 collective-permute-start.1
  15.0 0.7 collective-permute-start
  15.7 1.8 collective-permute-start.3
  18.2 19.1 %collective-permute-done.2.rest_3_ = bf16[2048,256]{1,0:T(8,128)(2,1)} collective-permute-done((bf16[2048,256]{1,0:T(8,128)(2,1)S(1)}, bf16[2048,256]{1,0:T(8,128)(2,1)}, u32[]{:S(2)}, u32[]{:S(2)}) %collective-permute-start.2) | collective-permute-done | bytes 1048608 | tf_op jit(solution)/shard_map/ppermute | solution.py:570
  37.3 23.2 %collective-permute-start.6 = (bf16[2048,256]{1,0:T(8,128)(2,1)}, bf16[2048,256]{1,0:T(8,128)(2,1)}, u32[]{:S(2)}, u32[]{:S(2)}) collective-permute-start(bf16[2048,256]{1,0:T(8,128)(2,1)} %collective-permute-done.2.rest_3_), channel_id=1, source_target_pairs={{0,1},{1,0},{2,3},{3,2},{4,5},{5,4},{6,7},{7,6},{8,9},{9,8},{10,11... | collective-permute-start | bytes 3145736 | tf_op jit(solution)/shard_map/ppermute | solution.py:615
  60.5 0.0 collective-permute-done.1.rest_2_
  60.5 0.0 collective-permute-start.5
  60.5 3.3 %collective-permute-done.rest_1_ = bf16[2048,256]{1,0:T(8,128)(2,1)} collective-permute-done((bf16[2048,256]{1,0:T(8,128)(2,1)S(1)}, bf16[2048,256]{1,0:T(8,128)(2,1)}, u32[]{:S(2)}, u32[]{:S(2)}) %collective-permute-start) | collective-permute-done | bytes 1048608 | tf_op jit(solution)/shard_map/ppermute | solution.py:570
  63.9 0.5 collective-permute-start.4
  64.3 0.0 all-to-all-done.x_ref
  64.3 0.0 copy-done.5
  64.4 0.0 copy-start.3
  64.4 0.0 copy-start.1
  64.4 0.0 copy-start.4
  64.4 10.6 %recurrence.1 = bf16[16,128,128]{2,1,0:T(8,128)(2,1)} custom-call(bf16[16,400,128]{2,1,0:T(8,128)(2,1)S(1)} %all-to-all-done.x_ref, f32[16,128]{1,0:T(8,128)S(1)} %bitcast.40, f32[1]{0:T(128)S(6)} %copy.19.rate_ref), custom_call_target="tpu_custom_call" | custom-call | flops 8000000000 | bytes 2097152 | tf_op jit(solution)/shard_map/recurrence/pallas_call | solution.py:293
  74.9 6.7 %all-to-all-start.1 = ((bf16[16,128,128]{2,1,0:T(8,128)(2,1)}), bf16[16,128,128]{2,1,0:T(8,128)(2,1)S(1)}, u32[]{:S(2)}, u32[]{:S(2)}) async-start(bf16[16,128,128]{2,1,0:T(8,128)(2,1)} %recurrence.1), calls=%async_computation.1 | async-start | bytes 1048576 | tf_op jit(solution)/shard_map/all_to_all | solution.py:612
  81.7 0.0 copy-done.3
  81.7 6.0 %slots.1 = (s32[512]{0:T(512)S(1)}, s32[768]{0:T(1024)S(1)}) custom-call(s32[512]{0:T(512)S(1)} %bitcast.38), custom_call_target="tpu_custom_call" | custom-call | tf_op jit(solution)/shard_map/slots/pallas_call | solution.py:337
  87.7 0.1 stack.35.place_ref
  87.8 0.0 collective-permute-done.3.rest_4_
  87.8 4.8 %all-to-all-done.1.rec_ref = bf16[16,128,128]{2,1,0:T(8,128)(2,1)S(1)} async-done(((bf16[16,128,128]{2,1,0:T(8,128)(2,1)}), bf16[16,128,128]{2,1,0:T(8,128)(2,1)S(1)}, u32[]{:S(2)}, u32[]{:S(2)}) %all-to-all-start.1) | async-done | bytes 524320 | tf_op jit(solution)/shard_map/all_to_all | solution.py:612
  92.6 0.0 collective-permute-done.6.rest_7_
  92.6 0.0 collective-permute-done.5.rest_6_
  92.6 0.0 collective-permute-done.4.rest_5_
  92.6 0.0 copy-done.1
  92.6 0.0 copy-done.4
  92.7 7.4 %project.1 = (bf16[128,16,128]{2,1,0:T(8,128)(2,1)S(1)}, bf16[768,16,128]{2,1,0:T(8,128)(2,1)S(1)}) custom-call(bf16[16,128,128]{2,1,0:T(8,128)(2,1)S(1)} %all-to-all-done.1.rec_ref, bf16[1,128,2048]{2,1,0:T(8,128)(2,1)} %gate_hbm.1, f32[1,128]{1,0:T(1,128)S(1)} %bitcast.39, bf16[1,128,2048]{2,1,0:T(8,128)(2,1)} %residual_hbm.1, f32[1,2048]{1,0:T(1,128)S(1)} %bitcast.36, ...), custom_call_target="tpu_custom_call" | custom-call | flops 1000000000 | bytes 16777216 | tf_op jit(solution)/shard_map/project/pallas_call | solution.py:404
  100.1 46.1 %all_to_all.20 = bf16[128,96,128]{2,1,0:T(8,128)(2,1)S(1)} all-to-all(bf16[128,96,128]{2,1,0:T(8,128)(2,1)S(1)} %bitcast.32), channel_id=1, replica_groups=mesh['sp'=16,'dp_0'=4,'dp_1'=2] {'sp','dp_0','dp_1'}, dimensions={0} | all-to-all | bytes 6291456 | tf_op jit(solution)/shard_map/all_to_all | solution.py:627
  146.1 15.1 %expert.1 = bf16[768,16,128]{2,1,0:T(8,128)(2,1)S(1)} custom-call(bf16[768,16,128]{2,1,0:T(8,128)(2,1)S(1)} %bitcast.33, bf16[2048,1024]{1,0:T(8,128)(2,1)} %bitcast.43, bf16[2048,1024]{1,0:T(8,128)(2,1)} %bitcast.44, bf16[1024,2048]{1,0:T(8,128)(2,1)} %bitcast.45), custom_call_target="tpu_custom_call" | custom-call | flops 10000000000 | bytes 16777216 | tf_op jit(solution)/shard_map/expert/pallas_call | solution.py:497
  161.2 0.0 copy-start
  161.3 0.0 copy-start.2
  161.3 45.6 %all_to_all.21 = bf16[128,96,128]{2,1,0:T(8,128)(2,1)S(1)} all-to-all(bf16[128,96,128]{2,1,0:T(8,128)(2,1)S(1)} %bitcast.34), channel_id=1, replica_groups=mesh['sp'=16,'dp_0'=4,'dp_1'=2] {'sp','dp_0','dp_1'}, dimensions={0} | all-to-all | bytes 6291456 | tf_op jit(solution)/shard_map/all_to_all | solution.py:635
  206.9 0.0 copy-done
  206.9 0.0 copy-done.2
  206.9 4.3 %combine.1 = f32[1,128,2048]{2,1,0:T(8,128)} custom-call(bf16[768,16,128]{2,1,0:T(8,128)(2,1)S(1)} %bitcast.31, bf16[128,16,128]{2,1,0:T(8,128)(2,1)S(1)} %get-tuple-element.11.normed_ref, f32[1,2048]{1,0:T(1,128)S(1)} %bitcast.35, s32[512]{0:T(512)S(1)} %get-tuple-element.12.dest_ref, f32[512]{0:T(512)S(1)} %bitcast.37), custom_call_target="tpu_custom_call" | custom-call | tf_op jit(solution)/shard_map/combine/pallas_call | solution.py:553
Async XLA Ops:
  0.0 11.9 %copy-start.6 = (bf16[2048,256]{1,0:T(8,128)(2,1)S(1)}, bf16[2048,256]{1,0:T(8,128)(2,1)}, u32[]{:S(2)}) copy-start(bf16[2048,256]{1,0:T(8,128)(2,1)} %rest_0_.1) | copy-start | bytes 3145732
  0.0 64.3 %copy-start.5 = (f32[1,1,2048]{2,1,0:T(1,128)S(1)}, f32[1,1,2048]{2,1,0:T(1,128)}, u32[]{:S(2)}) copy-start(f32[1,1,2048]{2,1,0:T(1,128)} %param.25) | copy-start | bytes 24580
  3.4 60.9 %all-to-all-start = ((bf16[16,400,128]{2,1,0:T(8,128)(2,1)}), bf16[16,400,128]{2,1,0:T(8,128)(2,1)S(1)}, u32[]{:S(2)}, u32[]{:S(2)}) async-start(bf16[16,400,128]{2,1,0:T(8,128)(2,1)} %pack.1), calls=%async_computation | async-start | bytes 3276800 | tf_op jit(solution)/shard_map/all_to_all | solution.py:610
  11.9 25.4 %collective-permute-start.2 = (bf16[2048,256]{1,0:T(8,128)(2,1)S(1)}, bf16[2048,256]{1,0:T(8,128)(2,1)}, u32[]{:S(2)}, u32[]{:S(2)}) collective-permute-start(bf16[2048,256]{1,0:T(8,128)(2,1)S(1)} %copy-done.6), channel_id=1, source_target_pairs={{0,6},{2,0},{4,2},{6,4},{1,7},{3,1},{5,3},{7,5},{8,14},{10,8},{12,... | collective-permute-start | bytes 3145736 | tf_op jit(solution)/shard_map/ppermute | solution.py:570
  14.7 45.8 %collective-permute-start.1 = (bf16[2048,256]{1,0:T(8,128)(2,1)S(1)}, bf16[2048,256]{1,0:T(8,128)(2,1)}, u32[]{:S(2)}, u32[]{:S(2)}) collective-permute-start(bf16[2048,256]{1,0:T(8,128)(2,1)S(1)} %copy-done.6), channel_id=1, source_target_pairs={{0,4},{2,6},{4,0},{6,2},{1,5},{3,7},{5,1},{7,3},{8,12},{10,14},{12... | collective-permute-start | bytes 3145736 | tf_op jit(solution)/shard_map/ppermute | solution.py:570
  15.0 48.8 %collective-permute-start = (bf16[2048,256]{1,0:T(8,128)(2,1)S(1)}, bf16[2048,256]{1,0:T(8,128)(2,1)}, u32[]{:S(2)}, u32[]{:S(2)}) collective-permute-start(bf16[2048,256]{1,0:T(8,128)(2,1)S(1)} %copy-done.6), channel_id=1, source_target_pairs={{0,2},{2,4},{4,6},{6,0},{1,3},{3,5},{5,7},{7,1},{8,10},{10,12},{12... | collective-permute-start | bytes 3145736 | tf_op jit(solution)/shard_map/ppermute | solution.py:570
  15.7 72.1 %collective-permute-start.3 = (bf16[2048,256]{1,0:T(8,128)(2,1)S(1)}, bf16[2048,256]{1,0:T(8,128)(2,1)}, u32[]{:S(2)}, u32[]{:S(2)}) collective-permute-start(bf16[2048,256]{1,0:T(8,128)(2,1)S(1)} %copy-done.6), channel_id=1, source_target_pairs={{0,1},{1,0},{2,3},{3,2},{4,5},{5,4},{6,7},{7,6},{8,9},{9,8},{10,11... | collective-permute-start | bytes 3145736 | tf_op jit(solution)/shard_map/ppermute | solution.py:615
  37.3 55.3 %collective-permute-start.6 = (bf16[2048,256]{1,0:T(8,128)(2,1)}, bf16[2048,256]{1,0:T(8,128)(2,1)}, u32[]{:S(2)}, u32[]{:S(2)}) collective-permute-start(bf16[2048,256]{1,0:T(8,128)(2,1)} %collective-permute-done.2.rest_3_), channel_id=1, source_target_pairs={{0,1},{1,0},{2,3},{3,2},{4,5},{5,4},{6,7},{7,6},{8,9},{9,8},{10,11... | collective-permute-start | bytes 3145736 | tf_op jit(solution)/shard_map/ppermute | solution.py:615
  60.5 32.1 %collective-permute-start.5 = (bf16[2048,256]{1,0:T(8,128)(2,1)}, bf16[2048,256]{1,0:T(8,128)(2,1)}, u32[]{:S(2)}, u32[]{:S(2)}) collective-permute-start(bf16[2048,256]{1,0:T(8,128)(2,1)} %collective-permute-done.1.rest_2_), channel_id=1, source_target_pairs={{0,1},{1,0},{2,3},{3,2},{4,5},{5,4},{6,7},{7,6},{8,9},{9,8},{10,11... | collective-permute-start | bytes 3145736 | tf_op jit(solution)/shard_map/ppermute | solution.py:615
  63.9 28.8 %collective-permute-start.4 = (bf16[2048,256]{1,0:T(8,128)(2,1)}, bf16[2048,256]{1,0:T(8,128)(2,1)}, u32[]{:S(2)}, u32[]{:S(2)}) collective-permute-start(bf16[2048,256]{1,0:T(8,128)(2,1)} %collective-permute-done.rest_1_), channel_id=1, source_target_pairs={{0,1},{1,0},{2,3},{3,2},{4,5},{5,4},{6,7},{7,6},{8,9},{9,8},{10,11... | collective-permute-start | bytes 3145736 | tf_op jit(solution)/shard_map/ppermute | solution.py:615
  64.4 17.3 %copy-start.3 = (s32[1,128,4]{1,2,0:T(4,128)S(1)}, s32[1,128,4]{1,2,0:T(4,128)}, u32[]{:S(2)}) copy-start(s32[1,128,4]{1,2,0:T(4,128)} %param.30) | copy-start | bytes 6148
  64.4 28.3 %copy-start.1 = (f32[2048]{0:T(1024)S(1)}, f32[2048]{0:T(1024)}, u32[]{:S(2)}) copy-start(f32[2048]{0:T(1024)} %param.29) | copy-start | bytes 24580
  64.4 28.3 %copy-start.4 = (f32[128]{0:T(128)S(1)}, f32[128]{0:T(128)}, u32[]{:S(2)}) copy-start(f32[128]{0:T(128)} %param.27) | copy-start | bytes 1540
  74.9 17.7 %all-to-all-start.1 = ((bf16[16,128,128]{2,1,0:T(8,128)(2,1)}), bf16[16,128,128]{2,1,0:T(8,128)(2,1)S(1)}, u32[]{:S(2)}, u32[]{:S(2)}) async-start(bf16[16,128,128]{2,1,0:T(8,128)(2,1)} %recurrence.1), calls=%async_computation.1 | async-start | bytes 1048576 | tf_op jit(solution)/shard_map/all_to_all | solution.py:612
  161.2 45.7 %copy-start = (f32[2048]{0:T(1024)S(1)}, f32[2048]{0:T(1024)}, u32[]{:S(2)}) copy-start(f32[2048]{0:T(1024)} %param.35) | copy-start | bytes 24580
  161.3 45.6 %copy-start.2 = (f32[1,128,4]{1,2,0:T(4,128)S(1)}, f32[1,128,4]{1,2,0:T(4,128)}, u32[]{:S(2)}) copy-start(f32[1,128,4]{1,2,0:T(4,128)} %param.31) | copy-start | bytes 6148

commit v6 on v5

--- a/solution.py
+++ b/solution.py
@@ -118,17 +118,24 @@
 
 
 def recurrence_kernel(
-    x_ref, added_ref, rate_ref, out_ref, base_ref, weight_ref, a_ref, b_ref, qe_ref, su_ref,
-    cum_col_ref, cum_row_ref, key_col_ref, key_row_ref, write_col_ref, write_row_ref,
+    x_ref, added_ref, rate_ref, out_hbm, base_ref, weight_ref, a_ref, b_ref, qe_ref, su_ref,
+    cum_col_ref, cum_row_ref, key_col_ref, key_row_ref, write_col_ref, write_row_ref, out_ref,
+    sems,
 ):
+    def send(g):
+        part = pl.ds(g * GROUP, GROUP)
+        return pltpu.make_async_copy(out_ref.at[part], out_hbm.at[part], sems.at[g])
+
     inverse_part(
         x_ref, added_ref, rate_ref, base_ref, weight_ref, a_ref,
         cum_col_ref, cum_row_ref, key_col_ref, key_row_ref, write_col_ref, write_row_ref,
     )
     delta_part(
         x_ref, base_ref, weight_ref, a_ref, cum_col_ref, cum_row_ref, key_col_ref, key_row_ref,
-        out_ref, b_ref, qe_ref, su_ref,
-    )
+        out_ref, b_ref, qe_ref, su_ref, send,
+    )
+    for g in range(x_ref.shape[0] // GROUP):
+        send(g).wait()
 
 
 def inverse_part(
@@ -223,7 +230,7 @@
 
 def delta_part(
     x_ref, base_ref, weight_ref, a_ref, cum_col_ref, cum_row_ref, key_col_ref, key_row_ref,
-    out_ref, b_ref, qe_ref, su_ref,
+    out_ref, b_ref, qe_ref, su_ref, send,
 ):
     chunks = x_ref.shape[0]
     row, column = iotas(C, C)
@@ -277,11 +284,13 @@
 
     def step(g, state):
         state = advance(g - 1, state)
+        send(g - 1).start()
         prepare(g)
         return state
 
     state = lax.fori_loop(1, chunks // GROUP, step, jnp.zeros((C, C), F32))
     advance(chunks // GROUP - 1, state)
+    send(chunks // GROUP - 1).start()
 
 
 def recurrence(blocks, added, decay_rate):
@@ -292,12 +301,13 @@
     rows = pltpu.VMEM((chunks, C), F32)
     return pl.pallas_call(
         recurrence_kernel,
-        out_shape=jax.ShapeDtypeStruct((chunks, C, C), BF16),
+        out_shape=pltpu.HBM((chunks, C, C), BF16),
         in_specs=[VMEM, VMEM, SMEM],
-        out_specs=VMEM,
+        out_specs=HBM,
         scratch_shapes=[
             wide, pltpu.VMEM((chunks, C, C), BF16), wide, square, wide, square,
             columns, rows, columns, rows, columns, rows,
+            pltpu.VMEM((chunks, C, C), BF16), pltpu.SemaphoreType.DMA((chunks // GROUP,)),
         ],
         compiler_params=pltpu.CompilerParams(vmem_limit_bytes=24 * 2**20),
         cost_estimate=pl.CostEstimate(flops=8 * 10**9, bytes_accessed=2**21, transcendentals=0),
@@ -348,6 +358,9 @@
     )(index)
 
 
+FETCHED = 6
+
+
 def project_kernel(
     rec_ref, gate_hbm, head_gain_ref, residual_hbm, gain_ref, source_ref, place_ref,
     *rest,
@@ -357,7 +370,7 @@
     gate_copy = pltpu.make_async_copy(gate_hbm, gate_ref, sems.at[8])
     gate_copy.start()
     copies = [
-        pltpu.make_async_copy(weight_refs[k], w_ref.at[k], sems.at[k]) for k in range(8)
+        pltpu.make_async_copy(weight_refs[k], w_ref.at[k], sems.at[k]) for k in range(FETCHED)
     ]
     for copy in copies:
         copy.start()
@@ -371,7 +384,9 @@
         gate = gate_ref[0, :, columns].astype(F32)
         gate = gate / (1.0 + jnp.exp(-gate))
         gated_ref[:, columns] = (rec_ref[h].astype(F32) * head_gain * gate).astype(BF16)
-    for k in range(8):
+    for k in range(FETCHED, 8):
+        mixed_ref[place_ref[k]] = dot(gated_ref[...], weight_refs[k][...])
+    for k in range(FETCHED):
         copies[k].wait()
         mixed_ref[place_ref[k]] = dot(gated_ref[...], w_ref[k])
     total = jnp.concatenate([mixed_ref[k] for k in range(8)], axis=1)
@@ -407,14 +422,15 @@
             jax.ShapeDtypeStruct((tokens, tiles, C), BF16),
             jax.ShapeDtypeStruct((source.shape[0], tiles, C), BF16),
         ),
-        in_specs=[VMEM, HBM, VMEM, HBM, VMEM] + [SMEM] * 2 + [HBM] * 8,
+        in_specs=[VMEM, HBM, VMEM, HBM, VMEM] + [SMEM] * 2
+        + [HBM] * FETCHED + [VMEM] * (8 - FETCHED),
         out_specs=(VMEM, VMEM),
         scratch_shapes=[
             pltpu.VMEM((1, tokens, features), BF16),
             pltpu.VMEM((1, tokens, features), BF16),
             pltpu.VMEM((tokens, features), BF16),
             pltpu.VMEM((8, tokens, features // 8), F32),
-            pltpu.VMEM((8, features, features // 8), BF16),
+            pltpu.VMEM((FETCHED, features, features // 8), BF16),
             pltpu.SemaphoreType.DMA((10,)),
         ],
         compiler_params=pltpu.CompilerParams(vmem_limit_bytes=24 * 2**20),
@@ -422,7 +438,7 @@
         name="project",
     )(
         near(recurrent), far(gate), head_gain, far(residual), gain, source, place,
-        *[far(w) for w in weights],
+        *[far(w) for w in weights[:FETCHED]], *[near(w) for w in weights[FETCHED:]],
     )
 
 
@@ -436,12 +452,17 @@
     sems,
 ):
     slots_, tiles, _ = x_ref.shape
-    copies = [
-        pltpu.make_async_copy(source, target, sems.at[k])
-        for k, (source, target) in enumerate(
-            ((gate_hbm, gate_ref), (up_hbm, up_ref), (down_hbm, down_ref))
-        )
-    ]
+    blocks = hidden_ref.shape[1] // FF_BLOCK
+    copies = []
+    for f in range(blocks):
+        columns = slice(f * FF_BLOCK, (f + 1) * FF_BLOCK)
+        for source, target in ((gate_hbm, gate_ref), (up_hbm, up_ref)):
+            copies.append(
+                pltpu.make_async_copy(
+                    source.at[:, columns], target.at[:, columns], sems.at[len(copies)]
+                )
+            )
+    copies.append(pltpu.make_async_copy(down_hbm, down_ref, sems.at[len(copies)]))
     for copy in copies:
         copy.start()
     swap = swap_matrix()
@@ -458,20 +479,16 @@
         return carry
 
     lax.fori_loop(0, slots_ // (32 * TURN_UNROLL), turn, 0)
-    copies[0].wait()
-    copies[1].wait()
-
-    def widen(f, carry):
-        columns = pl.ds(pl.multiple_of(f * FF_BLOCK, FF_BLOCK), FF_BLOCK)
+    for f in range(blocks):
+        copies[2 * f].wait()
+        copies[2 * f + 1].wait()
+        columns = slice(f * FF_BLOCK, (f + 1) * FF_BLOCK)
         rows = rows_ref[...]
         gate = jnp.minimum(dot(rows, gate_ref[:, columns]), CLAMP_LIMIT)
         up = jnp.clip(dot(rows, up_ref[:, columns]), -CLAMP_LIMIT, CLAMP_LIMIT)
         hidden = gate / (1.0 + jnp.exp(-SWISH_SLOPE * gate)) * (up + 1.0)
         hidden_ref[:, columns] = hidden.astype(BF16)
-        return carry
-
-    lax.fori_loop(0, hidden_ref.shape[1] // FF_BLOCK, widen, 0)
-    copies[2].wait()
+    copies[-1].wait()
 
     def narrow(i, carry):
         start = pl.multiple_of(i * DOWN_ROWS, DOWN_ROWS)
@@ -505,7 +522,7 @@
             pltpu.VMEM(down_weight.shape, BF16),
             pltpu.VMEM((slots_, features), BF16),
             pltpu.VMEM((slots_, hidden), BF16),
-            pltpu.SemaphoreType.DMA((3,)),
+            pltpu.SemaphoreType.DMA((2 * (hidden // FF_BLOCK) + 1,)),
         ],
         compiler_params=pltpu.CompilerParams(vmem_limit_bytes=36 * 2**20),
         cost_estimate=pl.CostEstimate(flops=10**10, bytes_accessed=2**24, transcendentals=0),
@@ -513,7 +530,9 @@
     )(near(rows), far(gate_weight), far(up_weight), far(down_weight))
 
 
-def combine_kernel(back_ref, normed_ref, gain_ref, dest_ref, weight_ref, out_ref, z_ref):
+def combine_kernel(
+    back_ref, normed_ref, gain_ref, dest_ref, weight_ref, out_hbm, z_ref, out_ref, sems
+):
     tokens, tiles, _ = normed_ref.shape
     swap = swap_matrix()
     gain = gain_ref[...]
@@ -542,20 +561,31 @@
         total = jnp.concatenate([turned[j * 16 : (j + 1) * 16] for j in range(tiles)], axis=1)
         centred = total - jnp.mean(total, axis=1, keepdims=True)
         variance = jnp.mean(centred * centred, axis=1, keepdims=True)
-        out_ref[0, pl.ds(start, 16), :] = centred * lax.rsqrt(variance + 1e-05) * gain
+        out_ref[pl.ds(start, 16), :] = centred * lax.rsqrt(variance + 1e-05) * gain
+        send(i).start()
         return carry
 
+    def send(i):
+        part = pl.ds(pl.multiple_of(i * 16, 16), 16)
+        return pltpu.make_async_copy(out_ref.at[part], out_hbm.at[0, part], sems.at[i])
+
     lax.fori_loop(0, tokens // 16, finish, 0, unroll=2)
+    for i in range(tokens // 16):
+        send(i).wait()
 
 
 def combine(back, normed, gain, dest, weight):
     tokens, tiles, _ = normed.shape
     return pl.pallas_call(
         combine_kernel,
-        out_shape=jax.ShapeDtypeStruct((1, tokens, tiles * C), F32),
+        out_shape=pltpu.HBM((1, tokens, tiles * C), F32),
         in_specs=[VMEM] * 3 + [SMEM] * 2,
-        out_specs=VMEM,
-        scratch_shapes=[pltpu.VMEM((tokens, tiles, C), F32)],
+        out_specs=HBM,
+        scratch_shapes=[
+            pltpu.VMEM((tokens, tiles, C), F32),
+            pltpu.VMEM((tokens, tiles * C), F32),
+            pltpu.SemaphoreType.DMA((tokens // 16,)),
+        ],
         compiler_params=pltpu.CompilerParams(vmem_limit_bytes=12 * 2**20),
         name="combine",
     )(near(back), near(normed), gain, dest, weight)

time: 212 us -> 211 us (level)
  no operation moved by 1% of the time
where the time goes in v6:
time: 211 us; the launch traced here: 210 us
  blocking collectives  91.7 us (43%)
  Pallas kernels  45.4 us (22%)
  starting transfers between devices  44.4 us (21%)
  waiting for transfers between devices  27.5 us (13%)
    all_to_all x1, blocking collectives, layer(): rows = lax.all_to_all(rows, SP_DP, split_axis=0, concat_axis=0, tiled=True)  46.1 us
    all_to_all x1, blocking collectives, layer(): back = lax.all_to_all(made, SP_DP, split_axis=0, concat_axis=0, tiled=True)  45.6 us
    ppermute x4, starting transfers between devices, layer(): weights.append(lax.ppermute(b, 'dp_1', [(0, 1), (1, 0)]))  25.5 us
    ppermute x3, waiting for transfers between devices, gathered(): found.append(lax.ppermute(block, 'dp_0', pairs))  22.6 us
    pallas_call x1, Pallas kernels, expert(): pl.pallas_call(expert_kernel, out_shape=jax.ShapeDtypeStruct(rows.shape,...  13.9 us
    pallas_call x1, Pallas kernels, recurrence(): pl.pallas_call(recurrence_kernel, out_shape=pltpu.HBM((chunks, C, C), BF1...  10.5 us
    all_to_all x1, starting transfers between devices, layer(): lax.all_to_all(blocks, 'sp', split_axis=0, concat_axis=0, tiled=True)  8.43 us
    pallas_call x1, Pallas kernels, project(): pl.pallas_call(project_kernel, out_shape=(jax.ShapeDtypeStruct((tokens, t...  7.52 us
  transfers between devices with their start and end apart: 9, of which 3 were waited for; matrix products, arithmetic and copies ran while one was open for 0% of the time, Pallas kernels for 8%

profile of v6, /device:TPU:1, one launch (start us, length us, event | category | flops | bytes accessed | tf_op | source)
XLA Modules:
  0.0 210.1 jit_solution(381129403843467520)
XLA Ops:
  0.0 0.0 copy-start.5
  0.0 3.3 %pack.1 = bf16[16,400,128]{2,1,0:T(8,128)(2,1)} custom-call(bf16[1,128,2048]{2,1,0:T(8,128)(2,1)} %q_ref.1, bf16[1,128,2048]{2,1,0:T(8,128)(2,1)} %k_ref.1, bf16[1,128,2048]{2,1,0:T(8,128)(2,1)} %v_ref.1, bf16[1,16,128]{2,1,0:T(8,128)(2,1)} %bitcast.41, bf16[1,16,128]{2,1,0:T(8,128)(2,1)} %bitcast.42), custom_call_target="tpu_custom_call" | custom-call | tf_op jit(solution)/shard_map/pack/pallas_call | solution.py:88
  3.4 8.4 %all-to-all-start = ((bf16[16,400,128]{2,1,0:T(8,128)(2,1)}), bf16[16,400,128]{2,1,0:T(8,128)(2,1)S(1)}, u32[]{:S(2)}, u32[]{:S(2)}) async-start(bf16[16,400,128]{2,1,0:T(8,128)(2,1)} %pack.1), calls=%async_computation | async-start | bytes 3276800 | tf_op jit(solution)/shard_map/all_to_all | solution.py:640
  11.8 2.8 %collective-permute-start.2 = (bf16[2048,256]{1,0:T(8,128)(2,1)}, bf16[2048,256]{1,0:T(8,128)(2,1)}, u32[]{:S(2)}, u32[]{:S(2)}) collective-permute-start(bf16[2048,256]{1,0:T(8,128)(2,1)} %rest_0_.1), channel_id=1, source_target_pairs={{0,6},{2,0},{4,2},{6,4},{1,7},{3,1},{5,3},{7,5},{8,14},{10,8},{12,... | collective-permute-start | bytes 3145736 | tf_op jit(solution)/shard_map/ppermute | solution.py:600
  14.6 0.3 collective-permute-start.1
  14.9 0.7 collective-permute-start
  15.6 1.8 collective-permute-start.3
  18.1 19.4 %collective-permute-done.2.rest_3_ = bf16[2048,256]{1,0:T(8,128)(2,1)} collective-permute-done((bf16[2048,256]{1,0:T(8,128)(2,1)}, bf16[2048,256]{1,0:T(8,128)(2,1)}, u32[]{:S(2)}, u32[]{:S(2)}) %collective-permute-start.2) | collective-permute-done | bytes 1048608 | tf_op jit(solution)/shard_map/ppermute | solution.py:600
  37.5 23.2 %collective-permute-start.6 = (bf16[2048,256]{1,0:T(8,128)(2,1)}, bf16[2048,256]{1,0:T(8,128)(2,1)S(1)}, u32[]{:S(2)}, u32[]{:S(2)}) collective-permute-start(bf16[2048,256]{1,0:T(8,128)(2,1)} %collective-permute-done.2.rest_3_), channel_id=1, source_target_pairs={{0,1},{1,0},{2,3},{3,2},{4,5},{5,4},{6,7},{7,6},{8,9},{9,8},{10,11... | collective-permute-start | bytes 3145736 | tf_op jit(solution)/shard_map/ppermute | solution.py:645
  60.8 0.0 collective-permute-done.1.rest_2_
  60.8 0.0 collective-permute-start.5
  60.8 3.2 %collective-permute-done.rest_1_ = bf16[2048,256]{1,0:T(8,128)(2,1)} collective-permute-done((bf16[2048,256]{1,0:T(8,128)(2,1)}, bf16[2048,256]{1,0:T(8,128)(2,1)}, u32[]{:S(2)}, u32[]{:S(2)}) %collective-permute-start) | collective-permute-done | bytes 1048608 | tf_op jit(solution)/shard_map/ppermute | solution.py:600
  64.0 0.5 collective-permute-start.4
  64.5 0.0 all-to-all-done.x_ref
  64.5 0.0 copy-done.5
  64.5 0.0 copy-start.3
  64.5 0.0 copy-start.1
  64.5 0.0 copy-start.4
  64.5 10.5 %recurrence.1 = bf16[16,128,128]{2,1,0:T(8,128)(2,1)} custom-call(bf16[16,400,128]{2,1,0:T(8,128)(2,1)S(1)} %all-to-all-done.x_ref, f32[16,128]{1,0:T(8,128)S(1)} %bitcast.40, f32[1]{0:T(128)S(6)} %copy.19.rate_ref), custom_call_target="tpu_custom_call" | custom-call | flops 8000000000 | bytes 2097152 | tf_op jit(solution)/shard_map/recurrence/pallas_call | solution.py:302
  75.0 6.6 %all-to-all-start.1 = ((bf16[16,128,128]{2,1,0:T(8,128)(2,1)}), bf16[16,128,128]{2,1,0:T(8,128)(2,1)S(1)}, u32[]{:S(2)}, u32[]{:S(2)}) async-start(bf16[16,128,128]{2,1,0:T(8,128)(2,1)} %recurrence.1), calls=%async_computation.1 | async-start | bytes 1048576 | tf_op jit(solution)/shard_map/all_to_all | solution.py:642
  81.7 0.0 copy-done.3
  81.7 6.0 %slots.1 = (s32[512]{0:T(512)S(1)}, s32[768]{0:T(1024)S(1)}) custom-call(s32[512]{0:T(512)S(1)} %bitcast.38), custom_call_target="tpu_custom_call" | custom-call | tf_op jit(solution)/shard_map/slots/pallas_call | solution.py:347
  87.7 0.1 stack.35.place_ref
  87.8 0.0 collective-permute-done.3.rest_4_
  87.8 4.8 %all-to-all-done.1.rec_ref = bf16[16,128,128]{2,1,0:T(8,128)(2,1)S(1)} async-done(((bf16[16,128,128]{2,1,0:T(8,128)(2,1)}), bf16[16,128,128]{2,1,0:T(8,128)(2,1)S(1)}, u32[]{:S(2)}, u32[]{:S(2)}) %all-to-all-start.1) | async-done | bytes 524320 | tf_op jit(solution)/shard_map/all_to_all | solution.py:642
  92.6 0.0 collective-permute-done.6.rest_7_
  92.6 0.0 collective-permute-done.5.rest_6_
  92.6 0.0 collective-permute-done.4.rest_5_
  92.6 0.0 copy-done.1
  92.6 0.0 copy-done.4
  92.7 7.5 %project.1 = (bf16[128,16,128]{2,1,0:T(8,128)(2,1)S(1)}, bf16[768,16,128]{2,1,0:T(8,128)(2,1)S(1)}) custom-call(bf16[16,128,128]{2,1,0:T(8,128)(2,1)S(1)} %all-to-all-done.1.rec_ref, bf16[1,128,2048]{2,1,0:T(8,128)(2,1)} %gate_hbm.1, f32[1,128]{1,0:T(1,128)S(1)} %bitcast.39, bf16[1,128,2048]{2,1,0:T(8,128)(2,1)} %residual_hbm.1, f32[1,2048]{1,0:T(1,128)S(1)} %bitcast.36, ...), custom_call_target="tpu_custom_call" | custom-call | flops 1000000000 | bytes 16777216 | tf_op jit(solution)/shard_map/project/pallas_call | solution.py:419
  100.2 46.1 %all_to_all.20 = bf16[128,96,128]{2,1,0:T(8,128)(2,1)S(1)} all-to-all(bf16[128,96,128]{2,1,0:T(8,128)(2,1)S(1)} %bitcast.32), channel_id=1, replica_groups=mesh['sp'=16,'dp_0'=4,'dp_1'=2] {'sp','dp_0','dp_1'}, dimensions={0} | all-to-all | bytes 6291456 | tf_op jit(solution)/shard_map/all_to_all | solution.py:657
  146.2 13.9 %expert.1 = bf16[768,16,128]{2,1,0:T(8,128)(2,1)S(1)} custom-call(bf16[768,16,128]{2,1,0:T(8,128)(2,1)S(1)} %bitcast.33, bf16[2048,1024]{1,0:T(8,128)(2,1)} %bitcast.43, bf16[2048,1024]{1,0:T(8,128)(2,1)} %bitcast.44, bf16[1024,2048]{1,0:T(8,128)(2,1)} %bitcast.45), custom_call_target="tpu_custom_call" | custom-call | flops 10000000000 | bytes 16777216 | tf_op jit(solution)/shard_map/expert/pallas_call | solution.py:514
  160.2 0.0 copy-start
  160.2 0.0 copy-start.2
  160.2 45.6 %all_to_all.21 = bf16[128,96,128]{2,1,0:T(8,128)(2,1)S(1)} all-to-all(bf16[128,96,128]{2,1,0:T(8,128)(2,1)S(1)} %bitcast.34), channel_id=1, replica_groups=mesh['sp'=16,'dp_0'=4,'dp_1'=2] {'sp','dp_0','dp_1'}, dimensions={0} | all-to-all | bytes 6291456 | tf_op jit(solution)/shard_map/all_to_all | solution.py:665
  205.8 0.0 copy-done
  205.8 0.0 copy-done.2
  205.8 4.1 %combine.1 = f32[1,128,2048]{2,1,0:T(8,128)} custom-call(bf16[768,16,128]{2,1,0:T(8,128)(2,1)S(1)} %bitcast.31, bf16[128,16,128]{2,1,0:T(8,128)(2,1)S(1)} %get-tuple-element.11.normed_ref, f32[1,2048]{1,0:T(1,128)S(1)} %bitcast.35, s32[512]{0:T(512)S(1)} %get-tuple-element.12.dest_ref, f32[512]{0:T(512)S(1)} %bitcast.37), custom_call_target="tpu_custom_call" | custom-call | tf_op jit(solution)/shard_map/combine/pallas_call | solution.py:579
Async XLA Ops:
  0.0 64.5 %copy-start.5 = (f32[1,1,2048]{2,1,0:T(1,128)S(1)}, f32[1,1,2048]{2,1,0:T(1,128)}, u32[]{:S(2)}) copy-start(f32[1,1,2048]{2,1,0:T(1,128)} %param.25) | copy-start | bytes 24580
  3.4 61.1 %all-to-all-start = ((bf16[16,400,128]{2,1,0:T(8,128)(2,1)}), bf16[16,400,128]{2,1,0:T(8,128)(2,1)S(1)}, u32[]{:S(2)}, u32[]{:S(2)}) async-start(bf16[16,400,128]{2,1,0:T(8,128)(2,1)} %pack.1), calls=%async_computation | async-start | bytes 3276800 | tf_op jit(solution)/shard_map/all_to_all | solution.py:640
  11.8 25.7 %collective-permute-start.2 = (bf16[2048,256]{1,0:T(8,128)(2,1)}, bf16[2048,256]{1,0:T(8,128)(2,1)}, u32[]{:S(2)}, u32[]{:S(2)}) collective-permute-start(bf16[2048,256]{1,0:T(8,128)(2,1)} %rest_0_.1), channel_id=1, source_target_pairs={{0,6},{2,0},{4,2},{6,4},{1,7},{3,1},{5,3},{7,5},{8,14},{10,8},{12,... | collective-permute-start | bytes 3145736 | tf_op jit(solution)/shard_map/ppermute | solution.py:600
  14.6 46.2 %collective-permute-start.1 = (bf16[2048,256]{1,0:T(8,128)(2,1)}, bf16[2048,256]{1,0:T(8,128)(2,1)}, u32[]{:S(2)}, u32[]{:S(2)}) collective-permute-start(bf16[2048,256]{1,0:T(8,128)(2,1)} %rest_0_.1), channel_id=1, source_target_pairs={{0,4},{2,6},{4,0},{6,2},{1,5},{3,7},{5,1},{7,3},{8,12},{10,14},{12... | collective-permute-start | bytes 3145736 | tf_op jit(solution)/shard_map/ppermute | solution.py:600
  14.9 49.0 %collective-permute-start = (bf16[2048,256]{1,0:T(8,128)(2,1)}, bf16[2048,256]{1,0:T(8,128)(2,1)}, u32[]{:S(2)}, u32[]{:S(2)}) collective-permute-start(bf16[2048,256]{1,0:T(8,128)(2,1)} %rest_0_.1), channel_id=1, source_target_pairs={{0,2},{2,4},{4,6},{6,0},{1,3},{3,5},{5,7},{7,1},{8,10},{10,12},{12... | collective-permute-start | bytes 3145736 | tf_op jit(solution)/shard_map/ppermute | solution.py:600
  15.6 72.2 %collective-permute-start.3 = (bf16[2048,256]{1,0:T(8,128)(2,1)}, bf16[2048,256]{1,0:T(8,128)(2,1)}, u32[]{:S(2)}, u32[]{:S(2)}) collective-permute-start(bf16[2048,256]{1,0:T(8,128)(2,1)} %rest_0_.1), channel_id=1, source_target_pairs={{0,1},{1,0},{2,3},{3,2},{4,5},{5,4},{6,7},{7,6},{8,9},{9,8},{10,11... | collective-permute-start | bytes 3145736 | tf_op jit(solution)/shard_map/ppermute | solution.py:645
  37.5 55.1 %collective-permute-start.6 = (bf16[2048,256]{1,0:T(8,128)(2,1)}, bf16[2048,256]{1,0:T(8,128)(2,1)S(1)}, u32[]{:S(2)}, u32[]{:S(2)}) collective-permute-start(bf16[2048,256]{1,0:T(8,128)(2,1)} %collective-permute-done.2.rest_3_), channel_id=1, source_target_pairs={{0,1},{1,0},{2,3},{3,2},{4,5},{5,4},{6,7},{7,6},{8,9},{9,8},{10,11... | collective-permute-start | bytes 3145736 | tf_op jit(solution)/shard_map/ppermute | solution.py:645
  60.8 31.9 %collective-permute-start.5 = (bf16[2048,256]{1,0:T(8,128)(2,1)}, bf16[2048,256]{1,0:T(8,128)(2,1)}, u32[]{:S(2)}, u32[]{:S(2)}) collective-permute-start(bf16[2048,256]{1,0:T(8,128)(2,1)} %collective-permute-done.1.rest_2_), channel_id=1, source_target_pairs={{0,1},{1,0},{2,3},{3,2},{4,5},{5,4},{6,7},{7,6},{8,9},{9,8},{10,11... | collective-permute-start | bytes 3145736 | tf_op jit(solution)/shard_map/ppermute | solution.py:645
  64.0 28.7 %collective-permute-start.4 = (bf16[2048,256]{1,0:T(8,128)(2,1)}, bf16[2048,256]{1,0:T(8,128)(2,1)}, u32[]{:S(2)}, u32[]{:S(2)}) collective-permute-start(bf16[2048,256]{1,0:T(8,128)(2,1)} %collective-permute-done.rest_1_), channel_id=1, source_target_pairs={{0,1},{1,0},{2,3},{3,2},{4,5},{5,4},{6,7},{7,6},{8,9},{9,8},{10,11... | collective-permute-start | bytes 3145736 | tf_op jit(solution)/shard_map/ppermute | solution.py:645
  64.5 17.2 %copy-start.3 = (s32[1,128,4]{1,2,0:T(4,128)S(1)}, s32[1,128,4]{1,2,0:T(4,128)}, u32[]{:S(2)}) copy-start(s32[1,128,4]{1,2,0:T(4,128)} %param.30) | copy-start | bytes 6148
  64.5 28.2 %copy-start.1 = (f32[2048]{0:T(1024)S(1)}, f32[2048]{0:T(1024)}, u32[]{:S(2)}) copy-start(f32[2048]{0:T(1024)} %param.29) | copy-start | bytes 24580
  64.5 28.2 %copy-start.4 = (f32[128]{0:T(128)S(1)}, f32[128]{0:T(128)}, u32[]{:S(2)}) copy-start(f32[128]{0:T(128)} %param.27) | copy-start | bytes 1540
  75.0 17.6 %all-to-all-start.1 = ((bf16[16,128,128]{2,1,0:T(8,128)(2,1)}), bf16[16,128,128]{2,1,0:T(8,128)(2,1)S(1)}, u32[]{:S(2)}, u32[]{:S(2)}) async-start(bf16[16,128,128]{2,1,0:T(8,128)(2,1)} %recurrence.1), calls=%async_computation.1 | async-start | bytes 1048576 | tf_op jit(solution)/shard_map/all_to_all | solution.py:642
  160.2 45.7 %copy-start = (f32[2048]{0:T(1024)S(1)}, f32[2048]{0:T(1024)}, u32[]{:S(2)}) copy-start(f32[2048]{0:T(1024)} %param.35) | copy-start | bytes 24580
  160.2 45.7 %copy-start.2 = (f32[1,128,4]{1,2,0:T(4,128)S(1)}, f32[1,128,4]{1,2,0:T(4,128)}, u32[]{:S(2)}) copy-start(f32[1,128,4]{1,2,0:T(4,128)} %param.31) | copy-start | bytes 6148

commit v7 on v6

--- a/solution.py
+++ b/solution.py
@@ -362,21 +362,17 @@
 
 
 def project_kernel(
-    rec_ref, gate_hbm, head_gain_ref, residual_hbm, gain_ref, source_ref, place_ref,
+    rec_ref, gate_ref, head_gain_ref, residual_hbm, gain_ref, source_ref, place_ref,
     *rest,
 ):
     weight_refs = rest[:8]
-    normed_ref, out_ref, gate_ref, residual_ref, gated_ref, mixed_ref, w_ref, sems = rest[8:]
-    gate_copy = pltpu.make_async_copy(gate_hbm, gate_ref, sems.at[8])
-    gate_copy.start()
+    normed_ref, out_ref, residual_ref, gated_ref, mixed_ref, w_ref, sems = rest[8:]
     copies = [
         pltpu.make_async_copy(weight_refs[k], w_ref.at[k], sems.at[k]) for k in range(FETCHED)
     ]
-    for copy in copies:
+    residual_copy = pltpu.make_async_copy(residual_hbm, residual_ref, sems.at[FETCHED])
+    for copy in (*copies, residual_copy):
         copy.start()
-    residual_copy = pltpu.make_async_copy(residual_hbm, residual_ref, sems.at[9])
-    residual_copy.start()
-    gate_copy.wait()
     heads = rec_ref.shape[0]
     head_gain = head_gain_ref[...]
     for h in range(heads):
@@ -422,22 +418,21 @@
             jax.ShapeDtypeStruct((tokens, tiles, C), BF16),
             jax.ShapeDtypeStruct((source.shape[0], tiles, C), BF16),
         ),
-        in_specs=[VMEM, HBM, VMEM, HBM, VMEM] + [SMEM] * 2
+        in_specs=[VMEM, VMEM, VMEM, HBM, VMEM] + [SMEM] * 2
         + [HBM] * FETCHED + [VMEM] * (8 - FETCHED),
         out_specs=(VMEM, VMEM),
         scratch_shapes=[
             pltpu.VMEM((1, tokens, features), BF16),
-            pltpu.VMEM((1, tokens, features), BF16),
             pltpu.VMEM((tokens, features), BF16),
             pltpu.VMEM((8, tokens, features // 8), F32),
             pltpu.VMEM((FETCHED, features, features // 8), BF16),
-            pltpu.SemaphoreType.DMA((10,)),
+            pltpu.SemaphoreType.DMA((FETCHED + 1,)),
         ],
         compiler_params=pltpu.CompilerParams(vmem_limit_bytes=24 * 2**20),
         cost_estimate=pl.CostEstimate(flops=10**9, bytes_accessed=2**24, transcendentals=0),
         name="project",
     )(
-        near(recurrent), far(gate), head_gain, far(residual), gain, source, place,
+        near(recurrent), near(gate), head_gain, far(residual), gain, source, place,
         *[far(w) for w in weights[:FETCHED]], *[near(w) for w in weights[FETCHED:]],
     )
 

time: 211 us -> 211 us (level)
  no operation moved by 1% of the time
where the time goes in v7:
time: 211 us; the launch traced here: 210 us
  blocking collectives  91.7 us (43%)
  Pallas kernels  45.3 us (21%)
  starting transfers between devices  44.4 us (21%)
  waiting for transfers between devices  27.5 us (13%)
    all_to_all x1, blocking collectives, layer(): rows = lax.all_to_all(rows, SP_DP, split_axis=0, concat_axis=0, tiled=True)  46.1 us
    all_to_all x1, blocking collectives, layer(): back = lax.all_to_all(made, SP_DP, split_axis=0, concat_axis=0, tiled=True)  45.6 us
    ppermute x4, starting transfers between devices, layer(): weights.append(lax.ppermute(b, 'dp_1', [(0, 1), (1, 0)]))  25.5 us
    ppermute x3, waiting for transfers between devices, gathered(): found.append(lax.ppermute(block, 'dp_0', pairs))  22.6 us
    pallas_call x1, Pallas kernels, expert(): pl.pallas_call(expert_kernel, out_shape=jax.ShapeDtypeStruct(rows.shape,...  13.9 us
    pallas_call x1, Pallas kernels, recurrence(): pl.pallas_call(recurrence_kernel, out_shape=pltpu.HBM((chunks, C, C), BF1...  10.5 us
    all_to_all x1, starting transfers between devices, layer(): lax.all_to_all(blocks, 'sp', split_axis=0, concat_axis=0, tiled=True)  8.43 us
    pallas_call x1, Pallas kernels, project(): pl.pallas_call(project_kernel, out_shape=(jax.ShapeDtypeStruct((tokens, t...  7.49 us
  transfers between devices with their start and end apart: 9, of which 3 were waited for; matrix products, arithmetic and copies ran while one was open for 0% of the time, Pallas kernels for 8%

profile of v7, /device:TPU:1, one launch (start us, length us, event | category | flops | bytes accessed | tf_op | source)
XLA Modules:
  0.0 210.0 jit_solution(8354080748158861688)
XLA Ops:
  0.0 0.0 copy-start.6
  0.0 3.4 %pack.1 = bf16[16,400,128]{2,1,0:T(8,128)(2,1)} custom-call(bf16[1,128,2048]{2,1,0:T(8,128)(2,1)} %q_ref.1, bf16[1,128,2048]{2,1,0:T(8,128)(2,1)} %k_ref.1, bf16[1,128,2048]{2,1,0:T(8,128)(2,1)} %v_ref.1, bf16[1,16,128]{2,1,0:T(8,128)(2,1)} %bitcast.41, bf16[1,16,128]{2,1,0:T(8,128)(2,1)} %bitcast.42), custom_call_target="tpu_custom_call" | custom-call | tf_op jit(solution)/shard_map/pack/pallas_call | solution.py:88
  3.4 8.4 %all-to-all-start = ((bf16[16,400,128]{2,1,0:T(8,128)(2,1)}), bf16[16,400,128]{2,1,0:T(8,128)(2,1)S(1)}, u32[]{:S(2)}, u32[]{:S(2)}) async-start(bf16[16,400,128]{2,1,0:T(8,128)(2,1)} %pack.1), calls=%async_computation | async-start | bytes 3276800 | tf_op jit(solution)/shard_map/all_to_all | solution.py:635
  11.8 2.8 %collective-permute-start.2 = (bf16[2048,256]{1,0:T(8,128)(2,1)}, bf16[2048,256]{1,0:T(8,128)(2,1)}, u32[]{:S(2)}, u32[]{:S(2)}) collective-permute-start(bf16[2048,256]{1,0:T(8,128)(2,1)} %rest_0_.1), channel_id=1, source_target_pairs={{0,6},{2,0},{4,2},{6,4},{1,7},{3,1},{5,3},{7,5},{8,14},{10,8},{12,... | collective-permute-start | bytes 3145736 | tf_op jit(solution)/shard_map/ppermute | solution.py:595
  14.6 0.3 collective-permute-start.1
  15.0 0.7 collective-permute-start
  15.6 1.8 collective-permute-start.3
  18.1 19.4 %collective-permute-done.2.rest_3_ = bf16[2048,256]{1,0:T(8,128)(2,1)} collective-permute-done((bf16[2048,256]{1,0:T(8,128)(2,1)}, bf16[2048,256]{1,0:T(8,128)(2,1)}, u32[]{:S(2)}, u32[]{:S(2)}) %collective-permute-start.2) | collective-permute-done | bytes 1048608 | tf_op jit(solution)/shard_map/ppermute | solution.py:595
  37.5 23.2 %collective-permute-start.6 = (bf16[2048,256]{1,0:T(8,128)(2,1)}, bf16[2048,256]{1,0:T(8,128)(2,1)S(1)}, u32[]{:S(2)}, u32[]{:S(2)}) collective-permute-start(bf16[2048,256]{1,0:T(8,128)(2,1)} %collective-permute-done.2.rest_3_), channel_id=1, source_target_pairs={{0,1},{1,0},{2,3},{3,2},{4,5},{5,4},{6,7},{7,6},{8,9},{9,8},{10,11... | collective-permute-start | bytes 3145736 | tf_op jit(solution)/shard_map/ppermute | solution.py:640
  60.8 0.0 collective-permute-done.1.rest_2_
  60.8 0.0 collective-permute-start.5
  60.8 3.2 %collective-permute-done.rest_1_ = bf16[2048,256]{1,0:T(8,128)(2,1)} collective-permute-done((bf16[2048,256]{1,0:T(8,128)(2,1)}, bf16[2048,256]{1,0:T(8,128)(2,1)}, u32[]{:S(2)}, u32[]{:S(2)}) %collective-permute-start) | collective-permute-done | bytes 1048608 | tf_op jit(solution)/shard_map/ppermute | solution.py:595
  64.0 0.5 collective-permute-start.4
  64.5 0.0 all-to-all-done.x_ref
  64.5 0.0 copy-done.6
  64.5 0.0 copy-start.4
  64.5 0.0 copy-start
  64.5 0.0 copy-start.2
  64.5 0.0 copy-start.5
  64.5 10.5 %recurrence.1 = bf16[16,128,128]{2,1,0:T(8,128)(2,1)} custom-call(bf16[16,400,128]{2,1,0:T(8,128)(2,1)S(1)} %all-to-all-done.x_ref, f32[16,128]{1,0:T(8,128)S(1)} %bitcast.40, f32[1]{0:T(128)S(6)} %copy.19.rate_ref), custom_call_target="tpu_custom_call" | custom-call | flops 8000000000 | bytes 2097152 | tf_op jit(solution)/shard_map/recurrence/pallas_call | solution.py:302
  75.0 6.6 %all-to-all-start.1 = ((bf16[16,128,128]{2,1,0:T(8,128)(2,1)}), bf16[16,128,128]{2,1,0:T(8,128)(2,1)S(1)}, u32[]{:S(2)}, u32[]{:S(2)}) async-start(bf16[16,128,128]{2,1,0:T(8,128)(2,1)} %recurrence.1), calls=%async_computation.1 | async-start | bytes 1048576 | tf_op jit(solution)/shard_map/all_to_all | solution.py:637
  81.7 0.0 copy-done.4
  81.7 6.0 %slots.1 = (s32[512]{0:T(512)S(1)}, s32[768]{0:T(1024)S(1)}) custom-call(s32[512]{0:T(512)S(1)} %bitcast.38), custom_call_target="tpu_custom_call" | custom-call | tf_op jit(solution)/shard_map/slots/pallas_call | solution.py:347
  87.7 0.1 stack.35.place_ref
  87.8 0.0 collective-permute-done.3.rest_4_
  87.8 4.8 %all-to-all-done.1.rec_ref = bf16[16,128,128]{2,1,0:T(8,128)(2,1)S(1)} async-done(((bf16[16,128,128]{2,1,0:T(8,128)(2,1)}), bf16[16,128,128]{2,1,0:T(8,128)(2,1)S(1)}, u32[]{:S(2)}, u32[]{:S(2)}) %all-to-all-start.1) | async-done | bytes 524320 | tf_op jit(solution)/shard_map/all_to_all | solution.py:637
  92.6 0.0 collective-permute-done.6.rest_7_
  92.6 0.0 collective-permute-done.5.rest_6_
  92.6 0.0 collective-permute-done.4.rest_5_
  92.7 0.0 copy-done
  92.7 0.0 copy-done.2
  92.7 0.0 copy-done.5
  92.7 7.5 %project.1 = (bf16[128,16,128]{2,1,0:T(8,128)(2,1)S(1)}, bf16[768,16,128]{2,1,0:T(8,128)(2,1)S(1)}) custom-call(bf16[16,128,128]{2,1,0:T(8,128)(2,1)S(1)} %all-to-all-done.1.rec_ref, bf16[1,128,2048]{2,1,0:T(8,128)(2,1)S(1)} %copy-done, f32[1,128]{1,0:T(1,128)S(1)} %bitcast.39, bf16[1,128,2048]{2,1,0:T(8,128)(2,1)} %residual_hbm.1, f32[1,2048]{1,0:T(1,128)S(1)} %bitcast.36, ...), custom_call_target="tpu_custom_call" | custom-call | flops 1000000000 | bytes 16777216 | tf_op jit(solution)/shard_map/project/pallas_call | solution.py:415
  100.2 46.1 %all_to_all.20 = bf16[128,96,128]{2,1,0:T(8,128)(2,1)S(1)} all-to-all(bf16[128,96,128]{2,1,0:T(8,128)(2,1)S(1)} %bitcast.32), channel_id=1, replica_groups=mesh['sp'=16,'dp_0'=4,'dp_1'=2] {'sp','dp_0','dp_1'}, dimensions={0} | all-to-all | bytes 6291456 | tf_op jit(solution)/shard_map/all_to_all | solution.py:652
  146.2 13.9 %expert.1 = bf16[768,16,128]{2,1,0:T(8,128)(2,1)S(1)} custom-call(bf16[768,16,128]{2,1,0:T(8,128)(2,1)S(1)} %bitcast.33, bf16[2048,1024]{1,0:T(8,128)(2,1)} %bitcast.43, bf16[2048,1024]{1,0:T(8,128)(2,1)} %bitcast.44, bf16[1024,2048]{1,0:T(8,128)(2,1)} %bitcast.45), custom_call_target="tpu_custom_call" | custom-call | flops 10000000000 | bytes 16777216 | tf_op jit(solution)/shard_map/expert/pallas_call | solution.py:509
  160.1 0.0 copy-start.1
  160.1 0.0 copy-start.3
  160.2 45.6 %all_to_all.21 = bf16[128,96,128]{2,1,0:T(8,128)(2,1)S(1)} all-to-all(bf16[128,96,128]{2,1,0:T(8,128)(2,1)S(1)} %bitcast.34), channel_id=1, replica_groups=mesh['sp'=16,'dp_0'=4,'dp_1'=2] {'sp','dp_0','dp_1'}, dimensions={0} | all-to-all | bytes 6291456 | tf_op jit(solution)/shard_map/all_to_all | solution.py:660
  205.8 0.0 copy-done.1
  205.8 0.0 copy-done.3
  205.8 4.1 %combine.1 = f32[1,128,2048]{2,1,0:T(8,128)} custom-call(bf16[768,16,128]{2,1,0:T(8,128)(2,1)S(1)} %bitcast.31, bf16[128,16,128]{2,1,0:T(8,128)(2,1)S(1)} %get-tuple-element.11.normed_ref, f32[1,2048]{1,0:T(1,128)S(1)} %bitcast.35, s32[512]{0:T(512)S(1)} %get-tuple-element.12.dest_ref, f32[512]{0:T(512)S(1)} %bitcast.37), custom_call_target="tpu_custom_call" | custom-call | tf_op jit(solution)/shard_map/combine/pallas_call | solution.py:574
Async XLA Ops:
  0.0 64.5 %copy-start.6 = (f32[1,1,2048]{2,1,0:T(1,128)S(1)}, f32[1,1,2048]{2,1,0:T(1,128)}, u32[]{:S(2)}) copy-start(f32[1,1,2048]{2,1,0:T(1,128)} %param.25) | copy-start | bytes 24580
  3.4 61.1 %all-to-all-start = ((bf16[16,400,128]{2,1,0:T(8,128)(2,1)}), bf16[16,400,128]{2,1,0:T(8,128)(2,1)S(1)}, u32[]{:S(2)}, u32[]{:S(2)}) async-start(bf16[16,400,128]{2,1,0:T(8,128)(2,1)} %pack.1), calls=%async_computation | async-start | bytes 3276800 | tf_op jit(solution)/shard_map/all_to_all | solution.py:635
  11.8 25.7 %collective-permute-start.2 = (bf16[2048,256]{1,0:T(8,128)(2,1)}, bf16[2048,256]{1,0:T(8,128)(2,1)}, u32[]{:S(2)}, u32[]{:S(2)}) collective-permute-start(bf16[2048,256]{1,0:T(8,128)(2,1)} %rest_0_.1), channel_id=1, source_target_pairs={{0,6},{2,0},{4,2},{6,4},{1,7},{3,1},{5,3},{7,5},{8,14},{10,8},{12,... | collective-permute-start | bytes 3145736 | tf_op jit(solution)/shard_map/ppermute | solution.py:595
  14.6 46.2 %collective-permute-start.1 = (bf16[2048,256]{1,0:T(8,128)(2,1)}, bf16[2048,256]{1,0:T(8,128)(2,1)}, u32[]{:S(2)}, u32[]{:S(2)}) collective-permute-start(bf16[2048,256]{1,0:T(8,128)(2,1)} %rest_0_.1), channel_id=1, source_target_pairs={{0,4},{2,6},{4,0},{6,2},{1,5},{3,7},{5,1},{7,3},{8,12},{10,14},{12... | collective-permute-start | bytes 3145736 | tf_op jit(solution)/shard_map/ppermute | solution.py:595
  15.0 49.0 %collective-permute-start = (bf16[2048,256]{1,0:T(8,128)(2,1)}, bf16[2048,256]{1,0:T(8,128)(2,1)}, u32[]{:S(2)}, u32[]{:S(2)}) collective-permute-start(bf16[2048,256]{1,0:T(8,128)(2,1)} %rest_0_.1), channel_id=1, source_target_pairs={{0,2},{2,4},{4,6},{6,0},{1,3},{3,5},{5,7},{7,1},{8,10},{10,12},{12... | collective-permute-start | bytes 3145736 | tf_op jit(solution)/shard_map/ppermute | solution.py:595
  15.6 72.2 %collective-permute-start.3 = (bf16[2048,256]{1,0:T(8,128)(2,1)}, bf16[2048,256]{1,0:T(8,128)(2,1)}, u32[]{:S(2)}, u32[]{:S(2)}) collective-permute-start(bf16[2048,256]{1,0:T(8,128)(2,1)} %rest_0_.1), channel_id=1, source_target_pairs={{0,1},{1,0},{2,3},{3,2},{4,5},{5,4},{6,7},{7,6},{8,9},{9,8},{10,11... | collective-permute-start | bytes 3145736 | tf_op jit(solution)/shard_map/ppermute | solution.py:640
  37.5 55.1 %collective-permute-start.6 = (bf16[2048,256]{1,0:T(8,128)(2,1)}, bf16[2048,256]{1,0:T(8,128)(2,1)S(1)}, u32[]{:S(2)}, u32[]{:S(2)}) collective-permute-start(bf16[2048,256]{1,0:T(8,128)(2,1)} %collective-permute-done.2.rest_3_), channel_id=1, source_target_pairs={{0,1},{1,0},{2,3},{3,2},{4,5},{5,4},{6,7},{7,6},{8,9},{9,8},{10,11... | collective-permute-start | bytes 3145736 | tf_op jit(solution)/shard_map/ppermute | solution.py:640
  60.8 31.9 %collective-permute-start.5 = (bf16[2048,256]{1,0:T(8,128)(2,1)}, bf16[2048,256]{1,0:T(8,128)(2,1)}, u32[]{:S(2)}, u32[]{:S(2)}) collective-permute-start(bf16[2048,256]{1,0:T(8,128)(2,1)} %collective-permute-done.1.rest_2_), channel_id=1, source_target_pairs={{0,1},{1,0},{2,3},{3,2},{4,5},{5,4},{6,7},{7,6},{8,9},{9,8},{10,11... | collective-permute-start | bytes 3145736 | tf_op jit(solution)/shard_map/ppermute | solution.py:640
  64.0 28.7 %collective-permute-start.4 = (bf16[2048,256]{1,0:T(8,128)(2,1)}, bf16[2048,256]{1,0:T(8,128)(2,1)}, u32[]{:S(2)}, u32[]{:S(2)}) collective-permute-start(bf16[2048,256]{1,0:T(8,128)(2,1)} %collective-permute-done.rest_1_), channel_id=1, source_target_pairs={{0,1},{1,0},{2,3},{3,2},{4,5},{5,4},{6,7},{7,6},{8,9},{9,8},{10,11... | collective-permute-start | bytes 3145736 | tf_op jit(solution)/shard_map/ppermute | solution.py:640
  64.5 17.2 %copy-start.4 = (s32[1,128,4]{1,2,0:T(4,128)S(1)}, s32[1,128,4]{1,2,0:T(4,128)}, u32[]{:S(2)}) copy-start(s32[1,128,4]{1,2,0:T(4,128)} %param.30) | copy-start | bytes 6148
  64.5 28.2 %copy-start = (bf16[1,128,2048]{2,1,0:T(8,128)(2,1)S(1)}, bf16[1,128,2048]{2,1,0:T(8,128)(2,1)}, u32[]{:S(2)}) copy-start(bf16[1,128,2048]{2,1,0:T(8,128)(2,1)} %gate_ref.1) | copy-start | bytes 1572868
  64.5 28.2 %copy-start.2 = (f32[2048]{0:T(1024)S(1)}, f32[2048]{0:T(1024)}, u32[]{:S(2)}) copy-start(f32[2048]{0:T(1024)} %param.29) | copy-start | bytes 24580
  64.5 28.2 %copy-start.5 = (f32[128]{0:T(128)S(1)}, f32[128]{0:T(128)}, u32[]{:S(2)}) copy-start(f32[128]{0:T(128)} %param.27) | copy-start | bytes 1540
  75.0 17.6 %all-to-all-start.1 = ((bf16[16,128,128]{2,1,0:T(8,128)(2,1)}), bf16[16,128,128]{2,1,0:T(8,128)(2,1)S(1)}, u32[]{:S(2)}, u32[]{:S(2)}) async-start(bf16[16,128,128]{2,1,0:T(8,128)(2,1)} %recurrence.1), calls=%async_computation.1 | async-start | bytes 1048576 | tf_op jit(solution)/shard_map/all_to_all | solution.py:637
  160.1 45.7 %copy-start.1 = (f32[2048]{0:T(1024)S(1)}, f32[2048]{0:T(1024)}, u32[]{:S(2)}) copy-start(f32[2048]{0:T(1024)} %param.35) | copy-start | bytes 24580
  160.1 45.7 %copy-start.3 = (f32[1,128,4]{1,2,0:T(4,128)S(1)}, f32[1,128,4]{1,2,0:T(4,128)}, u32[]{:S(2)}) copy-start(f32[1,128,4]{1,2,0:T(4,128)} %param.31) | copy-start | bytes 6148
